TPU v7x, 512 devices: a whole 4x4x16 slice. The times are simulated.
512 devices in a mesh: sp: 16 (over z), tp: 4 (over y), dp: 8 (over x, core).
Axes of the slice: x: 4, y: 4, z: 16, core: 2. Of those that a mesh axis runs over, the one named last changes fastest.
Arguments:
- latent: bfloat16 [8, 4096, 2048], P('dp', 'sp'), may hold values from -6 to 6
- context: bfloat16 [8, 512, 2048], P('dp', 'sp'), may hold values from -6 to 6
- condition: bfloat16 [8, 2048], P('dp'), may hold values from -6 to 6
- mod_weight: bfloat16 [2048, 6144], P(None, ('sp', 'tp')), may hold values from -0.125 to 0.125
- norm_gain: float32 [2048], replicated, may hold values from 0.1 to 1.9
- w_query: bfloat16 [2048, 1024], P(None, 'tp'), may hold values from -0.125 to 0.125
- w_key: bfloat16 [2048, 256], P(None, 'tp'), may hold values from -0.125 to 0.125
- w_value: bfloat16 [2048, 256], P(None, 'tp'), may hold values from -0.125 to 0.125
- q_gain: float32 [64], replicated, may hold values from 0.4 to 14, as said below
- k_gain: float32 [64], replicated, may hold values from 0.4 to 14, as said below
- w_out: bfloat16 [1024, 2048], P('tp'), may hold values from -0.1875 to 0.1875
Outputs:
- mixed: bfloat16 [8, 4096, 2048], P('dp', ('sp', 'tp'))
Inputs may be any that keep to these rules, and one draw needn't show every extreme that they name: `q_gain`: gains of the normalized query channels. `k_gain`: gains of the normalized key channels.
All inputs are finite; a program needn't handle non-finite values.
Results may differ from a plain program's by a relative error of at most 0.015.
The roundings to bfloat16 on the way count: a program that leaves them out, or rounds other values in their place, can miss the bound.
Values may be sent and summed in bfloat16 or wider, within the bound.
No kernel may reach another device: no remote copies, remote signals or barrier semaphores. Data moves between devices by JAX's collectives and lax.ppermute only.
A program may use at most 64 MiB of HBM per device.

v0:
```python
import jax
import jax.numpy as jnp
from jax import lax
from jax.sharding import PartitionSpec as P

GRID_W = 64


epsilon = 1e-06
rope_base = 10000.0


def in_order(tiles, dim):
    dims = list(tiles.shape[1:])
    dims[dim] *= tiles.shape[0]
    return jnp.moveaxis(tiles, 0, dim).reshape(dims)


def copy_for_each(shard, axis):
    devices = lax.axis_size(axis)
    return lax.all_to_all(
        jnp.broadcast_to(shard[None], (devices, *shard.shape)), axis, 0, 0, tiled=True
    )


def collect(shard, axis, dim):
    return in_order(copy_for_each(shard, axis), dim)


def sent_together(arrays, axis, dim, along):
    ends, at = ([], 0)
    for a in arrays[:-1]:
        at += a.shape[along]
        ends.append(at)
    both = jnp.concatenate(arrays, axis=along)
    return tuple(jnp.split(lax.all_gather(both, axis, axis=dim, tiled=True), ends, axis=along))


def cut_along(shard, dim, devices):
    before, after = (shard.shape[:dim], shard.shape[dim + 1 :])
    return jnp.moveaxis(shard.reshape(*before, devices, -1, *after), dim, 0)


def sum_at_owner(shard, axis, dim):
    devices = lax.axis_size(axis)
    tiles = lax.all_to_all(cut_along(shard, dim, devices), axis, 0, 0, tiled=True)
    return jnp.sum(tiles.astype(jnp.float32), axis=0)


def normalize(values, gain):
    mean_sq = jnp.mean(values * values, axis=-1, keepdims=True)
    return values * lax.rsqrt(mean_sq + epsilon) * gain


def turn_half(values, cosine, sine):
    first, second = jnp.split(values, 2, axis=-1)
    return jnp.concatenate(
        [first * cosine - second * sine, first * sine + second * cosine], axis=-1
    )


def rotary(values, tables):
    row_cos, row_sin, col_cos, col_sin = tables
    by_row, by_col = jnp.split(values, 2, axis=-1)
    return jnp.concatenate(
        [turn_half(by_row, row_cos, row_sin), turn_half(by_col, col_cos, col_sin)], axis=-1
    )


def shards(
    latent,
    context,
    condition,
    mod_weight,
    norm_gain,
    w_query,
    w_key,
    w_value,
    q_gain,
    k_gain,
    w_out,
):
    samples, length, width = latent.shape
    head_dim = q_gain.shape[0]
    local_kv = w_key.shape[1] // head_dim
    group_size = w_query.shape[1] // w_key.shape[1]
    cond_act = jax.nn.silu(condition.astype(jnp.float32)).astype(jnp.bfloat16)
    mod_piece = jnp.dot(cond_act, mod_weight, preferred_element_type=jnp.float32)
    modulation = collect(mod_piece, ("sp", "tp"), 1)
    shift = modulation[:, None, :width]
    scale = modulation[:, None, width : 2 * width]
    gate = modulation[:, None, 2 * width :]
    widened = latent.astype(jnp.float32)
    hidden = (normalize(widened, norm_gain) * (1.0 + scale) + shift).astype(jnp.bfloat16)
    where = lax.axis_index("sp") * length + jnp.arange(length, dtype=jnp.int32)
    grid_row = (where // GRID_W).astype(jnp.float32)
    grid_col = (where % GRID_W).astype(jnp.float32)
    quarter = head_dim // 4
    freqs = rope_base ** (-jnp.arange(quarter, dtype=jnp.float32) / quarter)
    by_row = grid_row[:, None] * freqs[None, :]
    by_col = grid_col[:, None] * freqs[None, :]
    tables = (jnp.cos(by_row), jnp.sin(by_row), jnp.cos(by_col), jnp.sin(by_col))
    key_tables = tuple((table[:, None, :] for table in tables))
    queries = jnp.einsum("srd,df->srf", hidden, w_query, preferred_element_type=jnp.float32)
    queries = queries.reshape(samples, length, local_kv, group_size, head_dim)
    queries = jnp.transpose(queries, (0, 2, 3, 1, 4))
    queries = rotary(normalize(queries, q_gain), tables).astype(jnp.bfloat16)
    own_keys = jnp.einsum("srd,df->srf", hidden, w_key, preferred_element_type=jnp.float32)
    own_keys = own_keys.reshape(samples, length, local_kv, head_dim)
    own_keys = rotary(normalize(own_keys, k_gain), key_tables).astype(jnp.bfloat16)
    own_keys = own_keys.reshape(samples, length, local_kv * head_dim)
    own_values = jnp.einsum(
        "srd,df->srf", hidden, w_value, preferred_element_type=jnp.float32
    ).astype(jnp.bfloat16)
    count = context.shape[1]
    ctx_keys = jnp.einsum("srd,df->srf", context, w_key, preferred_element_type=jnp.float32)
    ctx_keys = normalize(ctx_keys.reshape(samples, count, local_kv, head_dim), k_gain).astype(
        jnp.bfloat16
    )
    ctx_values = jnp.einsum(
        "srd,df->srf", context, w_value, preferred_element_type=jnp.float32
    ).astype(jnp.bfloat16)
    local_k = ctx_keys.reshape(samples, count, local_kv * head_dim)
    context_k, context_v = sent_together((local_k, ctx_values), "sp", 1, 0)
    score_scale = head_dim ** (-0.5)

    def score_block(key_block):
        shaped = key_block.reshape(samples, key_block.shape[1], local_kv, head_dim)
        return (
            jnp.einsum("skgrd,snkd->skgrn", queries, shaped, preferred_element_type=jnp.float32)
            * score_scale
        )

    def weigh_values(weights, value_block):
        shaped = value_block.reshape(samples, value_block.shape[1], local_kv, head_dim)
        return jnp.einsum(
            "skgrn,snkd->skgrd",
            weights.astype(jnp.bfloat16),
            shaped,
            preferred_element_type=jnp.float32,
        )

    first_scores = score_block(context_k)
    first_max = jnp.max(first_scores, axis=-1, keepdims=True)
    first_weights = jnp.exp(first_scores - first_max)
    first_total = jnp.sum(first_weights, axis=-1, keepdims=True)
    first_acc = weigh_values(first_weights, context_v)
    key_block, value_block = sent_together((own_keys, own_values), "sp", 1, 0)
    scores = score_block(key_block)
    new_max = jnp.maximum(first_max, jnp.max(scores, axis=-1, keepdims=True))
    shrink = jnp.exp(first_max - new_max)
    weights = jnp.exp(scores - new_max)
    new_total = first_total * shrink + jnp.sum(weights, axis=-1, keepdims=True)
    new_acc = first_acc * shrink + weigh_values(weights, value_block)
    attended = (new_acc / new_total).astype(jnp.bfloat16)
    attended = jnp.transpose(attended, (3, 0, 1, 2, 4)).reshape(
        length, samples, local_kv * group_size * head_dim
    )
    kept_rows = length // lax.axis_size("tp")
    term = jnp.einsum("rsf,fd->rsd", attended, w_out, preferred_element_type=jnp.float32)
    projected = sum_at_owner(
        lax.optimization_barrier(term.astype(jnp.bfloat16))
        .astype(jnp.float32)
        .astype(jnp.bfloat16),
        "tp",
        0,
    )
    projected = jnp.transpose(projected, (1, 0, 2))
    residual = lax.dynamic_slice_in_dim(widened, lax.axis_index("tp") * kept_rows, kept_rows, 1)
    return (residual + gate * projected).astype(jnp.bfloat16)


def solution(mesh):
    placed = (
        P("dp", "sp", None),
        P("dp", "sp", None),
        P("dp", None),
        P(None, ("sp", "tp")),
        P(),
        P(None, "tp"),
        P(None, "tp"),
        P(None, "tp"),
        P(),
        P(),
        P("tp", None),
    )
    return jax.shard_map(
        shards, mesh=mesh, in_specs=placed, out_specs=P("dp", ("sp", "tp"), None), check_vma=False
    )
```

profile of v0, /device:TPU:6, one launch (start us, length us, event | category | flops | bytes accessed | tf_op | source)
XLA Modules:
  0.0 165.9 jit_solution(2387909187312785744)
XLA Ops:
  6.6 1.4 convolution_bitcast_fusion.1
  7.9 0.7 broadcast_in_dim.2
  8.6 19.0 %all-to-all-start = ((f32[64,1,96]{2,1,0:T(1,128)}), f32[64,1,96]{2,1,0:T(1,128)}, u32[]{:S(2)}, u32[]{:S(2)}) async-start(f32[64,1,96]{2,1,0:T(1,128)} %broadcast_in_dim.2), calls=%async_computation | async-start | bytes 65536 | tf_op jit(solution)/shard_map/all_to_all | solution.py:21
  27.6 1.5 multiply_reduce_fusion.1
  29.1 0.6 add_rsqrt_fusion.2
  29.7 1.5 copy.18
  31.6 0.7 fusion.46
  32.3 0.6 multiply_power_fusion
  32.9 9.1 %all-to-all-done = f32[64,1,96]{2,1,0:T(1,128)} async-done(((f32[64,1,96]{2,1,0:T(1,128)}), f32[64,1,96]{2,1,0:T(1,128)}, u32[]{:S(2)}, u32[]{:S(2)}) %all-to-all-start) | async-done | bytes 24608 | tf_op jit(solution)/shard_map/all_to_all | solution.py:21
  42.0 0.5 broadcast.422
  42.5 2.0 %reduce.18 = f32[64,96]{1,0:T(8,128)} reduce(f32[64,1,96]{2,1,0:T(1,128)} %all-to-all-done, f32[]{:T(128)} %broadcast.422), dimensions={1}, to_apply=%all_to_all.6.reduce_sub_computation.3 | reduce | bytes 49156 | tf_op jit(solution)/shard_map/all_to_all | solution.py:21
  44.5 1.5 reshape_transpose.3
  46.0 0.8 fusion.65
  46.8 1.3 multiply_reduce_fusion.4
  48.2 1.4 fusion.10
  49.9 0.6 pad_maximum_fusion.1
  50.7 0.7 pad_maximum_fusion.4
  51.4 28.3 %all_gather.6 = bf16[2,512,64]{2,1,0:T(8,128)(2,1)S(1)} all-gather(bf16[2,32,64]{2,1,0:T(8,128)(2,1)S(1)} %pad_maximum_fusion.4), channel_id=1, replica_groups=mesh['sp'=16,'tp'=4,'dp'=8] {'sp'}, dimensions={1}, use_global_device_ids=true | all-gather | bytes 139264 | tf_op jit(solution)/shard_map/all_gather | solution.py:36
  79.7 0.9 multiply_cosine_fusion.3
  80.6 1.4 multiply_reduce_fusion.3
  82.2 0.5 multiply_reduce_fusion.2
  82.8 0.6 fusion.5
  83.3 31.0 %all-gather.2.cloned.1.call-done = bf16[2,4096,64]{1,2,0:T(8,128)(2,1)} async-done(((bf16[2,256,64]{1,2,0:T(8,128)(2,1)}), bf16[2,4096,64]{1,2,0:T(8,128)(2,1)}) %all-gather.2.cloned.1.call-update) | async-done | bytes 1048592 | tf_op jit(solution)/shard_map/all_gather | solution.py:36
  114.3 9.1 %multiply_reduce_fusion = (f32[4,256]{1,0:T(4,128)S(1)}, f32[4,256,4096]{2,1,0:T(8,128)}) fusion(bf16[2,4096,64]{1,2,0:T(8,128)(2,1)} %all-gather.2.cloned.1.call-done, bf16[4,256,16]{1,2,0:T(8,128)(2,1)S(1)} %get-tuple-element.11, bf16[4,256,16]{1,2,0:T(8,128)(2,1)S(1)} %get-tuple-element.12, bf16[4,256,16]{1,2,0:T(8,128)(2,1)S(1)} %get-tuple-element.8, ...), kind=kOutput, calls=%fused_computation.1 | convolution fusion | flops 545782784 | bytes 17436672 | tf_op jit(solution)/shard_map/skgrd,snkd->skgrn/dot_general | solution.py:130
  123.4 8.7 %fusion = f32[4,256]{1,0:T(4,128)S(1)} fusion(f32[4,256,4096]{2,1,0:T(8,128)} %get-tuple-element.37, f32[4,256]{1,0:T(4,128)S(1)} %max.14), kind=kLoop, calls=%fused_computation.2 | loop fusion | flops 12581888 | bytes 16785408 | tf_op jit(solution)/shard_map/reduce_sum | solution.py:153
  132.2 7.4 %fusion.2 = f32[4,256,64]{1,2,0:T(8,128)S(1)} fusion(f32[4,256,4096]{2,1,0:T(8,128)} %get-tuple-element.37, f32[4,256]{1,0:T(4,128)S(1)} %max.14, bf16[2,4096,64]{1,2,0:T(8,128)(2,1)S(1)} %copy-done.3), kind=kOutput, calls=%fused_computation.4 | convolution fusion | flops 549453824 | bytes 17567744 | tf_op jit(solution)/shard_map/skgrn,snkd->skgrd/dot_general | solution.py:136
  139.6 0.6 fusion.9
  140.2 1.5 fusion.4
  141.7 4.5 %all-to-all-start.1 = ((bf16[4,64,1,2048]{3,1,2,0:T(8,128)(2,1)}), bf16[4,64,1,2048]{3,1,2,0:T(8,128)(2,1)S(1)}, u32[]{:S(2)}, u32[]{:S(2)}) async-start(bf16[4,64,1,2048]{3,1,2,0:T(8,128)(2,1)} %bitcast.104), calls=%async_computation.1 | async-start | bytes 2097152 | tf_op jit(solution)/shard_map/all_to_all | solution.py:46
  146.2 1.6 convert_element_type.85
  147.8 9.3 %all-to-all-done.1 = bf16[4,64,1,2048]{3,1,2,0:T(8,128)(2,1)S(1)} async-done(((bf16[4,64,1,2048]{3,1,2,0:T(8,128)(2,1)}), bf16[4,64,1,2048]{3,1,2,0:T(8,128)(2,1)S(1)}, u32[]{:S(2)}, u32[]{:S(2)}) %all-to-all-start.1) | async-done | bytes 1048608 | tf_op jit(solution)/shard_map/all_to_all | solution.py:46
  157.3 1.8 %fusion.21 = bf16[1,64,2048]{2,1,0:T(8,128)(2,1)} fusion(f32[64,2048]{1,0:T(8,128)S(1)} %convert_reduce_fusion, f32[1,256,2048]{2,1,0:T(8,128)} %convert_element_type.85, s32[]{:T(128)S(6)} %select_n.23, f32[2048]{0:T(1024)S(1)} %bitcast.107), kind=kLoop, calls=%fused_computation.35 | loop fusion | flops 393216 | bytes 1318916 | tf_op jit(solution)/shard_map/convert_element_type | solution.py:170
  (43 shorter events, 1.2 us)
Async XLA Ops:
  6.5 133.7 %copy-start = (bf16[256,2048]{1,0:T(8,128)(2,1)S(1)}, bf16[256,2048]{1,0:T(8,128)(2,1)}, u32[]{:S(2)}) copy-start(bf16[256,2048]{1,0:T(8,128)(2,1)} %param.21) | copy-start | bytes 3145732
  6.5 40.2 %copy-start.1 = (bf16[1,256,2048]{2,1,0:T(8,128)(2,1)S(1)}, bf16[1,256,2048]{2,1,0:T(8,128)(2,1)}, u32[]{:S(2)}) copy-start(bf16[1,256,2048]{2,1,0:T(8,128)(2,1)} %param.11) | copy-start | bytes 3145732
  6.5 24.7 %copy-start.5 = (bf16[2048,64]{0,1:T(8,128)(2,1)S(1)}, bf16[2048,64]{0,1:T(8,128)(2,1)}, u32[]{:S(2)}) copy-start(bf16[2048,64]{0,1:T(8,128)(2,1)} %param.17) | copy-start | bytes 786436
  6.5 24.7 %copy-start.4 = (bf16[1,32,2048]{2,1,0:T(8,128)(2,1)S(1)}, bf16[1,32,2048]{2,1,0:T(8,128)(2,1)}, u32[]{:S(2)}) copy-start(bf16[1,32,2048]{2,1,0:T(8,128)(2,1)} %param.12) | copy-start | bytes 393220
  6.5 25.0 %copy-start.11 = (f32[64]{0:T(128)S(1)}, f32[64]{0:T(128)}, u32[]{:S(2)}) copy-start(f32[64]{0:T(128)} %param.20) | copy-start | bytes 772
  8.6 33.4 %all-to-all-start = ((f32[64,1,96]{2,1,0:T(1,128)}), f32[64,1,96]{2,1,0:T(1,128)}, u32[]{:S(2)}, u32[]{:S(2)}) async-start(f32[64,1,96]{2,1,0:T(1,128)} %broadcast_in_dim.2), calls=%async_computation | async-start | bytes 65536 | tf_op jit(solution)/shard_map/all_to_all | solution.py:21
  27.6 86.7 %all-gather.2.cloned.1.call-start = ((), (), s32[]{:S(2)}) async-start(), calls=%async_computation.2 | async-start | bytes 1114112 | tf_op jit(solution)/shard_map/all_gather | solution.py:36
  46.0 2.1 %copy-start.6 = (bf16[2048,64]{0,1:T(8,128)(2,1)S(1)}, bf16[2048,64]{0,1:T(8,128)(2,1)}, u32[]{:S(2)}) copy-start(bf16[2048,64]{0,1:T(8,128)(2,1)} %param.18) | copy-start | bytes 786436
  46.8 2.8 %copy-start.8 = (f32[1,2048]{1,0:T(1,128)}, f32[1,2048]{1,0:T(1,128)S(1)}, u32[]{:S(2)}) copy-start(f32[1,2048]{1,0:T(1,128)S(1)} %get-tuple-element.20) | copy-start | bytes 24580
  46.8 2.8 %copy-start.9 = (f32[1,2048]{1,0:T(1,128)}, f32[1,2048]{1,0:T(1,128)S(1)}, u32[]{:S(2)}) copy-start(f32[1,2048]{1,0:T(1,128)S(1)} %get-tuple-element.21) | copy-start | bytes 24580
  48.1 1.4 copy-start.12
  48.1 1.5 copy-start.10
  48.1 2.4 %copy-start.7 = (bf16[2048,64]{0,1:T(8,128)(2,1)S(1)}, bf16[2048,64]{0,1:T(8,128)(2,1)}, u32[]{:S(2)}) copy-start(bf16[2048,64]{0,1:T(8,128)(2,1)} %param.18) | copy-start | bytes 786436
  80.6 1.5 copy-start.13
  123.4 8.7 %copy-start.3 = (bf16[2,4096,64]{1,2,0:T(8,128)(2,1)S(1)}, bf16[2,4096,64]{1,2,0:T(8,128)(2,1)}, u32[]{:S(2)}) copy-start(bf16[2,4096,64]{1,2,0:T(8,128)(2,1)} %all-gather.2.cloned.1.call-done) | copy-start | bytes 3145732
  140.2 6.0 %copy-start.2 = (bf16[1,256,2048]{2,1,0:T(8,128)(2,1)S(1)}, bf16[1,256,2048]{2,1,0:T(8,128)(2,1)}, u32[]{:S(2)}) copy-start(bf16[1,256,2048]{2,1,0:T(8,128)(2,1)} %param.11) | copy-start | bytes 3145732
  141.7 15.4 %all-to-all-start.1 = ((bf16[4,64,1,2048]{3,1,2,0:T(8,128)(2,1)}), bf16[4,64,1,2048]{3,1,2,0:T(8,128)(2,1)S(1)}, u32[]{:S(2)}, u32[]{:S(2)}) async-start(bf16[4,64,1,2048]{3,1,2,0:T(8,128)(2,1)} %bitcast.104), calls=%async_computation.1 | async-start | bytes 2097152 | tf_op jit(solution)/shard_map/all_to_all | solution.py:46
Sparse Core Ops, SparseCore 0:
  50.6 63.5 all-gather.1
where the time goes:
time: 167 us; the launch traced here: 166 us
  waiting for transfers between devices  49.4 us (30%)
  blocking collectives  28.3 us (17%)
  matrix products  25.2 us (15%)
  starting transfers between devices  23.5 us (14%)
  other arithmetic  21.7 us (13%)
  between operations  13.7 us (8%)
  local copies, waits for them, and re-layouts  4.17 us (2%)
    all_gather x1, waiting for transfers between devices, sent_together(): lax.all_gather(both, axis, axis=dim, tiled=True)  31 us
    all_gather x1, blocking collectives, sent_together(): lax.all_gather(both, axis, axis=dim, tiled=True)  28.3 us
    all_to_all x1, starting transfers between devices, copy_for_each(): lax.all_to_all(jnp.broadcast_to(shard[None], (devices, *shard.shape)), ax...  19 us
    dot_general x2, matrix products, score_block(): jnp.einsum('skgrd,snkd->skgrn', queries, shaped, preferred_element_type=j...  9.69 us
    all_to_all x1, waiting for transfers between devices, sum_at_owner(): lax.all_to_all(cut_along(shard, dim, devices), axis, 0, 0, tiled=True)  9.31 us
    all_to_all x1, waiting for transfers between devices, copy_for_each(): lax.all_to_all(jnp.broadcast_to(shard[None], (devices, *shard.shape)), ax...  9.12 us
    reduce_sum x1, other arithmetic, shards(): new_total = first_total * shrink + jnp.sum(weights, axis=-1, keepdims=True)  8.71 us
    dot_general x2, matrix products, weigh_values(): jnp.einsum('skgrn,snkd->skgrd', weights.astype(jnp.bfloat16), shaped, pre...  8.06 us
  transfers between devices with their start and end apart: 3, of which 3 were waited for; matrix products, arithmetic and copies ran while one was open for 7% of the time, Pallas kernels for 0%

commit v1 on v0

v1 whole, which is shorter than its diff:
```python
import functools

import jax
import jax.numpy as jnp
from jax import lax
from jax.experimental import pallas as pl
from jax.experimental.pallas import tpu as pltpu
from jax.sharding import PartitionSpec as P

GRID_W = 64
LANES = 128
KEY_STEP = 512

epsilon = 1e-06
rope_base = 10000.0


def copy_for_each(shard, axis):
    devices = lax.axis_size(axis)
    return lax.all_to_all(
        jnp.broadcast_to(shard[None], (devices, *shard.shape)), axis, 0, 0, tiled=True
    )


def rotary_tables(first, rows, extra, head_dim):
    shape = (rows + extra, LANES)
    row = lax.broadcasted_iota(jnp.int32, shape, 0)
    lane = lax.broadcasted_iota(jnp.int32, shape, 1)
    where = first + row
    quarter = head_dim // 4
    place = jnp.where(lane % head_dim < head_dim // 2, where // GRID_W, where % GRID_W)
    place = jnp.where(row < rows, place, 0)
    freqs = rope_base ** (-(lane % quarter).astype(jnp.float32) / quarter)
    angle = place.astype(jnp.float32) * freqs
    sine = jnp.sin(angle)
    return jnp.cos(angle), jnp.where(lane % (2 * quarter) < quarter, -sine, sine)


def project(
    lat_ref,
    ctx_ref,
    mod_ref,
    gain_ref,
    wq_ref,
    wk_ref,
    wv_ref,
    qg_ref,
    kg_ref,
    cos_ref,
    sin_ref,
    q_ref,
    kv_ref,
    gate_ref,
    hid_ref,
    mods_ref,
):
    rows, width = lat_ref.shape
    count = ctx_ref.shape[0]
    head_dim = qg_ref.shape[1]
    pieces, _, piece = mod_ref.shape
    for j in range(pieces):
        mods_ref[0:1, piece * j : piece * (j + 1)] = mod_ref[j]
    shift = mods_ref[0:1, 0:width]
    scale = 1.0 + mods_ref[0:1, width : 2 * width]
    gate_ref[...] = mods_ref[0:1, 2 * width : 3 * width]
    gain = gain_ref[...]
    step = 32
    for r in range(0, rows, step):
        x = lat_ref[r : r + step, :].astype(jnp.float32)
        mean_sq = jnp.mean(x * x, axis=-1, keepdims=True)
        hidden = x * lax.rsqrt(mean_sq + epsilon) * gain * scale + shift
        hid_ref[r : r + step, :] = hidden.astype(jnp.bfloat16)
    hid_ref[rows:, :] = ctx_ref[...]

    lane = lax.broadcasted_iota(jnp.int32, (1, LANES), 1)
    low = lane < head_dim
    first = lane % (head_dim // 2) < head_dim // 4
    a = lax.broadcasted_iota(jnp.int32, (LANES, LANES), 0) // head_dim
    b = lax.broadcasted_iota(jnp.int32, (LANES, LANES), 1) // head_dim
    average = jnp.where(a == b, 1.0 / head_dim, 0.0).astype(jnp.float32)

    def turned(values, gains, cosine, sine):
        mean_sq = jnp.dot(
            values * values,
            average,
            preferred_element_type=jnp.float32,
            precision=lax.Precision.HIGHEST,
        )
        values = values * lax.rsqrt(mean_sq + epsilon) * gains
        ahead = pltpu.roll(values, LANES - head_dim // 4, 1)
        behind = pltpu.roll(values, head_dim // 4, 1)
        return values * cosine + jnp.where(first, ahead, behind) * sine

    qg = jnp.concatenate([qg_ref[...]] * 2, axis=1)
    kg = jnp.concatenate([kg_ref[...]] * 2, axis=1)
    cosine, sine = cos_ref[...], sin_ref[...]
    hid = hid_ref[...]
    keys = jnp.dot(hid, wk_ref[...], preferred_element_type=jnp.float32)
    values = jnp.dot(hid, wv_ref[...], preferred_element_type=jnp.float32)
    both = jnp.concatenate([keys, values], axis=1)
    kv_ref[...] = jnp.where(low, turned(both, kg, cosine, sine), both).astype(jnp.bfloat16)
    queries = jnp.dot(hid[:rows], wq_ref[...], preferred_element_type=jnp.float32)
    zero = jnp.zeros((), jnp.bfloat16)
    for g in range(queries.shape[1] // LANES):
        pair = turned(
            queries[:, LANES * g : LANES * (g + 1)], qg, cosine[:rows], sine[:rows]
        )
        pair = pair.astype(jnp.bfloat16).astype(jnp.float32) * head_dim**-0.5
        other = pltpu.roll(pair, head_dim, 1)
        q_ref[2 * g] = jnp.where(low, pair, 0.0).astype(jnp.bfloat16)
        q_ref[2 * g + 1] = jnp.where(low, other, 0.0).astype(jnp.bfloat16)


def attend(q_ref, kv_ref, o_ref, s_ref):
    heads, rows, _ = q_ref.shape
    head_dim = o_ref.shape[1] // heads
    total_keys = kv_ref.shape[0]
    steps = total_keys // KEY_STEP
    for h in range(heads):
        q = q_ref[h]
        m = jnp.full((rows, LANES), -jnp.inf, jnp.float32)
        for c in range(steps):
            part = slice(c * KEY_STEP, (c + 1) * KEY_STEP)
            s = lax.dot_general(
                q, kv_ref[part, :], (((1,), (1,)), ((), ())), preferred_element_type=jnp.float32
            )
            s_ref[h % 2, :, part] = s
            for j in range(0, KEY_STEP, LANES):
                m = jnp.maximum(m, s[:, j : j + LANES])
        row_max = jnp.max(m, axis=1, keepdims=True)
        total = jnp.zeros((rows, LANES), jnp.float32)
        acc = jnp.zeros((rows, LANES), jnp.float32)
        for c in range(steps):
            part = slice(c * KEY_STEP, (c + 1) * KEY_STEP)
            p = jnp.exp(s_ref[h % 2, :, part] - row_max)
            for j in range(0, KEY_STEP, LANES):
                total = total + p[:, j : j + LANES]
            acc = acc + jnp.dot(
                p.astype(jnp.bfloat16), kv_ref[part, :], preferred_element_type=jnp.float32
            )
        total = jnp.sum(total, axis=1, keepdims=True)
        o_ref[:, head_dim * h : head_dim * (h + 1)] = (acc[:, head_dim:] / total).astype(
            jnp.bfloat16
        )


def finish(at_ref, att_ref, w_ref, lat_ref, gate_ref, out_ref):
    projected = 0.0
    for g in range(att_ref.shape[0]):
        term = jnp.dot(att_ref[g], w_ref[g], preferred_element_type=jnp.float32)
        projected = projected + term.astype(jnp.bfloat16).astype(jnp.float32)
    residual = lat_ref[...].astype(jnp.float32)
    out_ref[...] = (residual + gate_ref[...] * projected).astype(jnp.bfloat16)


def shards(
    latent,
    context,
    condition,
    mod_weight,
    norm_gain,
    w_query,
    w_key,
    w_value,
    q_gain,
    k_gain,
    w_out,
):
    _, length, width = latent.shape
    count = context.shape[1]
    head_dim = q_gain.shape[0]
    heads = w_query.shape[1] // head_dim
    sp, tp = lax.axis_size("sp"), lax.axis_size("tp")
    cond_act = jax.nn.silu(condition.astype(jnp.float32)).astype(jnp.bfloat16)
    mod_piece = jnp.dot(cond_act, mod_weight, preferred_element_type=jnp.float32)
    modulation = copy_for_each(mod_piece, ("sp", "tp"))
    cosine, sine = rotary_tables(lax.axis_index("sp") * length, length, count, head_dim)

    queries, own_kv, gate = pl.pallas_call(
        project,
        out_shape=(
            jax.ShapeDtypeStruct((heads, length, LANES), jnp.bfloat16),
            jax.ShapeDtypeStruct((length + count, LANES), jnp.bfloat16),
            jax.ShapeDtypeStruct((1, width), jnp.float32),
        ),
        scratch_shapes=[
            pltpu.VMEM((length + count, width), jnp.bfloat16),
            pltpu.VMEM((8, 3 * width), jnp.float32),
        ],
        compiler_params=pltpu.CompilerParams(vmem_limit_bytes=40 * 2**20),
        name="project",
    )(
        latent[0],
        context[0],
        modulation,
        norm_gain[None],
        w_query,
        w_key,
        w_value,
        q_gain[None],
        k_gain[None],
        cosine,
        sine,
    )
    all_kv = copy_for_each(own_kv, "sp").reshape(sp * (length + count), LANES)
    late_w_out, _ = lax.optimization_barrier((w_out, own_kv))
    whole_w_out = copy_for_each(late_w_out, "tp")
    attended = pl.pallas_call(
        attend,
        out_shape=jax.ShapeDtypeStruct((length, heads * head_dim), jnp.bfloat16),
        scratch_shapes=[pltpu.VMEM((2, length, all_kv.shape[0]), jnp.float32)],
        compiler_params=pltpu.CompilerParams(vmem_limit_bytes=40 * 2**20),
        name="attend",
    )(queries, all_kv)
    kept = length // tp
    attended = lax.all_to_all(
        attended.reshape(tp, kept, heads * head_dim), "tp", 0, 0, tiled=True
    )
    cols = 512
    mixed = pl.pallas_call(
        finish,
        grid_spec=pltpu.PrefetchScalarGridSpec(
            num_scalar_prefetch=1,
            grid=(width // cols,),
            in_specs=[
                pl.BlockSpec((tp, kept, heads * head_dim), lambda i, at: (0, 0, 0)),
                pl.BlockSpec((tp, heads * head_dim, cols), lambda i, at: (0, 0, i)),
                pl.BlockSpec((kept, cols), lambda i, at: (at[0], i)),
                pl.BlockSpec((1, cols), lambda i, at: (0, i)),
            ],
            out_specs=pl.BlockSpec((kept, cols), lambda i, at: (0, i)),
        ),
        out_shape=jax.ShapeDtypeStruct((kept, width), jnp.bfloat16),
        name="finish",
    )(lax.axis_index("tp").astype(jnp.int32)[None], attended, whole_w_out, latent[0], gate)
    return mixed[None]


def solution(mesh):
    placed = (
        P("dp", "sp", None),
        P("dp", "sp", None),
        P("dp", None),
        P(None, ("sp", "tp")),
        P(),
        P(None, "tp"),
        P(None, "tp"),
        P(None, "tp"),
        P(),
        P(),
        P("tp", None),
    )
    return jax.shard_map(
        shards, mesh=mesh, in_specs=placed, out_specs=P("dp", ("sp", "tp"), None), check_vma=False
    )
```

time: 167 us -> 171 us (1.024)
  waiting for transfers between devices: 49.4 us -> 108 us
  blocking collectives: 28.3 us -> 0 us
  matrix products: 25.2 us -> 0.9 us
  other arithmetic: 21.7 us -> 0.8 us
  Pallas kernels: 0 us -> 14.2 us
  between operations: 13.7 us -> 0.15 us
  local copies, waits for them, and re-layouts: 4.17 us -> 14.5 us
  starting transfers between devices: 23.5 us -> 30.8 us
    all_to_all x1 -> x3, waiting for transfers between devices: 9.12 us -> 102 us  [copy_for_each(): lax.all_to_all(jnp.broadcast_to(shard[None], (devices, *shard.shape)), ax...]
    all_gather x1 -> x0, waiting for transfers between devices: 31 us -> none  [sent_together(): lax.all_gather(both, axis, axis=dim, tiled=True)]
    all_gather x1 -> x0, blocking collectives: 28.3 us -> none  [sent_together(): lax.all_gather(both, axis, axis=dim, tiled=True)]
    dot_general x10 -> x0, matrix products: 23.8 us -> none  [the longest x2 9.69 us: score_block(): jnp.einsum('skgrd,snkd->skgrn', queries, shaped, preferred_element_type=j...]
    pallas_call x0 -> x3, Pallas kernels: none -> 14.2 us  [the longest x1 7.38 us: shards(): pl.pallas_call(attend, out_shape=jax.ShapeDtypeStruct((length, heads * he...]
    reduce_sum x4 -> x0, other arithmetic: 10.9 us -> none  [the longest x1 8.71 us: shards(): new_total = first_total * shrink + jnp.sum(weights, axis=-1, keepdims=True)]
    unnamed x29 -> x22, local copies, waits for them, and re-layouts: 1.55 us -> 10.1 us
    all_to_all x1 -> x3, starting transfers between devices: 19 us -> 27.5 us  [copy_for_each(): lax.all_to_all(jnp.broadcast_to(shard[None], (devices, *shard.shape)), ax...]
  transfers between devices with their start and end apart: 3 -> 4, of which waited for: 3 -> 4; matrix products, arithmetic and copies ran while one was open for 7% -> 2% of each run, Pallas kernels for 0% -> 4%
where the time goes in v1:
time: 171 us; the launch traced here: 170 us
  waiting for transfers between devices  108 us (63%)
  starting transfers between devices  30.8 us (18%)
  local copies, waits for them, and re-layouts  14.5 us (8%)
  Pallas kernels  14.2 us (8%)
    all_to_all x3, waiting for transfers between devices, copy_for_each(): lax.all_to_all(jnp.broadcast_to(shard[None], (devices, *shard.shape)), ax...  102 us
    all_to_all x3, starting transfers between devices, copy_for_each(): lax.all_to_all(jnp.broadcast_to(shard[None], (devices, *shard.shape)), ax...  27.5 us
    unnamed x22, local copies, waits for them, and re-layouts  10.1 us
    pallas_call x1, Pallas kernels, shards(): pl.pallas_call(attend, out_shape=jax.ShapeDtypeStruct((length, heads * he...  7.38 us
    all_to_all x1, waiting for transfers between devices, shards(): lax.all_to_all(attended.reshape(tp, kept, heads * head_dim), 'tp', 0, 0,...  5.94 us
    pallas_call x1, Pallas kernels, shards(): pl.pallas_call(finish, grid_spec=pltpu.PrefetchScalarGridSpec(num_scalar_...  4.51 us
    broadcast_in_dim x3, local copies, waits for them, and re-layouts, copy_for_each(): jnp.broadcast_to(shard[None], (devices, *shard.shape))  4.4 us
  transfers between devices with their start and end apart: 4, of which 4 were waited for; matrix products, arithmetic and copies ran while one was open for 2% of the time, Pallas kernels for 4%

profile of v1, /device:TPU:6, one launch (start us, length us, event | category | flops | bytes accessed | tf_op | source)
XLA Modules:
  0.0 169.6 jit_solution(8803013477513771268)
XLA Ops:
  0.0 0.0 copy-start
  0.0 1.0 copy-done
  1.0 0.9 convolution_bitcast_fusion
  1.9 0.6 broadcast_in_dim.36
  2.5 18.7 %all-to-all-start = ((f32[64,1,96]{2,1,0:T(1,128)}), f32[64,1,96]{2,1,0:T(1,128)S(1)}, u32[]{:S(2)}, u32[]{:S(2)}) async-start(f32[64,1,96]{2,1,0:T(1,128)} %broadcast_in_dim.36), calls=%async_computation | async-start | bytes 65536 | tf_op jit(solution)/shard_map/all_to_all | solution.py:20
  21.4 0.7 negate_select_fusion
  22.2 0.0 copy-start.8
  22.2 1.3 copy.12.wk_ref
  23.5 1.2 copy.13.wv_ref
  24.7 11.1 %all-to-all-done.mod_ref = f32[64,1,96]{2,1,0:T(1,128)S(1)} async-done(((f32[64,1,96]{2,1,0:T(1,128)}), f32[64,1,96]{2,1,0:T(1,128)S(1)}, u32[]{:S(2)}, u32[]{:S(2)}) %all-to-all-start) | async-done | bytes 24608 | tf_op jit(solution)/shard_map/all_to_all | solution.py:20
  35.8 0.0 copy-start.1
  35.8 1.2 copy-done.1
  37.1 1.2 copy-done.2
  38.3 0.9 copy-done.3
  39.2 0.7 copy-done.4
  39.9 0.7 copy-done.6
  40.6 0.7 copy-done.7
  41.2 2.3 %project.1 = (bf16[4,256,128]{2,1,0:T(8,128)(2,1)S(1)}, bf16[288,128]{1,0:T(8,128)(2,1)S(1)}, f32[1,2048]{1,0:T(1,128)S(1)}) custom-call(bf16[256,2048]{1,0:T(8,128)(2,1)S(1)} %bitcast.17, bf16[32,2048]{1,0:T(8,128)(2,1)S(1)} %bitcast.18, f32[64,1,96]{2,1,0:T(1,128)S(1)} %all-to-all-done.mod_ref, f32[1,2048]{1,0:T(1,128)S(1)} %bitcast.19, ...), custom_call_target="tpu_custom_call" | custom-call | tf_op jit(solution)/shard_map/project/pallas_call | solution.py:179
  43.5 0.0 copy-start.5
  43.5 0.6 copy-done.5
  44.1 1.2 broadcast_in_dim.40
  45.3 3.7 %all-to-all-start.1 = ((bf16[16,288,128]{2,1,0:T(8,128)(2,1)}), bf16[16,288,128]{2,1,0:T(8,128)(2,1)S(1)}, u32[]{:S(2)}, u32[]{:S(2)}) async-start(bf16[16,288,128]{2,1,0:T(8,128)(2,1)} %broadcast_in_dim.40), calls=%async_computation.1 | async-start | bytes 2359296 | tf_op jit(solution)/shard_map/all_to_all | solution.py:20
  49.0 53.9 %all-to-all-done.1 = bf16[16,288,128]{2,1,0:T(8,128)(2,1)S(1)} async-done(((bf16[16,288,128]{2,1,0:T(8,128)(2,1)}), bf16[16,288,128]{2,1,0:T(8,128)(2,1)S(1)}, u32[]{:S(2)}, u32[]{:S(2)}) %all-to-all-start.1) | async-done | bytes 1179680 | tf_op jit(solution)/shard_map/all_to_all | solution.py:20
  102.9 0.0 copy-done.8
  102.9 2.5 %broadcast_in_dim.41 = bf16[4,256,2048]{2,1,0:T(8,128)(2,1)} broadcast(bf16[256,2048]{1,0:T(8,128)(2,1)S(1)} %copy-done.8), dimensions={1,2} | broadcast | bytes 5242880 | tf_op jit(solution)/shard_map/broadcast_in_dim | solution.py:21
  105.5 5.1 %all-to-all-start.3 = ((bf16[4,256,2048]{2,1,0:T(8,128)(2,1)}), bf16[4,256,2048]{2,1,0:T(8,128)(2,1)}, u32[]{:S(2)}, u32[]{:S(2)}) async-start(bf16[4,256,2048]{2,1,0:T(8,128)(2,1)} %broadcast_in_dim.41), calls=%async_computation.3 | async-start | bytes 8388608 | tf_op jit(solution)/shard_map/all_to_all | solution.py:20
  110.6 7.4 %attend.1 = bf16[256,256]{1,0:T(8,128)(2,1)} custom-call(bf16[4,256,128]{2,1,0:T(8,128)(2,1)S(1)} %get-tuple-element.9.q_ref, bf16[4608,128]{1,0:T(8,128)(2,1)S(1)} %bitcast.15), custom_call_target="tpu_custom_call" | custom-call | tf_op jit(solution)/shard_map/attend/pallas_call | solution.py:208
  117.9 37.2 %all-to-all-done.3.w_ref = bf16[4,256,2048]{2,1,0:T(8,128)(2,1)} async-done(((bf16[4,256,2048]{2,1,0:T(8,128)(2,1)}), bf16[4,256,2048]{2,1,0:T(8,128)(2,1)}, u32[]{:S(2)}, u32[]{:S(2)}) %all-to-all-start.3) | async-done | bytes 4194336 | tf_op jit(solution)/shard_map/all_to_all | solution.py:20
  155.2 3.3 %all-to-all-start.2 = ((bf16[4,64,256]{2,1,0:T(8,128)(2,1)}), bf16[4,64,256]{2,1,0:T(8,128)(2,1)S(1)}, u32[]{:S(2)}, u32[]{:S(2)}) async-start(bf16[4,64,256]{2,1,0:T(8,128)(2,1)} %bitcast.8), calls=%async_computation.2 | async-start | bytes 262144 | tf_op jit(solution)/shard_map/all_to_all | solution.py:216
  158.5 5.9 %all-to-all-done.2.att_ref = bf16[4,64,256]{2,1,0:T(8,128)(2,1)S(1)} async-done(((bf16[4,64,256]{2,1,0:T(8,128)(2,1)}), bf16[4,64,256]{2,1,0:T(8,128)(2,1)S(1)}, u32[]{:S(2)}, u32[]{:S(2)}) %all-to-all-start.2) | async-done | bytes 131104 | tf_op jit(solution)/shard_map/all_to_all | solution.py:216
  164.4 0.7 copy-done.9
  165.1 4.5 %finish.1 = bf16[64,2048]{1,0:T(8,128)(2,1)} custom-call(s32[1]{0:T(128)} %bitcast.at_ref, bf16[4,64,256]{2,1,0:T(8,128)(2,1)} %copy-done.9, bf16[4,256,2048]{2,1,0:T(8,128)(2,1)} %all-to-all-done.3.w_ref, bf16[256,2048]{1,0:T(8,128)(2,1)} %bitcast.16, f32[1,2048]{1,0:T(1,128)} %copy-done.5), custom_call_target="tpu_custom_call" | custom-call | tf_op jit(solution)/shard_map/finish/pallas_call | solution.py:220
  (15 shorter events, 0.1 us)
Async XLA Ops:
  0.0 1.0 copy-start
  2.5 33.3 %all-to-all-start = ((f32[64,1,96]{2,1,0:T(1,128)}), f32[64,1,96]{2,1,0:T(1,128)S(1)}, u32[]{:S(2)}, u32[]{:S(2)}) async-start(f32[64,1,96]{2,1,0:T(1,128)} %broadcast_in_dim.36), calls=%async_computation | async-start | bytes 65536 | tf_op jit(solution)/shard_map/all_to_all | solution.py:20
  22.2 80.8 %copy-start.8 = (bf16[256,2048]{1,0:T(8,128)(2,1)S(1)}, bf16[256,2048]{1,0:T(8,128)(2,1)}, u32[]{:S(2)}) copy-start(bf16[256,2048]{1,0:T(8,128)(2,1)} %param.21) | copy-start | bytes 3145732
  35.8 1.2 copy-start.1
  37.1 1.2 copy-start.2
  38.3 0.9 copy-start.3
  39.2 0.7 copy-start.4
  39.9 0.7 copy-start.6
  40.5 0.7 copy-start.7
  43.5 0.6 copy-start.5
  45.3 57.6 %all-to-all-start.1 = ((bf16[16,288,128]{2,1,0:T(8,128)(2,1)}), bf16[16,288,128]{2,1,0:T(8,128)(2,1)S(1)}, u32[]{:S(2)}, u32[]{:S(2)}) async-start(bf16[16,288,128]{2,1,0:T(8,128)(2,1)} %broadcast_in_dim.40), calls=%async_computation.1 | async-start | bytes 2359296 | tf_op jit(solution)/shard_map/all_to_all | solution.py:20
  105.5 49.7 %all-to-all-start.3 = ((bf16[4,256,2048]{2,1,0:T(8,128)(2,1)}), bf16[4,256,2048]{2,1,0:T(8,128)(2,1)}, u32[]{:S(2)}, u32[]{:S(2)}) async-start(bf16[4,256,2048]{2,1,0:T(8,128)(2,1)} %broadcast_in_dim.41), calls=%async_computation.3 | async-start | bytes 8388608 | tf_op jit(solution)/shard_map/all_to_all | solution.py:20
  155.2 9.3 %all-to-all-start.2 = ((bf16[4,64,256]{2,1,0:T(8,128)(2,1)}), bf16[4,64,256]{2,1,0:T(8,128)(2,1)S(1)}, u32[]{:S(2)}, u32[]{:S(2)}) async-start(bf16[4,64,256]{2,1,0:T(8,128)(2,1)} %bitcast.8), calls=%async_computation.2 | async-start | bytes 262144 | tf_op jit(solution)/shard_map/all_to_all | solution.py:216
  164.4 0.7 copy-start.9

commit v2 on v1

v2 whole, which is shorter than its diff:
```python
import jax
import jax.numpy as jnp
from jax import lax
from jax.experimental import pallas as pl
from jax.experimental.pallas import tpu as pltpu
from jax.sharding import PartitionSpec as P

GRID_W = 64
LANES = 128
KEY_STEP = 512

epsilon = 1e-06
rope_base = 10000.0


def copy_for_each(shard, axis):
    devices = lax.axis_size(axis)
    return lax.all_to_all(
        jnp.broadcast_to(shard[None], (devices, *shard.shape)), axis, 0, 0, tiled=True
    )


def rotary_tables(first, rows, extra, head_dim):
    shape = (rows + extra, LANES)
    row = lax.broadcasted_iota(jnp.int32, shape, 0)
    lane = lax.broadcasted_iota(jnp.int32, shape, 1)
    where = first + row
    quarter = head_dim // 4
    place = jnp.where(lane % head_dim < head_dim // 2, where // GRID_W, where % GRID_W)
    place = jnp.where(row < rows, place, 0)
    freqs = rope_base ** (-(lane % quarter).astype(jnp.float32) / quarter)
    angle = place.astype(jnp.float32) * freqs
    sine = jnp.sin(angle)
    return jnp.cos(angle), jnp.where(lane % (2 * quarter) < quarter, -sine, sine)


def turner(head_dim):
    lane = lax.broadcasted_iota(jnp.int32, (1, LANES), 1)
    first = lane % (head_dim // 2) < head_dim // 4
    a = lax.broadcasted_iota(jnp.int32, (LANES, LANES), 0) // head_dim
    b = lax.broadcasted_iota(jnp.int32, (LANES, LANES), 1) // head_dim
    average = jnp.where(a == b, 1.0 / head_dim, 0.0).astype(jnp.float32)

    def scaled(values, gains):
        mean_sq = jnp.dot(
            values * values,
            average,
            preferred_element_type=jnp.float32,
            precision=lax.Precision.HIGHEST,
        )
        return values * lax.rsqrt(mean_sq + epsilon) * gains

    def turned(values, cosine, sine):
        ahead = pltpu.roll(values, LANES - head_dim // 4, 1)
        behind = pltpu.roll(values, head_dim // 4, 1)
        return values * cosine + jnp.where(first, ahead, behind) * sine

    return scaled, turned, lane < head_dim


def contract_last(a, b):
    return lax.dot_general(a, b, (((1,), (1,)), ((), ())), preferred_element_type=jnp.float32)


def start_all(pairs, sems):
    copies = [pltpu.make_async_copy(a, b, sems.at[i]) for i, (a, b) in enumerate(pairs)]
    for copy in copies:
        copy.start()
    return copies


def prepare(
    lat_hbm, ctx_hbm, wk_hbm, wv_hbm, kg_ref, inv_ref, ctx_kv_ref, lat_ref, ctx_ref, wkv_ref, sems
):
    rows = lat_ref.shape[0]
    head_dim = kg_ref.shape[1]
    copies = start_all(
        (
            (lat_hbm, lat_ref),
            (ctx_hbm, ctx_ref),
            (wk_hbm, wkv_ref.at[pl.ds(0, head_dim)]),
            (wv_hbm, wkv_ref.at[pl.ds(head_dim, head_dim)]),
        ),
        sems,
    )
    copies[0].wait()
    step = 32
    for r in range(0, rows, step):
        x = lat_ref[r : r + step, :].astype(jnp.float32)
        mean_sq = jnp.mean(x * x, axis=-1, keepdims=True)
        inv_ref[r : r + step, :] = jnp.broadcast_to(lax.rsqrt(mean_sq + epsilon), (step, LANES))
    for copy in copies[1:]:
        copy.wait()
    scaled, _, low = turner(head_dim)
    both = contract_last(ctx_ref[...], wkv_ref[...])
    kg = jnp.concatenate([kg_ref[...]] * 2, axis=1)
    ctx_kv_ref[...] = jnp.where(low, scaled(both, kg), both).astype(jnp.bfloat16)


def project(
    lat_hbm,
    wq_hbm,
    wk_hbm,
    wv_hbm,
    inv_ref,
    ctx_kv_ref,
    mod_ref,
    gain_ref,
    qg_ref,
    kg_ref,
    cos_ref,
    sin_ref,
    q_ref,
    main_ref,
    rest_ref,
    gate_ref,
    lat_ref,
    wq_ref,
    wkv_ref,
    hid_ref,
    mods_ref,
    sems,
):
    rows, width = lat_ref.shape
    main = main_ref.shape[0]
    head_dim = qg_ref.shape[1]
    copies = start_all(
        (
            (lat_hbm, lat_ref),
            (wk_hbm, wkv_ref.at[pl.ds(0, head_dim)]),
            (wv_hbm, wkv_ref.at[pl.ds(head_dim, head_dim)]),
            (wq_hbm, wq_ref),
        ),
        sems,
    )
    pieces, _, piece = mod_ref.shape
    for j in range(pieces):
        mods_ref[0:1, piece * j : piece * (j + 1)] = mod_ref[j]
    shift = mods_ref[0:1, 0:width]
    scale = 1.0 + mods_ref[0:1, width : 2 * width]
    gate_ref[...] = mods_ref[0:1, 2 * width : 3 * width]
    gain = gain_ref[...]
    step = 32
    copies[0].wait()
    for r in range(0, rows, step):
        x = lat_ref[r : r + step, :].astype(jnp.float32)
        hidden = x * inv_ref[r : r + step, 0:1] * gain * scale + shift
        hid_ref[r : r + step, :] = hidden.astype(jnp.bfloat16)

    scaled, turned, low = turner(head_dim)
    qg = jnp.concatenate([qg_ref[...]] * 2, axis=1)
    kg = jnp.concatenate([kg_ref[...]] * 2, axis=1)
    cosine, sine = cos_ref[...], sin_ref[...]
    hid = hid_ref[...]
    copies[1].wait()
    copies[2].wait()
    both = contract_last(hid, wkv_ref[...])
    both = jnp.where(low, turned(scaled(both, kg), cosine, sine), both).astype(jnp.bfloat16)
    main_ref[...] = both[:main]
    rest_ref[0 : rows - main, :] = both[main:]
    rest_ref[rows - main :, :] = ctx_kv_ref[...]
    copies[3].wait()
    queries = jnp.dot(hid, wq_ref[...], preferred_element_type=jnp.float32)
    for g in range(queries.shape[1] // LANES):
        pair = turned(scaled(queries[:, LANES * g : LANES * (g + 1)], qg), cosine, sine)
        pair = pair.astype(jnp.bfloat16).astype(jnp.float32) * head_dim**-0.5
        other = pltpu.roll(pair, head_dim, 1)
        q_ref[2 * g] = jnp.where(low, pair, 0.0).astype(jnp.bfloat16)
        q_ref[2 * g + 1] = jnp.where(low, other, 0.0).astype(jnp.bfloat16)


def attend(q_hbm, main_ref, rest_ref, w_hbm, o_ref, q_ref, s_ref, at_ref, w_ref, sems):
    copies = start_all(((q_hbm, q_ref), (w_hbm, w_ref)), sems)
    heads, rows, _ = q_ref.shape
    head_dim = at_ref.shape[1] // heads
    parts, at = [], 0
    for ref in (main_ref, rest_ref):
        count = ref.shape[0]
        for c in range(0, count, KEY_STEP):
            size = min(KEY_STEP, count - c)
            parts.append((ref, c, at, size))
            at += size
    copies[0].wait()
    for h in range(heads):
        q = q_ref[h]
        m = jnp.full((rows, LANES), -jnp.inf, jnp.float32)
        for ref, c, at, size in parts:
            s = contract_last(q, ref[c : c + size, :])
            s_ref[h % 2, :, at : at + size] = s
            for j in range(0, size, LANES):
                m = jnp.maximum(m, s[:, j : j + LANES])
        row_max = jnp.max(m, axis=1, keepdims=True)
        total = jnp.zeros((rows, LANES), jnp.float32)
        acc = jnp.zeros((rows, LANES), jnp.float32)
        for ref, c, at, size in parts:
            p = jnp.exp(s_ref[h % 2, :, at : at + size] - row_max)
            for j in range(0, size, LANES):
                total = total + p[:, j : j + LANES]
            acc = acc + jnp.dot(
                p.astype(jnp.bfloat16), ref[c : c + size, :], preferred_element_type=jnp.float32
            )
        total = jnp.sum(total, axis=1, keepdims=True)
        at_ref[:, head_dim * h : head_dim * (h + 1)] = (acc[:, head_dim:] / total).astype(
            jnp.bfloat16
        )
    copies[1].wait()
    o_ref[...] = jnp.dot(at_ref[...], w_ref[...], preferred_element_type=jnp.float32).astype(
        jnp.bfloat16
    )


def finish(at_ref, lat_hbm, terms_ref, gate_ref, out_ref, kept_ref, sems):
    kept = kept_ref.shape[0]
    at = pl.multiple_of(at_ref[0] * kept, kept)
    (copy,) = start_all(((lat_hbm.at[pl.ds(at, kept)], kept_ref),), sems)
    projected = terms_ref[0].astype(jnp.float32)
    for g in range(1, terms_ref.shape[0]):
        projected = projected + terms_ref[g].astype(jnp.float32)
    copy.wait()
    residual = kept_ref[...].astype(jnp.float32)
    out_ref[...] = (residual + gate_ref[...] * projected).astype(jnp.bfloat16)


def vmem(mebibytes):
    return pltpu.CompilerParams(vmem_limit_bytes=mebibytes * 2**20)


def in_vmem(count):
    return [pl.BlockSpec(memory_space=pltpu.VMEM)] * count


def in_hbm(count):
    return [pl.BlockSpec(memory_space=pltpu.HBM)] * count


def shards(
    latent,
    context,
    condition,
    mod_weight,
    norm_gain,
    w_query,
    w_key,
    w_value,
    q_gain,
    k_gain,
    w_out,
):
    _, length, width = latent.shape
    count = context.shape[1]
    head_dim = q_gain.shape[0]
    heads = w_query.shape[1] // head_dim
    sp, tp = lax.axis_size("sp"), lax.axis_size("tp")
    kept = length // tp
    main = length - 8
    rest = length - main + count
    half, single = jnp.bfloat16, jnp.float32
    shape = jax.ShapeDtypeStruct
    cond_act = jax.nn.silu(condition.astype(jnp.float32)).astype(jnp.bfloat16)
    mod_piece = jnp.dot(cond_act, mod_weight, preferred_element_type=jnp.float32)
    modulation = copy_for_each(mod_piece, ("sp", "tp"))
    cosine, sine = rotary_tables(lax.axis_index("sp") * length, length, 0, head_dim)

    dma = lambda count: pltpu.SemaphoreType.DMA((count,))
    wk, wv = w_key.T, w_value.T
    inverse, ctx_kv = pl.pallas_call(
        prepare,
        out_shape=(shape((length, LANES), single), shape((count, LANES), half)),
        in_specs=in_hbm(4) + in_vmem(1),
        scratch_shapes=[
            pltpu.VMEM((length, width), half),
            pltpu.VMEM((count, width), half),
            pltpu.VMEM((2 * head_dim, width), half),
            dma(4),
        ],
        compiler_params=vmem(12),
        name="prepare",
    )(latent[0], context[0], wk, wv, k_gain[None])
    queries, own_main, own_rest, gate = pl.pallas_call(
        project,
        out_shape=(
            shape((heads, length, LANES), half),
            shape((main, LANES), half),
            shape((rest, LANES), half),
            shape((1, width), single),
        ),
        in_specs=in_hbm(4) + in_vmem(8),
        scratch_shapes=[
            pltpu.VMEM((length, width), half),
            pltpu.VMEM(w_query.shape, half),
            pltpu.VMEM((2 * head_dim, width), half),
            pltpu.VMEM((length, width), half),
            pltpu.VMEM((8, 3 * width), single),
            dma(4),
        ],
        compiler_params=vmem(16),
        name="project",
    )(
        latent[0],
        w_query,
        wk,
        wv,
        inverse,
        ctx_kv,
        modulation,
        norm_gain[None],
        q_gain[None],
        k_gain[None],
        cosine,
        sine,
    )
    all_rest = copy_for_each(own_rest, "sp").reshape(sp * rest, LANES)
    all_main = lax.all_gather(own_main, "sp", axis=0, tiled=True)
    all_keys = sp * (main + rest)
    terms = pl.pallas_call(
        attend,
        out_shape=shape((length, width), half),
        in_specs=in_hbm(1) + in_vmem(2) + in_hbm(1),
        scratch_shapes=[
            pltpu.VMEM((heads, length, LANES), half),
            pltpu.VMEM((2, length, all_keys), single),
            pltpu.VMEM((length, heads * head_dim), half),
            pltpu.VMEM(w_out.shape, half),
            dma(2),
        ],
        compiler_params=vmem(32),
        name="attend",
    )(queries, all_main, all_rest, w_out)
    terms = lax.all_to_all(terms.reshape(tp, kept, width), "tp", 0, 0, tiled=True)
    mixed = pl.pallas_call(
        finish,
        out_shape=shape((kept, width), half),
        in_specs=[pl.BlockSpec(memory_space=pltpu.SMEM)] + in_hbm(1) + in_vmem(2),
        scratch_shapes=[pltpu.VMEM((kept, width), half), dma(1)],
        compiler_params=vmem(8),
        name="finish",
    )(lax.axis_index("tp").astype(jnp.int32)[None], latent[0], terms, gate)
    return mixed[None]


def solution(mesh):
    placed = (
        P("dp", "sp", None),
        P("dp", "sp", None),
        P("dp", None),
        P(None, ("sp", "tp")),
        P(),
        P(None, "tp"),
        P(None, "tp"),
        P(None, "tp"),
        P(),
        P(),
        P("tp", None),
    )
    return jax.shard_map(
        shards, mesh=mesh, in_specs=placed, out_specs=P("dp", ("sp", "tp"), None), check_vma=False
    )
```

time: 171 us -> 112 us (0.65)
  waiting for transfers between devices: 108 us -> 21.6 us
  blocking collectives: 0 us -> 38.2 us
  local copies, waits for them, and re-layouts: 14.5 us -> 8.36 us
  starting transfers between devices: 30.8 us -> 26.4 us
    all_to_all x3 -> x2, waiting for transfers between devices: 102 us -> 10.7 us  [copy_for_each(): lax.all_to_all(jnp.broadcast_to(shard[None], (devices, *shard.shape)), ax...]
    all_gather x0 -> x1, blocking collectives: none -> 38.2 us  [shards(): all_main = lax.all_gather(own_main, 'sp', axis=0, tiled=True)]
    all_to_all x1, waiting for transfers between devices: 5.94 us -> 10.9 us  [shards(): lax.all_to_all(terms.reshape(tp, kept, width), 'tp', 0, 0, tiled=True)]
    all_to_all x3 -> x2, starting transfers between devices: 27.5 us -> 22.9 us  [copy_for_each(): lax.all_to_all(jnp.broadcast_to(shard[None], (devices, *shard.shape)), ax...]
    unnamed x22 -> x28, local copies, waits for them, and re-layouts: 10.1 us -> 7.03 us
    broadcast_in_dim x3 -> x2, local copies, waits for them, and re-layouts: 4.4 us -> 1.33 us  [copy_for_each(): jnp.broadcast_to(shard[None], (devices, *shard.shape))]
    pallas_call x3 -> x4, Pallas kernels: 14.2 us -> 14.4 us  [the longest x1 9.29 us: shards(): pl.pallas_call(attend, out_shape=shape((length, width), half), in_specs=i...]
  transfers between devices with their start and end apart: 4 -> 3, of which waited for: 4 -> 2; matrix products, arithmetic and copies ran while one was open for 2% -> 1% of each run, Pallas kernels for 4% -> 1%
where the time goes in v2:
time: 112 us; the launch traced here: 111 us
  blocking collectives  38.2 us (34%)
  starting transfers between devices  26.4 us (24%)
  waiting for transfers between devices  21.6 us (19%)
  Pallas kernels  14.4 us (13%)
  local copies, waits for them, and re-layouts  8.36 us (7%)
    all_gather x1, blocking collectives, shards(): all_main = lax.all_gather(own_main, 'sp', axis=0, tiled=True)  38.2 us
    all_to_all x2, starting transfers between devices, copy_for_each(): lax.all_to_all(jnp.broadcast_to(shard[None], (devices, *shard.shape)), ax...  22.9 us
    all_to_all x1, waiting for transfers between devices, shards(): lax.all_to_all(terms.reshape(tp, kept, width), 'tp', 0, 0, tiled=True)  10.9 us
    all_to_all x2, waiting for transfers between devices, copy_for_each(): lax.all_to_all(jnp.broadcast_to(shard[None], (devices, *shard.shape)), ax...  10.7 us
    pallas_call x1, Pallas kernels, shards(): pl.pallas_call(attend, out_shape=shape((length, width), half), in_specs=i...  9.29 us
    unnamed x28, local copies, waits for them, and re-layouts  7.03 us
    all_to_all x1, starting transfers between devices, shards(): lax.all_to_all(terms.reshape(tp, kept, width), 'tp', 0, 0, tiled=True)  3.53 us
    pallas_call x1, Pallas kernels, shards(): pl.pallas_call(project, out_shape=(shape((heads, length, LANES), half), s...  3.03 us
  transfers between devices with their start and end apart: 3, of which 2 were waited for; matrix products, arithmetic and copies ran while one was open for 1% of the time, Pallas kernels for 1%

profile of v2, /device:TPU:6, one launch (start us, length us, event | category | flops | bytes accessed | tf_op | source)
XLA Modules:
  0.0 111.0 jit_solution(10957165477772613362)
XLA Ops:
  0.0 0.0 copy-start
  0.0 1.0 copy-done
  1.0 0.9 convolution_bitcast_fusion
  1.9 0.6 broadcast_in_dim.32
  2.6 18.7 %all-to-all-start = ((f32[64,1,96]{2,1,0:T(1,128)}), f32[64,1,96]{2,1,0:T(1,128)S(1)}, u32[]{:S(2)}, u32[]{:S(2)}) async-start(f32[64,1,96]{2,1,0:T(1,128)} %broadcast_in_dim.32), calls=%async_computation | async-start | bytes 65536 | tf_op jit(solution)/shard_map/all_to_all | solution.py:18
  21.5 0.0 copy-start.9
  21.5 0.7 negate_select_fusion
  22.1 0.0 copy-start.12
  22.1 0.0 copy-done.6
  22.2 0.0 copy-done.5
  22.2 0.2 copy-done.9
  22.4 0.5 copy-done.12
  22.8 1.2 %copy-done.1 = bf16[1,256,2048]{2,1,0:T(8,128)(2,1)S(1)} copy-done((bf16[1,256,2048]{2,1,0:T(8,128)(2,1)S(1)}, bf16[1,256,2048]{2,1,0:T(8,128)(2,1)}, u32[]{:S(2)}) %copy-start.1) | copy-done | bytes 1048600
  24.0 1.1 %prepare.1 = (f32[256,128]{1,0:T(8,128)S(1)}, bf16[32,128]{1,0:T(8,128)(2,1)S(1)}) custom-call(bf16[256,2048]{1,0:T(8,128)(2,1)S(1)} %bitcast.17, bf16[32,2048]{1,0:T(8,128)(2,1)S(1)} %bitcast.24, bf16[64,2048]{1,0:T(8,128)(2,1)S(1)} %bitcast.20, bf16[64,2048]{1,0:T(8,128)(2,1)S(1)} %bitcast.22, f32[1,64]{1,0:T(1,128)S(1)} %bitcast.26), custom_call_target="tpu_custom_call" | custom-call | tf_op jit(solution)/shard_map/prepare/pallas_call | solution.py:266
  25.2 0.0 copy-start.11
  25.2 10.7 %all-to-all-done.mod_ref = f32[64,1,96]{2,1,0:T(1,128)S(1)} async-done(((f32[64,1,96]{2,1,0:T(1,128)}), f32[64,1,96]{2,1,0:T(1,128)S(1)}, u32[]{:S(2)}, u32[]{:S(2)}) %all-to-all-start) | async-done | bytes 24608 | tf_op jit(solution)/shard_map/all_to_all | solution.py:18
  35.9 0.0 copy-done.2
  35.9 0.6 copy-done.13
  36.5 1.2 %copy-done.4 = bf16[2048,256]{1,0:T(8,128)(2,1)S(1)} copy-done((bf16[2048,256]{1,0:T(8,128)(2,1)S(1)}, bf16[2048,256]{1,0:T(8,128)(2,1)}, u32[]{:S(2)}) %copy-start.4) | copy-done | bytes 1048600
  37.8 3.0 %project.1 = (bf16[4,256,128]{2,1,0:T(8,128)(2,1)S(1)}, bf16[248,128]{1,0:T(8,128)(2,1)S(1)}, bf16[40,128]{1,0:T(8,128)(2,1)S(1)}, f32[1,2048]{1,0:T(1,128)S(1)}) custom-call(bf16[256,2048]{1,0:T(8,128)(2,1)S(1)} %bitcast.18, bf16[2048,256]{1,0:T(8,128)(2,1)S(1)} %copy-done.4, bf16[64,2048]{1,0:T(8,128)(2,1)S(1)} %bitcast.21, bf16[64,2048]{1,0:T(8,128)(2,1)S(1)} %bitcast.23, ...), custom_call_target="tpu_custom_call" | custom-call | tf_op jit(solution)/shard_map/project/pallas_call | solution.py:279
  40.8 0.0 copy-start.7
  40.8 0.7 copy-done.7
  41.5 0.6 copy-done.10
  42.1 0.7 broadcast_in_dim.35
  42.8 4.2 %all-to-all-start.1 = ((bf16[16,40,128]{2,1,0:T(8,128)(2,1)}), bf16[16,40,128]{2,1,0:T(8,128)(2,1)}, u32[]{:S(2)}, u32[]{:S(2)}) async-start(bf16[16,40,128]{2,1,0:T(8,128)(2,1)} %broadcast_in_dim.35), calls=%async_computation.1 | async-start | bytes 327680 | tf_op jit(solution)/shard_map/all_to_all | solution.py:18
  47.0 38.2 %all_gather.3.main_ref = bf16[3968,128]{1,0:T(8,128)(2,1)S(1)} all-gather(bf16[248,128]{1,0:T(8,128)(2,1)} %copy-done.10), channel_id=1, replica_groups=mesh['sp'=16,'tp'=4,'dp'=8] {'sp'}, dimensions={0}, use_global_device_ids=true | all-gather | bytes 1079296 | tf_op jit(solution)/shard_map/all_gather | solution.py:313
  85.2 0.0 all-to-all-done.1
  85.2 0.9 copy-done.8
  86.1 9.3 %attend.1 = bf16[256,2048]{1,0:T(8,128)(2,1)} custom-call(bf16[4,256,128]{2,1,0:T(8,128)(2,1)S(1)} %copy-done.8, bf16[3968,128]{1,0:T(8,128)(2,1)S(1)} %all_gather.3.main_ref, bf16[640,128]{1,0:T(8,128)(2,1)} %bitcast.9.rest_ref, bf16[256,2048]{1,0:T(8,128)(2,1)S(1)} %copy-done.3), custom_call_target="tpu_custom_call" | custom-call | tf_op jit(solution)/shard_map/attend/pallas_call | solution.py:315
  95.4 3.5 %all-to-all-start.2 = ((bf16[4,64,2048]{2,1,0:T(8,128)(2,1)}), bf16[4,64,2048]{2,1,0:T(8,128)(2,1)S(1)}, u32[]{:S(2)}, u32[]{:S(2)}) async-start(bf16[4,64,2048]{2,1,0:T(8,128)(2,1)} %bitcast.10), calls=%async_computation.2 | async-start | bytes 2097152 | tf_op jit(solution)/shard_map/all_to_all | solution.py:329
  99.0 10.9 %all-to-all-done.2.terms_ref = bf16[4,64,2048]{2,1,0:T(8,128)(2,1)S(1)} async-done(((bf16[4,64,2048]{2,1,0:T(8,128)(2,1)}), bf16[4,64,2048]{2,1,0:T(8,128)(2,1)S(1)}, u32[]{:S(2)}, u32[]{:S(2)}) %all-to-all-start.2) | async-done | bytes 1048608 | tf_op jit(solution)/shard_map/all_to_all | solution.py:329
  109.8 1.0 finish.1
  (20 shorter events, 0.1 us)
Async XLA Ops:
  0.0 1.0 copy-start
  1.0 21.2 %copy-start.6 = (bf16[2048,64]{0,1:T(8,128)(2,1)S(1)}, bf16[2048,64]{0,1:T(8,128)(2,1)}, u32[]{:S(2)}) copy-start(bf16[2048,64]{0,1:T(8,128)(2,1)} %param.18) | copy-start | bytes 786436
  1.9 20.2 %copy-start.5 = (bf16[2048,64]{0,1:T(8,128)(2,1)S(1)}, bf16[2048,64]{0,1:T(8,128)(2,1)}, u32[]{:S(2)}) copy-start(bf16[2048,64]{0,1:T(8,128)(2,1)} %param.17) | copy-start | bytes 786436
  2.6 33.3 %all-to-all-start = ((f32[64,1,96]{2,1,0:T(1,128)}), f32[64,1,96]{2,1,0:T(1,128)S(1)}, u32[]{:S(2)}, u32[]{:S(2)}) async-start(f32[64,1,96]{2,1,0:T(1,128)} %broadcast_in_dim.32), calls=%async_computation | async-start | bytes 65536 | tf_op jit(solution)/shard_map/all_to_all | solution.py:18
  21.5 0.9 copy-start.9
  22.1 0.7 copy-start.12
  22.8 1.2 %copy-start.1 = (bf16[1,256,2048]{2,1,0:T(8,128)(2,1)S(1)}, bf16[1,256,2048]{2,1,0:T(8,128)(2,1)}, u32[]{:S(2)}) copy-start(bf16[1,256,2048]{2,1,0:T(8,128)(2,1)} %param.11) | copy-start | bytes 3145732
  24.0 11.9 %copy-start.2 = (bf16[1,256,2048]{2,1,0:T(8,128)(2,1)S(1)}, bf16[1,256,2048]{2,1,0:T(8,128)(2,1)}, u32[]{:S(2)}) copy-start(bf16[1,256,2048]{2,1,0:T(8,128)(2,1)} %param.11) | copy-start | bytes 3145732
  25.2 10.7 %copy-start.11 = (f32[2048]{0:T(1024)S(1)}, f32[2048]{0:T(1024)}, u32[]{:S(2)}) copy-start(f32[2048]{0:T(1024)} %param.15) | copy-start | bytes 24580
  35.9 0.7 copy-start.13
  36.5 1.2 %copy-start.4 = (bf16[2048,256]{1,0:T(8,128)(2,1)S(1)}, bf16[2048,256]{1,0:T(8,128)(2,1)}, u32[]{:S(2)}) copy-start(bf16[2048,256]{1,0:T(8,128)(2,1)} %wq_hbm.1) | copy-start | bytes 3145732
  40.8 0.7 copy-start.7
  41.5 0.6 copy-start.10
  42.1 43.0 %copy-start.3 = (bf16[256,2048]{1,0:T(8,128)(2,1)S(1)}, bf16[256,2048]{1,0:T(8,128)(2,1)}, u32[]{:S(2)}) copy-start(bf16[256,2048]{1,0:T(8,128)(2,1)} %w_hbm.1) | copy-start | bytes 3145732
  42.8 42.3 %all-to-all-start.1 = ((bf16[16,40,128]{2,1,0:T(8,128)(2,1)}), bf16[16,40,128]{2,1,0:T(8,128)(2,1)}, u32[]{:S(2)}, u32[]{:S(2)}) async-start(bf16[16,40,128]{2,1,0:T(8,128)(2,1)} %broadcast_in_dim.35), calls=%async_computation.1 | async-start | bytes 327680 | tf_op jit(solution)/shard_map/all_to_all | solution.py:18
  85.2 1.0 copy-start.8
  95.4 14.4 %all-to-all-start.2 = ((bf16[4,64,2048]{2,1,0:T(8,128)(2,1)}), bf16[4,64,2048]{2,1,0:T(8,128)(2,1)S(1)}, u32[]{:S(2)}, u32[]{:S(2)}) async-start(bf16[4,64,2048]{2,1,0:T(8,128)(2,1)} %bitcast.10), calls=%async_computation.2 | async-start | bytes 2097152 | tf_op jit(solution)/shard_map/all_to_all | solution.py:329

commit v3 on v2

--- a/solution.py
+++ b/solution.py
@@ -11,13 +11,6 @@
 
 epsilon = 1e-06
 rope_base = 10000.0
-
-
-def copy_for_each(shard, axis):
-    devices = lax.axis_size(axis)
-    return lax.all_to_all(
-        jnp.broadcast_to(shard[None], (devices, *shard.shape)), axis, 0, 0, tiled=True
-    )
 
 
 def rotary_tables(first, rows, extra, head_dim):
@@ -67,6 +60,16 @@
     for copy in copies:
         copy.start()
     return copies
+
+
+def modulate(cond_ref, w_hbm, out_ref, w_ref, sems):
+    (copy,) = start_all(((w_hbm, w_ref),), sems)
+    cond = cond_ref[...].astype(jnp.float32)
+    active = (cond / (1.0 + jnp.exp(-cond))).astype(jnp.bfloat16)
+    active = jnp.broadcast_to(active, (16, active.shape[1]))
+    copy.wait()
+    piece = contract_last(active, w_ref[...])[0:1]
+    out_ref[...] = jnp.broadcast_to(piece[None], out_ref.shape)
 
 
 def prepare(
@@ -110,19 +113,23 @@
     kg_ref,
     cos_ref,
     sin_ref,
-    q_ref,
-    main_ref,
-    rest_ref,
+    q_hbm,
+    main_hbm,
+    rest_hbm,
     gate_ref,
     lat_ref,
     wq_ref,
     wkv_ref,
     hid_ref,
     mods_ref,
+    q_ref,
+    kv_ref,
     sems,
+    out_sems,
 ):
     rows, width = lat_ref.shape
-    main = main_ref.shape[0]
+    main = main_hbm.shape[0]
+    rest = rest_hbm.shape[1]
     head_dim = qg_ref.shape[1]
     copies = start_all(
         (
@@ -156,9 +163,14 @@
     copies[2].wait()
     both = contract_last(hid, wkv_ref[...])
     both = jnp.where(low, turned(scaled(both, kg), cosine, sine), both).astype(jnp.bfloat16)
-    main_ref[...] = both[:main]
-    rest_ref[0 : rows - main, :] = both[main:]
-    rest_ref[rows - main :, :] = ctx_kv_ref[...]
+    kv_ref[0:rows, :] = both
+    kv_ref[rows:, :] = ctx_kv_ref[...]
+    sent = kv_ref.at[pl.ds(main, rest)]
+    outs = start_all(
+        [(kv_ref.at[pl.ds(0, main)], main_hbm)]
+        + [(sent, rest_hbm.at[z]) for z in range(rest_hbm.shape[0])],
+        out_sems,
+    )
     copies[3].wait()
     queries = jnp.dot(hid, wq_ref[...], preferred_element_type=jnp.float32)
     for g in range(queries.shape[1] // LANES):
@@ -167,6 +179,11 @@
         other = pltpu.roll(pair, head_dim, 1)
         q_ref[2 * g] = jnp.where(low, pair, 0.0).astype(jnp.bfloat16)
         q_ref[2 * g + 1] = jnp.where(low, other, 0.0).astype(jnp.bfloat16)
+    last = pltpu.make_async_copy(q_ref, q_hbm, sems.at[4])
+    last.start()
+    for copy in outs:
+        copy.wait()
+    last.wait()
 
 
 def attend(q_hbm, main_ref, rest_ref, w_hbm, o_ref, q_ref, s_ref, at_ref, w_ref, sems):
@@ -181,28 +198,33 @@
             parts.append((ref, c, at, size))
             at += size
     copies[0].wait()
-    for h in range(heads):
-        q = q_ref[h]
-        m = jnp.full((rows, LANES), -jnp.inf, jnp.float32)
+    row_max = None
+    for h in range(heads + 1):
+        if h < heads:
+            q = q_ref[h]
+            m = jnp.full((rows, LANES), -jnp.inf, jnp.float32)
+        if h > 0:
+            total = jnp.zeros((rows, LANES), jnp.float32)
+            acc = jnp.zeros((rows, LANES), jnp.float32)
         for ref, c, at, size in parts:
-            s = contract_last(q, ref[c : c + size, :])
-            s_ref[h % 2, :, at : at + size] = s
-            for j in range(0, size, LANES):
-                m = jnp.maximum(m, s[:, j : j + LANES])
+            if h < heads:
+                s = contract_last(q, ref[c : c + size, :])
+                s_ref[h % 2, :, at : at + size] = s
+                for j in range(0, size, LANES):
+                    m = jnp.maximum(m, s[:, j : j + LANES])
+            if h > 0:
+                p = jnp.exp(s_ref[(h + 1) % 2, :, at : at + size] - row_max)
+                for j in range(0, size, LANES):
+                    total = total + p[:, j : j + LANES]
+                acc = acc + jnp.dot(
+                    p.astype(jnp.bfloat16), ref[c : c + size, :], preferred_element_type=jnp.float32
+                )
+        if h > 0:
+            total = jnp.sum(total, axis=1, keepdims=True)
+            at_ref[:, head_dim * (h - 1) : head_dim * h] = (acc[:, head_dim:] / total).astype(
+                jnp.bfloat16
+            )
         row_max = jnp.max(m, axis=1, keepdims=True)
-        total = jnp.zeros((rows, LANES), jnp.float32)
-        acc = jnp.zeros((rows, LANES), jnp.float32)
-        for ref, c, at, size in parts:
-            p = jnp.exp(s_ref[h % 2, :, at : at + size] - row_max)
-            for j in range(0, size, LANES):
-                total = total + p[:, j : j + LANES]
-            acc = acc + jnp.dot(
-                p.astype(jnp.bfloat16), ref[c : c + size, :], preferred_element_type=jnp.float32
-            )
-        total = jnp.sum(total, axis=1, keepdims=True)
-        at_ref[:, head_dim * h : head_dim * (h + 1)] = (acc[:, head_dim:] / total).astype(
-            jnp.bfloat16
-        )
     copies[1].wait()
     o_ref[...] = jnp.dot(at_ref[...], w_ref[...], preferred_element_type=jnp.float32).astype(
         jnp.bfloat16
@@ -256,12 +278,18 @@
     rest = length - main + count
     half, single = jnp.bfloat16, jnp.float32
     shape = jax.ShapeDtypeStruct
-    cond_act = jax.nn.silu(condition.astype(jnp.float32)).astype(jnp.bfloat16)
-    mod_piece = jnp.dot(cond_act, mod_weight, preferred_element_type=jnp.float32)
-    modulation = copy_for_each(mod_piece, ("sp", "tp"))
+    dma = lambda count: pltpu.SemaphoreType.DMA((count,))
+    mod_pieces = pl.pallas_call(
+        modulate,
+        out_shape=shape((sp * tp, 1, mod_weight.shape[1]), single),
+        in_specs=in_vmem(1) + in_hbm(1),
+        scratch_shapes=[pltpu.VMEM(mod_weight.shape[::-1], half), dma(1)],
+        compiler_params=vmem(8),
+        name="modulate",
+    )(condition, mod_weight.T)
+    modulation = lax.all_to_all(mod_pieces, ("sp", "tp"), 0, 0, tiled=True)
     cosine, sine = rotary_tables(lax.axis_index("sp") * length, length, 0, head_dim)
 
-    dma = lambda count: pltpu.SemaphoreType.DMA((count,))
     wk, wv = w_key.T, w_value.T
     inverse, ctx_kv = pl.pallas_call(
         prepare,
@@ -281,19 +309,23 @@
         out_shape=(
             shape((heads, length, LANES), half),
             shape((main, LANES), half),
-            shape((rest, LANES), half),
+            shape((sp, rest, LANES), half),
             shape((1, width), single),
         ),
         in_specs=in_hbm(4) + in_vmem(8),
+        out_specs=tuple(in_hbm(3) + in_vmem(1)),
         scratch_shapes=[
             pltpu.VMEM((length, width), half),
             pltpu.VMEM(w_query.shape, half),
             pltpu.VMEM((2 * head_dim, width), half),
             pltpu.VMEM((length, width), half),
             pltpu.VMEM((8, 3 * width), single),
-            dma(4),
+            pltpu.VMEM((heads, length, LANES), half),
+            pltpu.VMEM((main + rest, LANES), half),
+            dma(5),
+            dma(1 + sp),
         ],
-        compiler_params=vmem(16),
+        compiler_params=vmem(60),
         name="project",
     )(
         latent[0],
@@ -309,7 +341,7 @@
         cosine,
         sine,
     )
-    all_rest = copy_for_each(own_rest, "sp").reshape(sp * rest, LANES)
+    all_rest = lax.all_to_all(own_rest, "sp", 0, 0, tiled=True).reshape(sp * rest, LANES)
     all_main = lax.all_gather(own_main, "sp", axis=0, tiled=True)
     all_keys = sp * (main + rest)
     terms = pl.pallas_call(

time: 112 us -> 110 us (0.982)
  Pallas kernels: 14.4 us -> 17.4 us
  local copies, waits for them, and re-layouts: 8.36 us -> 5.42 us
  waiting for transfers between devices: 21.6 us -> 19.4 us
    pallas_call x1, Pallas kernels: 3.03 us -> 6.54 us  [shards(): pl.pallas_call(project, out_shape=(shape((heads, length, LANES), half), s...]
    all_to_all x2, waiting for transfers between devices: 10.7 us -> 8.56 us  [the longest x1 8.56 us: shards(): modulation = lax.all_to_all(mod_pieces, ('sp', 'tp'), 0, 0, tiled=True)]
    unnamed x28, local copies, waits for them, and re-layouts: 7.03 us -> 5.42 us
    pallas_call x1, Pallas kernels: 9.29 us -> 7.69 us  [shards(): pl.pallas_call(attend, out_shape=shape((length, width), half), in_specs=i...]
    broadcast_in_dim x2 -> x0, local copies, waits for them, and re-layouts: 1.33 us -> none  [copy_for_each(): jnp.broadcast_to(shard[None], (devices, *shard.shape))]
  transfers between devices with their start and end apart: 3 -> 3, of which waited for: 2 -> 2; matrix products, arithmetic and copies ran while one was open for 1% -> 2% of each run, Pallas kernels for 1% -> 1%
where the time goes in v3:
time: 110 us
  blocking collectives  38.6 us (35%)
  starting transfers between devices  27 us (25%)
  waiting for transfers between devices  19.4 us (18%)
  Pallas kernels  17.4 us (16%)
  local copies, waits for them, and re-layouts  5.42 us (5%)
  other arithmetic  1.69 us (2%)
    all_gather x1, blocking collectives, shards(): all_main = lax.all_gather(own_main, 'sp', axis=0, tiled=True)  38.6 us
    all_to_all x1, starting transfers between devices, shards(): modulation = lax.all_to_all(mod_pieces, ('sp', 'tp'), 0, 0, tiled=True)  18.9 us
    all_to_all x1, waiting for transfers between devices, shards(): lax.all_to_all(terms.reshape(tp, kept, width), 'tp', 0, 0, tiled=True)  10.9 us
    all_to_all x1, waiting for transfers between devices, shards(): modulation = lax.all_to_all(mod_pieces, ('sp', 'tp'), 0, 0, tiled=True)  8.56 us
    pallas_call x1, Pallas kernels, shards(): pl.pallas_call(attend, out_shape=shape((length, width), half), in_specs=i...  7.69 us
    pallas_call x1, Pallas kernels, shards(): pl.pallas_call(project, out_shape=(shape((heads, length, LANES), half), s...  6.54 us
    unnamed x28, local copies, waits for them, and re-layouts  5.42 us
    all_to_all x1, starting transfers between devices, shards(): lax.all_to_all(terms.reshape(tp, kept, width), 'tp', 0, 0, tiled=True)  4.48 us
  transfers between devices with their start and end apart: 3, of which 2 were waited for; matrix products, arithmetic and copies ran while one was open for 2% of the time, Pallas kernels for 1%

profile of v3, /device:TPU:6, one launch (start us, length us, event | category | flops | bytes accessed | tf_op | source)
XLA Modules:
  0.0 109.8 jit_solution(15674823521269286206)
XLA Ops:
  0.0 1.0 copy-done.5
  1.0 0.7 copy-done.10
  1.7 1.1 modulate.1
  2.8 0.0 copy-start.3
  2.8 18.9 %all-to-all-start = ((f32[64,1,96]{2,1,0:T(1,128)}), f32[64,1,96]{2,1,0:T(1,128)S(1)}, u32[]{:S(2)}, u32[]{:S(2)}) async-start(f32[64,1,96]{2,1,0:T(1,128)} %modulate.1), calls=%async_computation | async-start | bytes 65536 | tf_op jit(solution)/shard_map/all_to_all | solution.py:290
  21.8 0.0 copy-start.7
  21.8 1.6 %negate_select_fusion = (f32[256,128]{1,0:T(8,128)}, f32[256,128]{1,0:T(8,128)}) fusion(s32[128]{0:T(128)S(1)} %get-tuple-element.27, s32[128]{0:T(128)S(1)} %get-tuple-element.30, s32[128]{0:T(128)S(1)} %get-tuple-element.28, s32[128]{0:T(128)S(1)} %get-tuple-element.31, s32[256]{0:T(256)S(1)} %get-tuple-element.22, s32[256]{0:T(256)S(1)} %get-tuple-element.23, ...), kind=kLoop, calls=%fused_computation | loop fusion | flops 524288 | bytes 270464 | tf_op jit(solution)/shard_map/jit(_where)/select_n | solution.py:27
  23.4 0.0 copy-done.4
  23.4 0.0 copy-done.3
  23.4 0.0 copy-done.7
  23.5 0.6 copy-done.12
  24.1 1.2 %copy-done = bf16[1,256,2048]{2,1,0:T(8,128)(2,1)S(1)} copy-done((bf16[1,256,2048]{2,1,0:T(8,128)(2,1)S(1)}, bf16[1,256,2048]{2,1,0:T(8,128)(2,1)}, u32[]{:S(2)}) %copy-start) | copy-done | bytes 1048600
  25.3 1.1 %prepare.1 = (f32[256,128]{1,0:T(8,128)S(1)}, bf16[32,128]{1,0:T(8,128)(2,1)S(1)}) custom-call(bf16[256,2048]{1,0:T(8,128)(2,1)S(1)} %bitcast.13, bf16[32,2048]{1,0:T(8,128)(2,1)S(1)} %bitcast.21, bf16[64,2048]{1,0:T(8,128)(2,1)S(1)} %bitcast.16, bf16[64,2048]{1,0:T(8,128)(2,1)S(1)} %bitcast.18, f32[1,64]{1,0:T(1,128)S(1)} %bitcast.23), custom_call_target="tpu_custom_call" | custom-call | tf_op jit(solution)/shard_map/prepare/pallas_call | solution.py:294
  26.4 0.0 copy-start.8
  26.4 0.6 copy-done.8
  27.1 0.6 copy-done.9
  27.7 8.6 %all-to-all-done.mod_ref = f32[64,1,96]{2,1,0:T(1,128)S(1)} async-done(((f32[64,1,96]{2,1,0:T(1,128)}), f32[64,1,96]{2,1,0:T(1,128)S(1)}, u32[]{:S(2)}, u32[]{:S(2)}) %all-to-all-start) | async-done | bytes 24608 | tf_op jit(solution)/shard_map/all_to_all | solution.py:290
  36.2 0.6 copy-done.13
  36.8 6.5 %project.1 = (bf16[4,256,128]{2,1,0:T(8,128)(2,1)}, bf16[248,128]{1,0:T(8,128)(2,1)}, bf16[16,40,128]{2,1,0:T(8,128)(2,1)}, f32[1,2048]{1,0:T(1,128)}) custom-call(bf16[256,2048]{1,0:T(8,128)(2,1)} %bitcast.12, bf16[2048,256]{1,0:T(8,128)(2,1)} %wq_hbm.1, bf16[64,2048]{1,0:T(8,128)(2,1)} %bitcast.15, bf16[64,2048]{1,0:T(8,128)(2,1)} %bitcast.17, ...), custom_call_target="tpu_custom_call" | custom-call | tf_op jit(solution)/shard_map/project/pallas_call | solution.py:307
  43.4 0.0 copy-start.2
  43.4 3.7 %all-to-all-start.1 = ((bf16[16,40,128]{2,1,0:T(8,128)(2,1)}), bf16[16,40,128]{2,1,0:T(8,128)(2,1)S(1)}, u32[]{:S(2)}, u32[]{:S(2)}) async-start(bf16[16,40,128]{2,1,0:T(8,128)(2,1)} %get-tuple-element.15), calls=%async_computation.1 | async-start | bytes 327680 | tf_op jit(solution)/shard_map/all_to_all | solution.py:344
  47.1 0.0 copy-start.6
  47.1 38.6 %all_gather.3.main_ref = bf16[3968,128]{1,0:T(8,128)(2,1)S(1)} all-gather(bf16[248,128]{1,0:T(8,128)(2,1)} %get-tuple-element.14), channel_id=1, replica_groups=mesh['sp'=16,'tp'=4,'dp'=8] {'sp'}, dimensions={0}, use_global_device_ids=true | all-gather | bytes 1079296 | tf_op jit(solution)/shard_map/all_gather | solution.py:345
  85.7 0.0 all-to-all-done.1
  85.7 0.0 copy-done.2
  85.7 0.0 copy-done.6
  85.7 7.7 %attend.1 = bf16[256,2048]{1,0:T(8,128)(2,1)} custom-call(bf16[4,256,128]{2,1,0:T(8,128)(2,1)S(1)} %copy-done.6, bf16[3968,128]{1,0:T(8,128)(2,1)S(1)} %all_gather.3.main_ref, bf16[640,128]{1,0:T(8,128)(2,1)S(1)} %bitcast.19, bf16[256,2048]{1,0:T(8,128)(2,1)S(1)} %copy-done.2), custom_call_target="tpu_custom_call" | custom-call | tf_op jit(solution)/shard_map/attend/pallas_call | solution.py:347
  93.4 0.0 copy-start.1
  93.4 4.5 %all-to-all-start.2 = ((bf16[4,64,2048]{2,1,0:T(8,128)(2,1)}), bf16[4,64,2048]{2,1,0:T(8,128)(2,1)S(1)}, u32[]{:S(2)}, u32[]{:S(2)}) async-start(bf16[4,64,2048]{2,1,0:T(8,128)(2,1)} %bitcast.10), calls=%async_computation.2 | async-start | bytes 2097152 | tf_op jit(solution)/shard_map/all_to_all | solution.py:361
  97.9 10.9 %all-to-all-done.2.terms_ref = bf16[4,64,2048]{2,1,0:T(8,128)(2,1)S(1)} async-done(((bf16[4,64,2048]{2,1,0:T(8,128)(2,1)}), bf16[4,64,2048]{2,1,0:T(8,128)(2,1)S(1)}, u32[]{:S(2)}, u32[]{:S(2)}) %all-to-all-start.2) | async-done | bytes 1048608 | tf_op jit(solution)/shard_map/all_to_all | solution.py:361
  108.8 0.0 copy-done.1
  108.8 1.0 finish.1
  (18 shorter events, 0.1 us)
Async XLA Ops:
  0.0 1.0 copy-start.5
  1.0 0.7 copy-start.10
  1.7 21.7 %copy-start.4 = (bf16[2048,64]{0,1:T(8,128)(2,1)S(1)}, bf16[2048,64]{0,1:T(8,128)(2,1)}, u32[]{:S(2)}) copy-start(bf16[2048,64]{0,1:T(8,128)(2,1)} %param.18) | copy-start | bytes 786436
  2.8 20.7 %copy-start.3 = (bf16[2048,64]{0,1:T(8,128)(2,1)S(1)}, bf16[2048,64]{0,1:T(8,128)(2,1)}, u32[]{:S(2)}) copy-start(bf16[2048,64]{0,1:T(8,128)(2,1)} %param.17) | copy-start | bytes 786436
  2.8 33.4 %all-to-all-start = ((f32[64,1,96]{2,1,0:T(1,128)}), f32[64,1,96]{2,1,0:T(1,128)S(1)}, u32[]{:S(2)}, u32[]{:S(2)}) async-start(f32[64,1,96]{2,1,0:T(1,128)} %modulate.1), calls=%async_computation | async-start | bytes 65536 | tf_op jit(solution)/shard_map/all_to_all | solution.py:290
  21.8 1.7 %copy-start.7 = (bf16[1,32,2048]{2,1,0:T(8,128)(2,1)S(1)}, bf16[1,32,2048]{2,1,0:T(8,128)(2,1)}, u32[]{:S(2)}) copy-start(bf16[1,32,2048]{2,1,0:T(8,128)(2,1)} %param.12) | copy-start | bytes 393220
  23.4 0.7 copy-start.12
  24.1 1.2 %copy-start = (bf16[1,256,2048]{2,1,0:T(8,128)(2,1)S(1)}, bf16[1,256,2048]{2,1,0:T(8,128)(2,1)}, u32[]{:S(2)}) copy-start(bf16[1,256,2048]{2,1,0:T(8,128)(2,1)} %param.11) | copy-start | bytes 3145732
  26.4 0.6 copy-start.8
  27.1 0.6 copy-start.9
  36.2 0.6 copy-start.13
  43.4 42.3 %copy-start.2 = (bf16[256,2048]{1,0:T(8,128)(2,1)S(1)}, bf16[256,2048]{1,0:T(8,128)(2,1)}, u32[]{:S(2)}) copy-start(bf16[256,2048]{1,0:T(8,128)(2,1)} %w_hbm.1) | copy-start | bytes 3145732
  43.4 42.3 %all-to-all-start.1 = ((bf16[16,40,128]{2,1,0:T(8,128)(2,1)}), bf16[16,40,128]{2,1,0:T(8,128)(2,1)S(1)}, u32[]{:S(2)}, u32[]{:S(2)}) async-start(bf16[16,40,128]{2,1,0:T(8,128)(2,1)} %get-tuple-element.15), calls=%async_computation.1 | async-start | bytes 327680 | tf_op jit(solution)/shard_map/all_to_all | solution.py:344
  47.1 38.6 %copy-start.6 = (bf16[4,256,128]{2,1,0:T(8,128)(2,1)S(1)}, bf16[4,256,128]{2,1,0:T(8,128)(2,1)}, u32[]{:S(2)}) copy-start(bf16[4,256,128]{2,1,0:T(8,128)(2,1)} %get-tuple-element.13.q_hbm) | copy-start | bytes 786436
  93.4 15.4 %copy-start.1 = (bf16[1,256,2048]{2,1,0:T(8,128)(2,1)S(1)}, bf16[1,256,2048]{2,1,0:T(8,128)(2,1)}, u32[]{:S(2)}) copy-start(bf16[1,256,2048]{2,1,0:T(8,128)(2,1)} %param.11) | copy-start | bytes 3145732
  93.4 15.4 %all-to-all-start.2 = ((bf16[4,64,2048]{2,1,0:T(8,128)(2,1)}), bf16[4,64,2048]{2,1,0:T(8,128)(2,1)S(1)}, u32[]{:S(2)}, u32[]{:S(2)}) async-start(bf16[4,64,2048]{2,1,0:T(8,128)(2,1)} %bitcast.10), calls=%async_computation.2 | async-start | bytes 2097152 | tf_op jit(solution)/shard_map/all_to_all | solution.py:361
  97.9 10.9 %copy-start.11 = (f32[1,2048]{1,0:T(1,128)S(1)}, f32[1,2048]{1,0:T(1,128)}, u32[]{:S(2)}) copy-start(f32[1,2048]{1,0:T(1,128)} %get-tuple-element.16.gate_ref) | copy-start | bytes 24580

commit v4 on v3

--- a/solution.py
+++ b/solution.py
@@ -4,6 +4,7 @@
 from jax.experimental import pallas as pl
 from jax.experimental.pallas import tpu as pltpu
 from jax.sharding import PartitionSpec as P
+
 
 GRID_W = 64
 LANES = 128
@@ -186,8 +187,8 @@
     last.wait()
 
 
-def attend(q_hbm, main_ref, rest_ref, w_hbm, o_ref, q_ref, s_ref, at_ref, w_ref, sems):
-    copies = start_all(((q_hbm, q_ref), (w_hbm, w_ref)), sems)
+def attend(q_hbm, main_ref, rest_ref, at_ref, q_ref, s_ref, sems):
+    copies = start_all(((q_hbm, q_ref),), sems)
     heads, rows, _ = q_ref.shape
     head_dim = at_ref.shape[1] // heads
     parts, at = [], 0
@@ -225,20 +226,27 @@
                 jnp.bfloat16
             )
         row_max = jnp.max(m, axis=1, keepdims=True)
-    copies[1].wait()
-    o_ref[...] = jnp.dot(at_ref[...], w_ref[...], preferred_element_type=jnp.float32).astype(
-        jnp.bfloat16
-    )
-
-
-def finish(at_ref, lat_hbm, terms_ref, gate_ref, out_ref, kept_ref, sems):
+
+
+def finish(at_ref, lat_hbm, *refs):
+    group = len(refs) - 6
+    weights_hbm, (att_ref, gate_ref, out_ref, kept_ref, w_ref, sems) = refs[:group], refs[group:]
     kept = kept_ref.shape[0]
-    at = pl.multiple_of(at_ref[0] * kept, kept)
-    (copy,) = start_all(((lat_hbm.at[pl.ds(at, kept)], kept_ref),), sems)
-    projected = terms_ref[0].astype(jnp.float32)
-    for g in range(1, terms_ref.shape[0]):
-        projected = projected + terms_ref[g].astype(jnp.float32)
-    copy.wait()
+    own = at_ref[0]
+    at = pl.multiple_of(own * kept, kept)
+    copies = start_all(
+        [(w, w_ref.at[k]) for k, w in enumerate(weights_hbm)]
+        + [(lat_hbm.at[pl.ds(at, kept)], kept_ref)],
+        sems,
+    )
+    projected = None
+    for k in range(group):
+        copies[k].wait()
+        heads = att_ref[(own + group - k) % group]
+        term = jnp.dot(heads, w_ref[k], preferred_element_type=jnp.float32)
+        term = term.astype(jnp.bfloat16).astype(jnp.float32)
+        projected = term if projected is None else projected + term
+    copies[group].wait()
     residual = kept_ref[...].astype(jnp.float32)
     out_ref[...] = (residual + gate_ref[...] * projected).astype(jnp.bfloat16)
 
@@ -255,7 +263,7 @@
     return [pl.BlockSpec(memory_space=pltpu.HBM)] * count
 
 
-def shards(
+def one_device(
     latent,
     context,
     condition,
@@ -288,6 +296,9 @@
         name="modulate",
     )(condition, mod_weight.T)
     modulation = lax.all_to_all(mod_pieces, ("sp", "tp"), 0, 0, tiled=True)
+    others = []
+    for k in range(1, tp):
+        others.append(lax.ppermute(w_out, "tp", [(i, (i + k) % tp) for i in range(tp)]))
     cosine, sine = rotary_tables(lax.axis_index("sp") * length, length, 0, head_dim)
 
     wk, wv = w_key.T, w_value.T
@@ -344,29 +355,39 @@
     all_rest = lax.all_to_all(own_rest, "sp", 0, 0, tiled=True).reshape(sp * rest, LANES)
     all_main = lax.all_gather(own_main, "sp", axis=0, tiled=True)
     all_keys = sp * (main + rest)
-    terms = pl.pallas_call(
+    attended = pl.pallas_call(
         attend,
-        out_shape=shape((length, width), half),
-        in_specs=in_hbm(1) + in_vmem(2) + in_hbm(1),
+        out_shape=shape((length, heads * head_dim), half),
+        in_specs=in_hbm(1) + in_vmem(2),
         scratch_shapes=[
             pltpu.VMEM((heads, length, LANES), half),
             pltpu.VMEM((2, length, all_keys), single),
-            pltpu.VMEM((length, heads * head_dim), half),
-            pltpu.VMEM(w_out.shape, half),
-            dma(2),
+            dma(1),
         ],
         compiler_params=vmem(32),
         name="attend",
-    )(queries, all_main, all_rest, w_out)
-    terms = lax.all_to_all(terms.reshape(tp, kept, width), "tp", 0, 0, tiled=True)
+    )(queries, all_main, all_rest)
+    attended = attended.reshape(tp, kept, heads * head_dim)
+    attended = lax.all_to_all(attended, "tp", 0, 0, tiled=True)
     mixed = pl.pallas_call(
         finish,
         out_shape=shape((kept, width), half),
-        in_specs=[pl.BlockSpec(memory_space=pltpu.SMEM)] + in_hbm(1) + in_vmem(2),
-        scratch_shapes=[pltpu.VMEM((kept, width), half), dma(1)],
-        compiler_params=vmem(8),
+        in_specs=[pl.BlockSpec(memory_space=pltpu.SMEM)] + in_hbm(1 + tp) + in_vmem(2),
+        scratch_shapes=[
+            pltpu.VMEM((kept, width), half),
+            pltpu.VMEM((tp, *w_out.shape), half),
+            dma(1 + tp),
+        ],
+        compiler_params=vmem(16),
         name="finish",
-    )(lax.axis_index("tp").astype(jnp.int32)[None], latent[0], terms, gate)
+    )(
+        lax.axis_index("tp").astype(jnp.int32)[None],
+        latent[0],
+        w_out,
+        *others,
+        attended,
+        gate,
+    )
     return mixed[None]
 
 
@@ -385,5 +406,5 @@
         P("tp", None),
     )
     return jax.shard_map(
-        shards, mesh=mesh, in_specs=placed, out_specs=P("dp", ("sp", "tp"), None), check_vma=False
-    )
+        one_device, mesh=mesh, in_specs=placed, out_specs=P("dp", ("sp", "tp"), None), check_vma=False
+    )

time: 110 us -> 135 us (1.23)
  starting transfers between devices: 27 us -> 48.2 us
    ppermute x0 -> x3, starting transfers between devices: none -> 12.2 us  [one_device(): lax.ppermute(w_out, 'tp', [(i, (i + k) % tp) for i in range(tp)])]
    all_to_all x3, starting transfers between devices: 27 us -> 36 us  [the longest x1 16.2 us: one_device(): modulation = lax.all_to_all(mod_pieces, ('sp', 'tp'), 0, 0, tiled=True)]
    unnamed x28 -> x30, local copies, waits for them, and re-layouts: 5.42 us -> 5.42 us
  transfers between devices with their start and end apart: 3 -> 6, of which waited for: 2 -> 2; matrix products, arithmetic and copies ran while one was open for 2% -> 1% of each run, Pallas kernels for 1% -> 12%
where the time goes in v4:
time: 135 us; the launch traced here: 134 us
  starting transfers between devices  48.2 us (36%)
  blocking collectives  39.3 us (29%)
  waiting for transfers between devices  20.6 us (15%)
  Pallas kernels  18.6 us (14%)
  local copies, waits for them, and re-layouts  5.42 us (4%)
  other arithmetic  1.7 us (1%)
    all_gather x1, blocking collectives, one_device(): all_main = lax.all_gather(own_main, 'sp', axis=0, tiled=True)  39.3 us
    all_to_all x1, starting transfers between devices, one_device(): modulation = lax.all_to_all(mod_pieces, ('sp', 'tp'), 0, 0, tiled=True)  16.2 us
    all_to_all x1, starting transfers between devices, one_device(): lax.all_to_all(own_rest, 'sp', 0, 0, tiled=True).reshape(sp * rest, LANES)  15.3 us
    all_to_all x1, waiting for transfers between devices, one_device(): modulation = lax.all_to_all(mod_pieces, ('sp', 'tp'), 0, 0, tiled=True)  14.6 us
    ppermute x3, starting transfers between devices, one_device(): lax.ppermute(w_out, 'tp', [(i, (i + k) % tp) for i in range(tp)])  12.2 us
    pallas_call x1, Pallas kernels, one_device(): pl.pallas_call(attend, out_shape=shape((length, heads * head_dim), half),...  6.86 us
    pallas_call x1, Pallas kernels, one_device(): pl.pallas_call(project, out_shape=(shape((heads, length, LANES), half), s...  6.54 us
    all_to_all x1, waiting for transfers between devices, one_device(): attended = lax.all_to_all(attended, 'tp', 0, 0, tiled=True)  5.97 us
  transfers between devices with their start and end apart: 6, of which 2 were waited for; matrix products, arithmetic and copies ran while one was open for 1% of the time, Pallas kernels for 12%

profile of v4, /device:TPU:6, one launch (start us, length us, event | category | flops | bytes accessed | tf_op | source)
XLA Modules:
  0.0 134.0 jit_solution(10624030063881295039)
XLA Ops:
  0.0 5.1 %collective-permute-start.1 = (bf16[256,2048]{1,0:T(8,128)(2,1)}, bf16[256,2048]{1,0:T(8,128)(2,1)}, u32[]{:S(2)}, u32[]{:S(2)}) collective-permute-start(bf16[256,2048]{1,0:T(8,128)(2,1)} %refs_0_.1), channel_id=1, source_target_pairs={{0,16},{8,24},{16,0},{24,8},{1,17},{9,25},{17,1},{25,9},{2,18},{10... | collective-permute-start | bytes 3145736 | tf_op jit(solution)/shard_map/ppermute | solution.py:301
  5.1 2.6 %collective-permute-start = (bf16[256,2048]{1,0:T(8,128)(2,1)}, bf16[256,2048]{1,0:T(8,128)(2,1)}, u32[]{:S(2)}, u32[]{:S(2)}) collective-permute-start(bf16[256,2048]{1,0:T(8,128)(2,1)} %refs_0_.1), channel_id=1, source_target_pairs={{0,8},{8,16},{16,24},{24,0},{1,9},{9,17},{17,25},{25,1},{2,10},{10... | collective-permute-start | bytes 3145736 | tf_op jit(solution)/shard_map/ppermute | solution.py:301
  7.7 4.5 %collective-permute-start.2 = (bf16[256,2048]{1,0:T(8,128)(2,1)}, bf16[256,2048]{1,0:T(8,128)(2,1)}, u32[]{:S(2)}, u32[]{:S(2)}) collective-permute-start(bf16[256,2048]{1,0:T(8,128)(2,1)} %refs_0_.1), channel_id=1, source_target_pairs={{0,24},{8,0},{16,8},{24,16},{1,25},{9,1},{17,9},{25,17},{2,26},{10... | collective-permute-start | bytes 3145736 | tf_op jit(solution)/shard_map/ppermute | solution.py:301
  12.2 0.0 copy-start.5
  12.2 1.0 copy-done.5
  13.2 0.7 copy-done.11
  13.9 1.1 modulate.1
  14.9 0.0 copy-start.3
  15.0 16.2 %all-to-all-start = ((f32[64,1,96]{2,1,0:T(1,128)}), f32[64,1,96]{2,1,0:T(1,128)S(1)}, u32[]{:S(2)}, u32[]{:S(2)}) async-start(f32[64,1,96]{2,1,0:T(1,128)} %modulate.1), calls=%async_computation | async-start | bytes 65536 | tf_op jit(solution)/shard_map/all_to_all | solution.py:298
  31.3 0.0 copy-start.7
  31.3 1.6 %negate_select_fusion = (f32[256,128]{1,0:T(8,128)}, f32[256,128]{1,0:T(8,128)}) fusion(s32[128]{0:T(128)S(1)} %get-tuple-element.27, s32[128]{0:T(128)S(1)} %get-tuple-element.30, s32[128]{0:T(128)S(1)} %get-tuple-element.28, s32[128]{0:T(128)S(1)} %get-tuple-element.31, s32[256]{0:T(256)S(1)} %get-tuple-element.22, s32[256]{0:T(256)S(1)} %get-tuple-element.23, ...), kind=kLoop, calls=%fused_computation | loop fusion | flops 524288 | bytes 270464 | tf_op jit(solution)/shard_map/jit(_where)/select_n | solution.py:28
  33.0 0.0 copy-done.3
  33.0 0.6 copy-done.12
  33.6 1.2 copy-done
  34.9 1.1 prepare.1
  36.0 0.6 copy-done.8
  36.6 0.6 copy-done.10
  37.2 14.6 %all-to-all-done.mod_ref = f32[64,1,96]{2,1,0:T(1,128)S(1)} async-done(((f32[64,1,96]{2,1,0:T(1,128)}), f32[64,1,96]{2,1,0:T(1,128)S(1)}, u32[]{:S(2)}, u32[]{:S(2)}) %all-to-all-start) | async-done | bytes 24608 | tf_op jit(solution)/shard_map/all_to_all | solution.py:298
  51.8 0.6 copy-done.13
  52.4 6.5 %project.1 = (bf16[4,256,128]{2,1,0:T(8,128)(2,1)}, bf16[248,128]{1,0:T(8,128)(2,1)}, bf16[16,40,128]{2,1,0:T(8,128)(2,1)}, f32[1,2048]{1,0:T(1,128)}) custom-call(bf16[256,2048]{1,0:T(8,128)(2,1)} %bitcast.12, bf16[2048,256]{1,0:T(8,128)(2,1)} %wq_hbm.1, bf16[64,2048]{1,0:T(8,128)(2,1)} %bitcast.15, bf16[64,2048]{1,0:T(8,128)(2,1)} %bitcast.17, ...), custom_call_target="tpu_custom_call" | custom-call | tf_op jit(solution)/shard_map/project/pallas_call | solution.py:318
  59.0 0.0 copy-start.6
  59.0 15.3 %all-to-all-start.1 = ((bf16[16,40,128]{2,1,0:T(8,128)(2,1)}), bf16[16,40,128]{2,1,0:T(8,128)(2,1)S(1)}, u32[]{:S(2)}, u32[]{:S(2)}) async-start(bf16[16,40,128]{2,1,0:T(8,128)(2,1)} %get-tuple-element.15), calls=%async_computation.1 | async-start | bytes 327680 | tf_op jit(solution)/shard_map/all_to_all | solution.py:355
  74.3 0.0 copy-start.2
  74.3 39.3 %all_gather.3.main_ref = bf16[3968,128]{1,0:T(8,128)(2,1)S(1)} all-gather(bf16[248,128]{1,0:T(8,128)(2,1)S(1)} %copy-done.14), channel_id=1, replica_groups=mesh['sp'=16,'tp'=4,'dp'=8] {'sp'}, dimensions={0}, use_global_device_ids=true | all-gather | bytes 1079296 | tf_op jit(solution)/shard_map/all_gather | solution.py:356
  113.6 0.0 all-to-all-done.1
  113.7 6.9 %attend.1 = bf16[256,256]{1,0:T(8,128)(2,1)} custom-call(bf16[4,256,128]{2,1,0:T(8,128)(2,1)S(1)} %copy-done.6, bf16[3968,128]{1,0:T(8,128)(2,1)S(1)} %all_gather.3.main_ref, bf16[640,128]{1,0:T(8,128)(2,1)S(1)} %bitcast.19), custom_call_target="tpu_custom_call" | custom-call | tf_op jit(solution)/shard_map/attend/pallas_call | solution.py:358
  120.5 4.4 %all-to-all-start.2 = ((bf16[4,64,256]{2,1,0:T(8,128)(2,1)}), bf16[4,64,256]{2,1,0:T(8,128)(2,1)S(1)}, u32[]{:S(2)}, u32[]{:S(2)}) async-start(bf16[4,64,256]{2,1,0:T(8,128)(2,1)} %bitcast.10), calls=%async_computation.2 | async-start | bytes 262144 | tf_op jit(solution)/shard_map/all_to_all | solution.py:371
  124.9 6.0 %all-to-all-done.2.refs_4_ = bf16[4,64,256]{2,1,0:T(8,128)(2,1)S(1)} async-done(((bf16[4,64,256]{2,1,0:T(8,128)(2,1)}), bf16[4,64,256]{2,1,0:T(8,128)(2,1)S(1)}, u32[]{:S(2)}, u32[]{:S(2)}) %all-to-all-start.2) | async-done | bytes 131104 | tf_op jit(solution)/shard_map/all_to_all | solution.py:371
  130.9 0.0 collective-permute-done.1.refs_2_
  130.9 0.0 collective-permute-done.refs_1_
  130.9 0.0 collective-permute-done.2.refs_3_
  131.0 3.0 %finish.1 = bf16[64,2048]{1,0:T(8,128)(2,1)} custom-call(s32[1]{0:T(128)} %bitcast.at_ref, bf16[256,2048]{1,0:T(8,128)(2,1)S(1)} %bitcast.14, bf16[256,2048]{1,0:T(8,128)(2,1)S(1)} %copy-done.2, bf16[256,2048]{1,0:T(8,128)(2,1)} %collective-permute-done.refs_1_, bf16[256,2048]{1,0:T(8,128)(2,1)} %collective-permute-done.1.refs_2_, ...), custom_call_target="tpu_custom_call" | custom-call | tf_op jit(solution)/shard_map/finish/pallas_call | solution.py:372
  (26 shorter events, 0.1 us)
Async XLA Ops:
  0.0 130.9 %collective-permute-start.1 = (bf16[256,2048]{1,0:T(8,128)(2,1)}, bf16[256,2048]{1,0:T(8,128)(2,1)}, u32[]{:S(2)}, u32[]{:S(2)}) collective-permute-start(bf16[256,2048]{1,0:T(8,128)(2,1)} %refs_0_.1), channel_id=1, source_target_pairs={{0,16},{8,24},{16,0},{24,8},{1,17},{9,25},{17,1},{25,9},{2,18},{10... | collective-permute-start | bytes 3145736 | tf_op jit(solution)/shard_map/ppermute | solution.py:301
  5.1 125.8 %collective-permute-start = (bf16[256,2048]{1,0:T(8,128)(2,1)}, bf16[256,2048]{1,0:T(8,128)(2,1)}, u32[]{:S(2)}, u32[]{:S(2)}) collective-permute-start(bf16[256,2048]{1,0:T(8,128)(2,1)} %refs_0_.1), channel_id=1, source_target_pairs={{0,8},{8,16},{16,24},{24,0},{1,9},{9,17},{17,25},{25,1},{2,10},{10... | collective-permute-start | bytes 3145736 | tf_op jit(solution)/shard_map/ppermute | solution.py:301
  7.7 123.2 %collective-permute-start.2 = (bf16[256,2048]{1,0:T(8,128)(2,1)}, bf16[256,2048]{1,0:T(8,128)(2,1)}, u32[]{:S(2)}, u32[]{:S(2)}) collective-permute-start(bf16[256,2048]{1,0:T(8,128)(2,1)} %refs_0_.1), channel_id=1, source_target_pairs={{0,24},{8,0},{16,8},{24,16},{1,25},{9,1},{17,9},{25,17},{2,26},{10... | collective-permute-start | bytes 3145736 | tf_op jit(solution)/shard_map/ppermute | solution.py:301
  12.2 1.0 copy-start.5
  13.2 0.7 copy-start.11
  13.9 19.1 %copy-start.4 = (bf16[2048,64]{0,1:T(8,128)(2,1)S(1)}, bf16[2048,64]{0,1:T(8,128)(2,1)}, u32[]{:S(2)}) copy-start(bf16[2048,64]{0,1:T(8,128)(2,1)} %param.18) | copy-start | bytes 786436
  14.9 18.0 %copy-start.3 = (bf16[2048,64]{0,1:T(8,128)(2,1)S(1)}, bf16[2048,64]{0,1:T(8,128)(2,1)}, u32[]{:S(2)}) copy-start(bf16[2048,64]{0,1:T(8,128)(2,1)} %param.17) | copy-start | bytes 786436
  15.0 36.8 %all-to-all-start = ((f32[64,1,96]{2,1,0:T(1,128)}), f32[64,1,96]{2,1,0:T(1,128)S(1)}, u32[]{:S(2)}, u32[]{:S(2)}) async-start(f32[64,1,96]{2,1,0:T(1,128)} %modulate.1), calls=%async_computation | async-start | bytes 65536 | tf_op jit(solution)/shard_map/all_to_all | solution.py:298
  31.3 1.7 %copy-start.7 = (bf16[1,32,2048]{2,1,0:T(8,128)(2,1)S(1)}, bf16[1,32,2048]{2,1,0:T(8,128)(2,1)}, u32[]{:S(2)}) copy-start(bf16[1,32,2048]{2,1,0:T(8,128)(2,1)} %param.12) | copy-start | bytes 393220
  33.0 0.7 copy-start.12
  33.6 1.2 copy-start
  36.0 0.7 copy-start.8
  36.6 0.6 copy-start.10
  51.8 0.6 copy-start.13
  58.9 15.4 %copy-start.14 = (bf16[248,128]{1,0:T(8,128)(2,1)S(1)}, bf16[248,128]{1,0:T(8,128)(2,1)}, u32[]{:S(2)}) copy-start(bf16[248,128]{1,0:T(8,128)(2,1)} %get-tuple-element.14) | copy-start | bytes 190468
  59.0 54.7 %copy-start.6 = (bf16[4,256,128]{2,1,0:T(8,128)(2,1)S(1)}, bf16[4,256,128]{2,1,0:T(8,128)(2,1)}, u32[]{:S(2)}) copy-start(bf16[4,256,128]{2,1,0:T(8,128)(2,1)} %get-tuple-element.13.q_hbm) | copy-start | bytes 786436
  59.0 54.7 %all-to-all-start.1 = ((bf16[16,40,128]{2,1,0:T(8,128)(2,1)}), bf16[16,40,128]{2,1,0:T(8,128)(2,1)S(1)}, u32[]{:S(2)}, u32[]{:S(2)}) async-start(bf16[16,40,128]{2,1,0:T(8,128)(2,1)} %get-tuple-element.15), calls=%async_computation.1 | async-start | bytes 327680 | tf_op jit(solution)/shard_map/all_to_all | solution.py:355
  74.3 56.6 %copy-start.2 = (bf16[256,2048]{1,0:T(8,128)(2,1)S(1)}, bf16[256,2048]{1,0:T(8,128)(2,1)}, u32[]{:S(2)}) copy-start(bf16[256,2048]{1,0:T(8,128)(2,1)} %refs_0_.1) | copy-start | bytes 3145732
  113.6 17.3 %copy-start.1 = (bf16[1,256,2048]{2,1,0:T(8,128)(2,1)S(1)}, bf16[1,256,2048]{2,1,0:T(8,128)(2,1)}, u32[]{:S(2)}) copy-start(bf16[1,256,2048]{2,1,0:T(8,128)(2,1)} %param.11) | copy-start | bytes 3145732
  120.5 10.4 %all-to-all-start.2 = ((bf16[4,64,256]{2,1,0:T(8,128)(2,1)}), bf16[4,64,256]{2,1,0:T(8,128)(2,1)S(1)}, u32[]{:S(2)}, u32[]{:S(2)}) async-start(bf16[4,64,256]{2,1,0:T(8,128)(2,1)} %bitcast.10), calls=%async_computation.2 | async-start | bytes 262144 | tf_op jit(solution)/shard_map/all_to_all | solution.py:371
  124.9 6.0 %copy-start.9 = (f32[1,2048]{1,0:T(1,128)S(1)}, f32[1,2048]{1,0:T(1,128)}, u32[]{:S(2)}) copy-start(f32[1,2048]{1,0:T(1,128)} %get-tuple-element.16.refs_5_) | copy-start | bytes 24580

commit v5 on v3

--- a/solution.py
+++ b/solution.py
@@ -73,27 +73,17 @@
 
 
 def prepare(
-    lat_hbm, ctx_hbm, wk_hbm, wv_hbm, kg_ref, inv_ref, ctx_kv_ref, lat_ref, ctx_ref, wkv_ref, sems
+    lat_ref, ctx_ref, wk_ref, wv_ref, kg_ref, inv_ref, ctx_kv_ref, wkv_ref
 ):
     rows = lat_ref.shape[0]
     head_dim = kg_ref.shape[1]
-    copies = start_all(
-        (
-            (lat_hbm, lat_ref),
-            (ctx_hbm, ctx_ref),
-            (wk_hbm, wkv_ref.at[pl.ds(0, head_dim)]),
-            (wv_hbm, wkv_ref.at[pl.ds(head_dim, head_dim)]),
-        ),
-        sems,
-    )
-    copies[0].wait()
     step = 32
     for r in range(0, rows, step):
         x = lat_ref[r : r + step, :].astype(jnp.float32)
         mean_sq = jnp.mean(x * x, axis=-1, keepdims=True)
         inv_ref[r : r + step, :] = jnp.broadcast_to(lax.rsqrt(mean_sq + epsilon), (step, LANES))
-    for copy in copies[1:]:
-        copy.wait()
+    wkv_ref[0:head_dim, :] = wk_ref[...]
+    wkv_ref[head_dim:, :] = wv_ref[...]
     scaled, _, low = turner(head_dim)
     both = contract_last(ctx_ref[...], wkv_ref[...])
     kg = jnp.concatenate([kg_ref[...]] * 2, axis=1)
@@ -101,10 +91,9 @@
 
 
 def project(
-    lat_hbm,
+    lat_ref,
     wq_hbm,
-    wk_hbm,
-    wv_hbm,
+    wkv_ref,
     inv_ref,
     ctx_kv_ref,
     mod_ref,
@@ -117,29 +106,20 @@
     main_hbm,
     rest_hbm,
     gate_ref,
-    lat_ref,
-    wq_ref,
-    wkv_ref,
     hid_ref,
     mods_ref,
     q_ref,
     kv_ref,
-    sems,
+    wq_ref,
+    wq_sems,
+    q_sems,
     out_sems,
 ):
+    (weights_in,) = start_all(((wq_hbm, wq_ref),), wq_sems)
     rows, width = lat_ref.shape
     main = main_hbm.shape[0]
     rest = rest_hbm.shape[1]
     head_dim = qg_ref.shape[1]
-    copies = start_all(
-        (
-            (lat_hbm, lat_ref),
-            (wk_hbm, wkv_ref.at[pl.ds(0, head_dim)]),
-            (wv_hbm, wkv_ref.at[pl.ds(head_dim, head_dim)]),
-            (wq_hbm, wq_ref),
-        ),
-        sems,
-    )
     pieces, _, piece = mod_ref.shape
     for j in range(pieces):
         mods_ref[0:1, piece * j : piece * (j + 1)] = mod_ref[j]
@@ -148,7 +128,6 @@
     gate_ref[...] = mods_ref[0:1, 2 * width : 3 * width]
     gain = gain_ref[...]
     step = 32
-    copies[0].wait()
     for r in range(0, rows, step):
         x = lat_ref[r : r + step, :].astype(jnp.float32)
         hidden = x * inv_ref[r : r + step, 0:1] * gain * scale + shift
@@ -159,8 +138,6 @@
     kg = jnp.concatenate([kg_ref[...]] * 2, axis=1)
     cosine, sine = cos_ref[...], sin_ref[...]
     hid = hid_ref[...]
-    copies[1].wait()
-    copies[2].wait()
     both = contract_last(hid, wkv_ref[...])
     both = jnp.where(low, turned(scaled(both, kg), cosine, sine), both).astype(jnp.bfloat16)
     kv_ref[0:rows, :] = both
@@ -171,7 +148,7 @@
         + [(sent, rest_hbm.at[z]) for z in range(rest_hbm.shape[0])],
         out_sems,
     )
-    copies[3].wait()
+    weights_in.wait()
     queries = jnp.dot(hid, wq_ref[...], preferred_element_type=jnp.float32)
     for g in range(queries.shape[1] // LANES):
         pair = turned(scaled(queries[:, LANES * g : LANES * (g + 1)], qg), cosine, sine)
@@ -179,11 +156,10 @@
         other = pltpu.roll(pair, head_dim, 1)
         q_ref[2 * g] = jnp.where(low, pair, 0.0).astype(jnp.bfloat16)
         q_ref[2 * g + 1] = jnp.where(low, other, 0.0).astype(jnp.bfloat16)
-    last = pltpu.make_async_copy(q_ref, q_hbm, sems.at[4])
-    last.start()
+        pair_of = pl.ds(2 * g, 2)
+        outs += start_all(((q_ref.at[pair_of], q_hbm.at[pair_of]),), q_sems.at[pl.ds(g, 1)])
     for copy in outs:
         copy.wait()
-    last.wait()
 
 
 def attend(q_hbm, main_ref, rest_ref, w_hbm, o_ref, q_ref, s_ref, at_ref, w_ref, sems):
@@ -284,24 +260,22 @@
         out_shape=shape((sp * tp, 1, mod_weight.shape[1]), single),
         in_specs=in_vmem(1) + in_hbm(1),
         scratch_shapes=[pltpu.VMEM(mod_weight.shape[::-1], half), dma(1)],
-        compiler_params=vmem(8),
+        compiler_params=vmem(60),
         name="modulate",
     )(condition, mod_weight.T)
     modulation = lax.all_to_all(mod_pieces, ("sp", "tp"), 0, 0, tiled=True)
     cosine, sine = rotary_tables(lax.axis_index("sp") * length, length, 0, head_dim)
 
     wk, wv = w_key.T, w_value.T
-    inverse, ctx_kv = pl.pallas_call(
+    inverse, ctx_kv, wkv = pl.pallas_call(
         prepare,
-        out_shape=(shape((length, LANES), single), shape((count, LANES), half)),
-        in_specs=in_hbm(4) + in_vmem(1),
-        scratch_shapes=[
-            pltpu.VMEM((length, width), half),
-            pltpu.VMEM((count, width), half),
-            pltpu.VMEM((2 * head_dim, width), half),
-            dma(4),
-        ],
-        compiler_params=vmem(12),
+        out_shape=(
+            shape((length, LANES), single),
+            shape((count, LANES), half),
+            shape((2 * head_dim, width), half),
+        ),
+        in_specs=in_vmem(5),
+        compiler_params=vmem(8),
         name="prepare",
     )(latent[0], context[0], wk, wv, k_gain[None])
     queries, own_main, own_rest, gate = pl.pallas_call(
@@ -312,26 +286,24 @@
             shape((sp, rest, LANES), half),
             shape((1, width), single),
         ),
-        in_specs=in_hbm(4) + in_vmem(8),
+        in_specs=in_vmem(1) + in_hbm(1) + in_vmem(9),
         out_specs=tuple(in_hbm(3) + in_vmem(1)),
         scratch_shapes=[
-            pltpu.VMEM((length, width), half),
-            pltpu.VMEM(w_query.shape, half),
-            pltpu.VMEM((2 * head_dim, width), half),
             pltpu.VMEM((length, width), half),
             pltpu.VMEM((8, 3 * width), single),
             pltpu.VMEM((heads, length, LANES), half),
             pltpu.VMEM((main + rest, LANES), half),
-            dma(5),
+            pltpu.VMEM(w_query.shape, half),
+            dma(1),
+            dma(heads // 2),
             dma(1 + sp),
         ],
-        compiler_params=vmem(60),
+        compiler_params=vmem(16),
         name="project",
     )(
         latent[0],
         w_query,
-        wk,
-        wv,
+        wkv,
         inverse,
         ctx_kv,
         modulation,

time: 110 us -> 107 us (0.973)
  waiting for transfers between devices: 19.4 us -> 22.1 us
  Pallas kernels: 17.4 us -> 15.3 us
    pallas_call x1, Pallas kernels: 6.54 us -> 3.43 us  [shards(): pl.pallas_call(project, out_shape=(shape((heads, length, LANES), half), s...]
    all_to_all x1, waiting for transfers between devices: 8.56 us -> 11.2 us  [shards(): modulation = lax.all_to_all(mod_pieces, ('sp', 'tp'), 0, 0, tiled=True)]
    pallas_call x1, Pallas kernels: 1.07 us -> 2.59 us  [shards(): pl.pallas_call(modulate, out_shape=shape((sp * tp, 1, mod_weight.shape[1]...]
    unnamed x28 -> x22, local copies, waits for them, and re-layouts: 5.42 us -> 4.39 us
  transfers between devices with their start and end apart: 3 -> 3, of which waited for: 2 -> 2; matrix products, arithmetic and copies ran while one was open for 2% -> 1% of each run, Pallas kernels for 1% -> 1%
where the time goes in v5:
time: 107 us
  blocking collectives  38.2 us (36%)
  starting transfers between devices  26.1 us (24%)
  waiting for transfers between devices  22.1 us (21%)
  Pallas kernels  15.3 us (14%)
  local copies, waits for them, and re-layouts  4.39 us (4%)
    all_gather x1, blocking collectives, shards(): all_main = lax.all_gather(own_main, 'sp', axis=0, tiled=True)  38.2 us
    all_to_all x1, starting transfers between devices, shards(): modulation = lax.all_to_all(mod_pieces, ('sp', 'tp'), 0, 0, tiled=True)  18.9 us
    all_to_all x1, waiting for transfers between devices, shards(): modulation = lax.all_to_all(mod_pieces, ('sp', 'tp'), 0, 0, tiled=True)  11.2 us
    all_to_all x1, waiting for transfers between devices, shards(): lax.all_to_all(terms.reshape(tp, kept, width), 'tp', 0, 0, tiled=True)  10.9 us
    pallas_call x1, Pallas kernels, shards(): pl.pallas_call(attend, out_shape=shape((length, width), half), in_specs=i...  7.72 us
    unnamed x22, local copies, waits for them, and re-layouts  4.39 us
    all_to_all x1, starting transfers between devices, shards(): lax.all_to_all(own_rest, 'sp', 0, 0, tiled=True).reshape(sp * rest, LANES)  3.65 us
    all_to_all x1, starting transfers between devices, shards(): lax.all_to_all(terms.reshape(tp, kept, width), 'tp', 0, 0, tiled=True)  3.53 us
  transfers between devices with their start and end apart: 3, of which 2 were waited for; matrix products, arithmetic and copies ran while one was open for 1% of the time, Pallas kernels for 1%

profile of v5, /device:TPU:6, one launch (start us, length us, event | category | flops | bytes accessed | tf_op | source)
XLA Modules:
  0.0 107.0 jit_solution(16301448087690445869)
XLA Ops:
  0.0 0.0 copy-start.5
  0.0 2.6 %modulate.1 = f32[64,1,96]{2,1,0:T(1,128)} custom-call(bf16[1,2048]{1,0:T(2,128)(2,1)} %cond_ref.1, bf16[96,2048]{1,0:T(8,128)(2,1)} %bitcast.23), custom_call_target="tpu_custom_call" | custom-call | tf_op jit(solution)/shard_map/modulate/pallas_call | solution.py:258
  2.6 0.0 copy-start.4
  2.6 18.9 %all-to-all-start = ((f32[64,1,96]{2,1,0:T(1,128)}), f32[64,1,96]{2,1,0:T(1,128)S(1)}, u32[]{:S(2)}, u32[]{:S(2)}) async-start(f32[64,1,96]{2,1,0:T(1,128)} %modulate.1), calls=%async_computation | async-start | bytes 65536 | tf_op jit(solution)/shard_map/all_to_all | solution.py:266
  21.6 0.0 copy-start.6
  21.6 0.7 negate_select_fusion
  22.3 0.0 copy-start.9
  22.3 0.0 copy-done.5
  22.3 0.0 copy-done.4
  22.3 0.2 copy-done.6
  22.5 0.5 copy-done.9
  23.0 0.0 copy-start
  23.0 1.2 %copy-done = bf16[1,256,2048]{2,1,0:T(8,128)(2,1)S(1)} copy-done((bf16[1,256,2048]{2,1,0:T(8,128)(2,1)S(1)}, bf16[1,256,2048]{2,1,0:T(8,128)(2,1)}, u32[]{:S(2)}) %copy-start) | copy-done | bytes 1048600
  24.2 0.0 copy-start.1
  24.2 0.6 prepare.1
  24.8 0.0 copy-start.8
  24.8 11.2 %all-to-all-done.mod_ref = f32[64,1,96]{2,1,0:T(1,128)S(1)} async-done(((f32[64,1,96]{2,1,0:T(1,128)}), f32[64,1,96]{2,1,0:T(1,128)S(1)}, u32[]{:S(2)}, u32[]{:S(2)}) %all-to-all-start) | async-done | bytes 24608 | tf_op jit(solution)/shard_map/all_to_all | solution.py:266
  36.1 0.0 copy-done.1
  36.1 0.0 copy-done.8
  36.1 0.6 copy-done.10
  36.7 1.2 %copy-done.3 = bf16[2048,256]{1,0:T(8,128)(2,1)S(1)} copy-done((bf16[2048,256]{1,0:T(8,128)(2,1)S(1)}, bf16[2048,256]{1,0:T(8,128)(2,1)}, u32[]{:S(2)}) %copy-start.3) | copy-done | bytes 1048600
  37.9 3.4 %project.1 = (bf16[4,256,128]{2,1,0:T(8,128)(2,1)S(1)}, bf16[248,128]{1,0:T(8,128)(2,1)S(1)}, bf16[16,40,128]{2,1,0:T(8,128)(2,1)}, f32[1,2048]{1,0:T(1,128)S(1)}) custom-call(bf16[256,2048]{1,0:T(8,128)(2,1)S(1)} %bitcast.13, bf16[2048,256]{1,0:T(8,128)(2,1)S(1)} %copy-done.3, bf16[128,2048]{1,0:T(8,128)(2,1)S(1)} %get-tuple-element.12.wkv_ref, ...), custom_call_target="tpu_custom_call" | custom-call | tf_op jit(solution)/shard_map/project/pallas_call | solution.py:281
  41.4 0.0 copy-start.7
  41.4 0.6 copy-done.7
  42.0 3.6 %all-to-all-start.1 = ((bf16[16,40,128]{2,1,0:T(8,128)(2,1)}), bf16[16,40,128]{2,1,0:T(8,128)(2,1)S(1)}, u32[]{:S(2)}, u32[]{:S(2)}) async-start(bf16[16,40,128]{2,1,0:T(8,128)(2,1)} %get-tuple-element.17), calls=%async_computation.1 | async-start | bytes 327680 | tf_op jit(solution)/shard_map/all_to_all | solution.py:316
  45.7 38.2 %all_gather.3.main_ref = bf16[3968,128]{1,0:T(8,128)(2,1)S(1)} all-gather(bf16[248,128]{1,0:T(8,128)(2,1)} %copy-done.7), channel_id=1, replica_groups=mesh['sp'=16,'tp'=4,'dp'=8] {'sp'}, dimensions={0}, use_global_device_ids=true | all-gather | bytes 1079296 | tf_op jit(solution)/shard_map/all_gather | solution.py:317
  83.9 0.0 all-to-all-done.1
  83.9 0.0 copy-done.2
  83.9 7.7 %attend.1 = bf16[256,2048]{1,0:T(8,128)(2,1)} custom-call(bf16[4,256,128]{2,1,0:T(8,128)(2,1)S(1)} %get-tuple-element.15.q_hbm, bf16[3968,128]{1,0:T(8,128)(2,1)S(1)} %all_gather.3.main_ref, bf16[640,128]{1,0:T(8,128)(2,1)S(1)} %bitcast.15, bf16[256,2048]{1,0:T(8,128)(2,1)S(1)} %copy-done.2), custom_call_target="tpu_custom_call" | custom-call | tf_op jit(solution)/shard_map/attend/pallas_call | solution.py:319
  91.6 3.5 %all-to-all-start.2 = ((bf16[4,64,2048]{2,1,0:T(8,128)(2,1)}), bf16[4,64,2048]{2,1,0:T(8,128)(2,1)S(1)}, u32[]{:S(2)}, u32[]{:S(2)}) async-start(bf16[4,64,2048]{2,1,0:T(8,128)(2,1)} %bitcast.10), calls=%async_computation.2 | async-start | bytes 2097152 | tf_op jit(solution)/shard_map/all_to_all | solution.py:333
  95.2 10.9 %all-to-all-done.2.terms_ref = bf16[4,64,2048]{2,1,0:T(8,128)(2,1)S(1)} async-done(((bf16[4,64,2048]{2,1,0:T(8,128)(2,1)}), bf16[4,64,2048]{2,1,0:T(8,128)(2,1)S(1)}, u32[]{:S(2)}, u32[]{:S(2)}) %all-to-all-start.2) | async-done | bytes 1048608 | tf_op jit(solution)/shard_map/all_to_all | solution.py:333
  106.0 1.0 finish.1
  (12 shorter events, 0.1 us)
Async XLA Ops:
  0.0 22.3 %copy-start.5 = (bf16[2048,64]{0,1:T(8,128)(2,1)S(1)}, bf16[2048,64]{0,1:T(8,128)(2,1)}, u32[]{:S(2)}) copy-start(bf16[2048,64]{0,1:T(8,128)(2,1)} %param.18) | copy-start | bytes 786436
  2.6 19.7 %copy-start.4 = (bf16[2048,64]{0,1:T(8,128)(2,1)S(1)}, bf16[2048,64]{0,1:T(8,128)(2,1)}, u32[]{:S(2)}) copy-start(bf16[2048,64]{0,1:T(8,128)(2,1)} %param.17) | copy-start | bytes 786436
  2.6 33.4 %all-to-all-start = ((f32[64,1,96]{2,1,0:T(1,128)}), f32[64,1,96]{2,1,0:T(1,128)S(1)}, u32[]{:S(2)}, u32[]{:S(2)}) async-start(f32[64,1,96]{2,1,0:T(1,128)} %modulate.1), calls=%async_computation | async-start | bytes 65536 | tf_op jit(solution)/shard_map/all_to_all | solution.py:266
  21.6 0.9 copy-start.6
  22.3 0.7 copy-start.9
  23.0 1.2 %copy-start = (bf16[1,256,2048]{2,1,0:T(8,128)(2,1)S(1)}, bf16[1,256,2048]{2,1,0:T(8,128)(2,1)}, u32[]{:S(2)}) copy-start(bf16[1,256,2048]{2,1,0:T(8,128)(2,1)} %param.11) | copy-start | bytes 3145732
  24.2 11.9 %copy-start.1 = (bf16[1,256,2048]{2,1,0:T(8,128)(2,1)S(1)}, bf16[1,256,2048]{2,1,0:T(8,128)(2,1)}, u32[]{:S(2)}) copy-start(bf16[1,256,2048]{2,1,0:T(8,128)(2,1)} %param.11) | copy-start | bytes 3145732
  24.8 11.2 %copy-start.8 = (f32[2048]{0:T(1024)S(1)}, f32[2048]{0:T(1024)}, u32[]{:S(2)}) copy-start(f32[2048]{0:T(1024)} %param.15) | copy-start | bytes 24580
  36.1 0.7 copy-start.10
  36.7 1.2 %copy-start.3 = (bf16[2048,256]{1,0:T(8,128)(2,1)S(1)}, bf16[2048,256]{1,0:T(8,128)(2,1)}, u32[]{:S(2)}) copy-start(bf16[2048,256]{1,0:T(8,128)(2,1)} %wq_hbm.1) | copy-start | bytes 3145732
  41.4 0.6 copy-start.7
  42.0 41.9 %copy-start.2 = (bf16[256,2048]{1,0:T(8,128)(2,1)S(1)}, bf16[256,2048]{1,0:T(8,128)(2,1)}, u32[]{:S(2)}) copy-start(bf16[256,2048]{1,0:T(8,128)(2,1)} %w_hbm.1) | copy-start | bytes 3145732
  42.0 41.9 %all-to-all-start.1 = ((bf16[16,40,128]{2,1,0:T(8,128)(2,1)}), bf16[16,40,128]{2,1,0:T(8,128)(2,1)S(1)}, u32[]{:S(2)}, u32[]{:S(2)}) async-start(bf16[16,40,128]{2,1,0:T(8,128)(2,1)} %get-tuple-element.17), calls=%async_computation.1 | async-start | bytes 327680 | tf_op jit(solution)/shard_map/all_to_all | solution.py:316
  91.6 14.4 %all-to-all-start.2 = ((bf16[4,64,2048]{2,1,0:T(8,128)(2,1)}), bf16[4,64,2048]{2,1,0:T(8,128)(2,1)S(1)}, u32[]{:S(2)}, u32[]{:S(2)}) async-start(bf16[4,64,2048]{2,1,0:T(8,128)(2,1)} %bitcast.10), calls=%async_computation.2 | async-start | bytes 2097152 | tf_op jit(solution)/shard_map/all_to_all | solution.py:333

commit v6 on v5

--- a/solution.py
+++ b/solution.py
@@ -62,8 +62,9 @@
     return copies
 
 
-def modulate(cond_ref, w_hbm, out_ref, w_ref, sems):
-    (copy,) = start_all(((w_hbm, w_ref),), sems)
+def modulate(cond_hbm, w_hbm, out_ref, cond_ref, w_ref, sems):
+    cond_in, copy = start_all(((cond_hbm, cond_ref), (w_hbm, w_ref)), sems)
+    cond_in.wait()
     cond = cond_ref[...].astype(jnp.float32)
     active = (cond / (1.0 + jnp.exp(-cond))).astype(jnp.bfloat16)
     active = jnp.broadcast_to(active, (16, active.shape[1]))
@@ -73,33 +74,56 @@
 
 
 def prepare(
-    lat_ref, ctx_ref, wk_ref, wv_ref, kg_ref, inv_ref, ctx_kv_ref, wkv_ref
+    lat_hbm,
+    ctx_hbm,
+    wk_hbm,
+    wv_hbm,
+    qg_ref,
+    kg_ref,
+    inv_ref,
+    ctx_kv_ref,
+    wkv_ref,
+    gains_ref,
+    lat_ref,
+    ctx_ref,
+    sems,
 ):
     rows = lat_ref.shape[0]
     head_dim = kg_ref.shape[1]
+    copies = start_all(
+        (
+            (lat_hbm, lat_ref),
+            (ctx_hbm, ctx_ref),
+            (wk_hbm, wkv_ref.at[pl.ds(0, head_dim)]),
+            (wv_hbm, wkv_ref.at[pl.ds(head_dim, head_dim)]),
+        ),
+        sems,
+    )
+    kg = jnp.concatenate([kg_ref[...]] * 2, axis=1)
+    gains_ref[0:1, :] = jnp.concatenate([qg_ref[...]] * 2, axis=1)
+    gains_ref[1:2, :] = kg
+    copies[0].wait()
     step = 32
     for r in range(0, rows, step):
         x = lat_ref[r : r + step, :].astype(jnp.float32)
         mean_sq = jnp.mean(x * x, axis=-1, keepdims=True)
         inv_ref[r : r + step, :] = jnp.broadcast_to(lax.rsqrt(mean_sq + epsilon), (step, LANES))
-    wkv_ref[0:head_dim, :] = wk_ref[...]
-    wkv_ref[head_dim:, :] = wv_ref[...]
+    for copy in copies[1:]:
+        copy.wait()
     scaled, _, low = turner(head_dim)
     both = contract_last(ctx_ref[...], wkv_ref[...])
-    kg = jnp.concatenate([kg_ref[...]] * 2, axis=1)
     ctx_kv_ref[...] = jnp.where(low, scaled(both, kg), both).astype(jnp.bfloat16)
 
 
 def project(
     lat_ref,
-    wq_hbm,
+    wq_ref,
     wkv_ref,
     inv_ref,
     ctx_kv_ref,
     mod_ref,
     gain_ref,
-    qg_ref,
-    kg_ref,
+    gains_ref,
     cos_ref,
     sin_ref,
     q_hbm,
@@ -110,16 +134,13 @@
     mods_ref,
     q_ref,
     kv_ref,
-    wq_ref,
-    wq_sems,
     q_sems,
     out_sems,
 ):
-    (weights_in,) = start_all(((wq_hbm, wq_ref),), wq_sems)
     rows, width = lat_ref.shape
     main = main_hbm.shape[0]
     rest = rest_hbm.shape[1]
-    head_dim = qg_ref.shape[1]
+    head_dim = wkv_ref.shape[0] // 2
     pieces, _, piece = mod_ref.shape
     for j in range(pieces):
         mods_ref[0:1, piece * j : piece * (j + 1)] = mod_ref[j]
@@ -134,8 +155,7 @@
         hid_ref[r : r + step, :] = hidden.astype(jnp.bfloat16)
 
     scaled, turned, low = turner(head_dim)
-    qg = jnp.concatenate([qg_ref[...]] * 2, axis=1)
-    kg = jnp.concatenate([kg_ref[...]] * 2, axis=1)
+    qg, kg = gains_ref[0:1, :], gains_ref[1:2, :]
     cosine, sine = cos_ref[...], sin_ref[...]
     hid = hid_ref[...]
     both = contract_last(hid, wkv_ref[...])
@@ -148,7 +168,6 @@
         + [(sent, rest_hbm.at[z]) for z in range(rest_hbm.shape[0])],
         out_sems,
     )
-    weights_in.wait()
     queries = jnp.dot(hid, wq_ref[...], preferred_element_type=jnp.float32)
     for g in range(queries.shape[1] // LANES):
         pair = turned(scaled(queries[:, LANES * g : LANES * (g + 1)], qg), cosine, sine)
@@ -162,8 +181,8 @@
         copy.wait()
 
 
-def attend(q_hbm, main_ref, rest_ref, w_hbm, o_ref, q_ref, s_ref, at_ref, w_ref, sems):
-    copies = start_all(((q_hbm, q_ref), (w_hbm, w_ref)), sems)
+def attend(q_ref, main_ref, rest_ref, w_hbm, o_ref, s_ref, at_ref, w_ref, sems):
+    (weights_in,) = start_all(((w_hbm, w_ref),), sems)
     heads, rows, _ = q_ref.shape
     head_dim = at_ref.shape[1] // heads
     parts, at = [], 0
@@ -173,7 +192,6 @@
             size = min(KEY_STEP, count - c)
             parts.append((ref, c, at, size))
             at += size
-    copies[0].wait()
     row_max = None
     for h in range(heads + 1):
         if h < heads:
@@ -201,7 +219,7 @@
                 jnp.bfloat16
             )
         row_max = jnp.max(m, axis=1, keepdims=True)
-    copies[1].wait()
+    weights_in.wait()
     o_ref[...] = jnp.dot(at_ref[...], w_ref[...], preferred_element_type=jnp.float32).astype(
         jnp.bfloat16
     )
@@ -258,8 +276,12 @@
     mod_pieces = pl.pallas_call(
         modulate,
         out_shape=shape((sp * tp, 1, mod_weight.shape[1]), single),
-        in_specs=in_vmem(1) + in_hbm(1),
-        scratch_shapes=[pltpu.VMEM(mod_weight.shape[::-1], half), dma(1)],
+        in_specs=in_hbm(2),
+        scratch_shapes=[
+            pltpu.VMEM(condition.shape, half),
+            pltpu.VMEM(mod_weight.shape[::-1], half),
+            dma(2),
+        ],
         compiler_params=vmem(60),
         name="modulate",
     )(condition, mod_weight.T)
@@ -267,17 +289,19 @@
     cosine, sine = rotary_tables(lax.axis_index("sp") * length, length, 0, head_dim)
 
     wk, wv = w_key.T, w_value.T
-    inverse, ctx_kv, wkv = pl.pallas_call(
+    inverse, ctx_kv, wkv, gains = pl.pallas_call(
         prepare,
         out_shape=(
             shape((length, LANES), single),
             shape((count, LANES), half),
             shape((2 * head_dim, width), half),
+            shape((2, LANES), single),
         ),
-        in_specs=in_vmem(5),
-        compiler_params=vmem(8),
+        in_specs=in_hbm(4) + in_vmem(2),
+        scratch_shapes=[pltpu.VMEM((length, width), half), pltpu.VMEM((count, width), half), dma(4)],
+        compiler_params=vmem(52),
         name="prepare",
-    )(latent[0], context[0], wk, wv, k_gain[None])
+    )(latent[0], context[0], wk, wv, q_gain[None], k_gain[None])
     queries, own_main, own_rest, gate = pl.pallas_call(
         project,
         out_shape=(
@@ -286,15 +310,13 @@
             shape((sp, rest, LANES), half),
             shape((1, width), single),
         ),
-        in_specs=in_vmem(1) + in_hbm(1) + in_vmem(9),
+        in_specs=in_vmem(10),
         out_specs=tuple(in_hbm(3) + in_vmem(1)),
         scratch_shapes=[
             pltpu.VMEM((length, width), half),
             pltpu.VMEM((8, 3 * width), single),
             pltpu.VMEM((heads, length, LANES), half),
             pltpu.VMEM((main + rest, LANES), half),
-            pltpu.VMEM(w_query.shape, half),
-            dma(1),
             dma(heads // 2),
             dma(1 + sp),
         ],
@@ -308,8 +330,7 @@
         ctx_kv,
         modulation,
         norm_gain[None],
-        q_gain[None],
-        k_gain[None],
+        gains,
         cosine,
         sine,
     )
@@ -319,13 +340,12 @@
     terms = pl.pallas_call(
         attend,
         out_shape=shape((length, width), half),
-        in_specs=in_hbm(1) + in_vmem(2) + in_hbm(1),
+        in_specs=in_vmem(3) + in_hbm(1),
         scratch_shapes=[
-            pltpu.VMEM((heads, length, LANES), half),
             pltpu.VMEM((2, length, all_keys), single),
             pltpu.VMEM((length, heads * head_dim), half),
             pltpu.VMEM(w_out.shape, half),
-            dma(2),
+            dma(1),
         ],
         compiler_params=vmem(32),
         name="attend",

time: 107 us -> 104 us (0.972)
  local copies, waits for them, and re-layouts: 4.39 us -> 0.99 us
    unnamed x22 -> x20, local copies, waits for them, and re-layouts: 4.39 us -> 0.99 us
    pallas_call x1, Pallas kernels: 0.6 us -> 2.06 us  [shards(): pl.pallas_call(prepare, out_shape=(shape((length, LANES), single), shape(...]
  transfers between devices with their start and end apart: 3 -> 3, of which waited for: 2 -> 2; matrix products, arithmetic and copies ran while one was open for 1% -> 1% of each run, Pallas kernels for 1% -> 2%
where the time goes in v6:
time: 104 us
  blocking collectives  38.2 us (37%)
  starting transfers between devices  26.1 us (25%)
  waiting for transfers between devices  21.5 us (21%)
  Pallas kernels  16 us (15%)
    all_gather x1, blocking collectives, shards(): all_main = lax.all_gather(own_main, 'sp', axis=0, tiled=True)  38.2 us
    all_to_all x1, starting transfers between devices, shards(): modulation = lax.all_to_all(mod_pieces, ('sp', 'tp'), 0, 0, tiled=True)  18.9 us
    all_to_all x1, waiting for transfers between devices, shards(): lax.all_to_all(terms.reshape(tp, kept, width), 'tp', 0, 0, tiled=True)  10.9 us
    all_to_all x1, waiting for transfers between devices, shards(): modulation = lax.all_to_all(mod_pieces, ('sp', 'tp'), 0, 0, tiled=True)  10.7 us
    pallas_call x1, Pallas kernels, shards(): pl.pallas_call(attend, out_shape=shape((length, width), half), in_specs=i...  7.65 us
    all_to_all x1, starting transfers between devices, shards(): lax.all_to_all(own_rest, 'sp', 0, 0, tiled=True).reshape(sp * rest, LANES)  3.66 us
    all_to_all x1, starting transfers between devices, shards(): lax.all_to_all(terms.reshape(tp, kept, width), 'tp', 0, 0, tiled=True)  3.53 us
    pallas_call x1, Pallas kernels, shards(): pl.pallas_call(project, out_shape=(shape((heads, length, LANES), half), s...  3.34 us
  transfers between devices with their start and end apart: 3, of which 2 were waited for; matrix products, arithmetic and copies ran while one was open for 1% of the time, Pallas kernels for 2%

profile of v6, /device:TPU:6, one launch (start us, length us, event | category | flops | bytes accessed | tf_op | source)
XLA Modules:
  0.0 103.7 jit_solution(9415542009912633260)
XLA Ops:
  0.0 0.0 copy-start.3
  0.0 0.0 copy-start.5
  0.0 0.0 copy-start.9
  0.0 1.9 %modulate.1 = f32[64,1,96]{2,1,0:T(1,128)} custom-call(bf16[1,2048]{1,0:T(2,128)(2,1)} %cond_hbm.1, bf16[96,2048]{1,0:T(8,128)(2,1)} %bitcast.22), custom_call_target="tpu_custom_call" | custom-call | tf_op jit(solution)/shard_map/modulate/pallas_call | solution.py:276
  2.0 0.0 copy-start
  2.0 0.0 copy-start.2
  2.0 18.9 %all-to-all-start = ((f32[64,1,96]{2,1,0:T(1,128)}), f32[64,1,96]{2,1,0:T(1,128)S(1)}, u32[]{:S(2)}, u32[]{:S(2)}) async-start(f32[64,1,96]{2,1,0:T(1,128)} %modulate.1), calls=%async_computation | async-start | bytes 65536 | tf_op jit(solution)/shard_map/all_to_all | solution.py:288
  21.0 0.7 negate_select_fusion
  21.7 0.0 copy-done.3
  21.7 0.0 copy-done.5
  21.7 0.0 copy-done.8
  21.7 0.0 copy-done.9
  21.7 0.0 copy-start.4
  21.7 0.9 copy-done.4
  22.6 2.1 %prepare.1 = (f32[256,128]{1,0:T(8,128)S(1)}, bf16[32,128]{1,0:T(8,128)(2,1)S(1)}, bf16[128,2048]{1,0:T(8,128)(2,1)S(1)}, f32[2,128]{1,0:T(2,128)S(1)}) custom-call(bf16[256,2048]{1,0:T(8,128)(2,1)} %bitcast.12, bf16[32,2048]{1,0:T(8,128)(2,1)S(1)} %bitcast.18, bf16[64,2048]{1,0:T(8,128)(2,1)S(1)} %bitcast.16, bf16[64,2048]{1,0:T(8,128)(2,1)S(1)} %bitcast.17, ...), custom_call_target="tpu_custom_call" | custom-call | tf_op jit(solution)/shard_map/prepare/pallas_call | solution.py:292
  24.7 0.0 copy-start.7
  24.7 10.7 %all-to-all-done.mod_ref = f32[64,1,96]{2,1,0:T(1,128)S(1)} async-done(((f32[64,1,96]{2,1,0:T(1,128)}), f32[64,1,96]{2,1,0:T(1,128)S(1)}, u32[]{:S(2)}, u32[]{:S(2)}) %all-to-all-start) | async-done | bytes 24608 | tf_op jit(solution)/shard_map/all_to_all | solution.py:288
  35.4 0.0 copy-done
  35.4 0.0 copy-done.2
  35.4 0.0 copy-done.7
  35.4 3.3 %project.1 = (bf16[4,256,128]{2,1,0:T(8,128)(2,1)S(1)}, bf16[248,128]{1,0:T(8,128)(2,1)S(1)}, bf16[16,40,128]{2,1,0:T(8,128)(2,1)}, f32[1,2048]{1,0:T(1,128)S(1)}) custom-call(bf16[256,2048]{1,0:T(8,128)(2,1)S(1)} %bitcast.13, bf16[2048,256]{1,0:T(8,128)(2,1)S(1)} %copy-done.2, bf16[128,2048]{1,0:T(8,128)(2,1)S(1)} %get-tuple-element.13.wkv_ref, ...), custom_call_target="tpu_custom_call" | custom-call | tf_op jit(solution)/shard_map/project/pallas_call | solution.py:305
  38.8 0.0 copy-start.6
  38.8 0.0 copy-start.1
  38.8 3.7 %all-to-all-start.1 = ((bf16[16,40,128]{2,1,0:T(8,128)(2,1)}), bf16[16,40,128]{2,1,0:T(8,128)(2,1)S(1)}, u32[]{:S(2)}, u32[]{:S(2)}) async-start(bf16[16,40,128]{2,1,0:T(8,128)(2,1)} %get-tuple-element.19), calls=%async_computation.1 | async-start | bytes 327680 | tf_op jit(solution)/shard_map/all_to_all | solution.py:337
  42.5 0.0 copy-done.6
  42.5 38.2 %all_gather.3.main_ref = bf16[3968,128]{1,0:T(8,128)(2,1)S(1)} all-gather(bf16[248,128]{1,0:T(8,128)(2,1)} %copy-done.6), channel_id=1, replica_groups=mesh['sp'=16,'tp'=4,'dp'=8] {'sp'}, dimensions={0}, use_global_device_ids=true | all-gather | bytes 1079296 | tf_op jit(solution)/shard_map/all_gather | solution.py:338
  80.7 0.0 all-to-all-done.1
  80.7 0.0 copy-done.1
  80.7 7.7 %attend.1 = bf16[256,2048]{1,0:T(8,128)(2,1)} custom-call(bf16[4,256,128]{2,1,0:T(8,128)(2,1)S(1)} %get-tuple-element.17.q_ref, bf16[3968,128]{1,0:T(8,128)(2,1)S(1)} %all_gather.3.main_ref, bf16[640,128]{1,0:T(8,128)(2,1)S(1)} %bitcast.15, bf16[256,2048]{1,0:T(8,128)(2,1)S(1)} %copy-done.1), custom_call_target="tpu_custom_call" | custom-call | tf_op jit(solution)/shard_map/attend/pallas_call | solution.py:340
  88.4 3.5 %all-to-all-start.2 = ((bf16[4,64,2048]{2,1,0:T(8,128)(2,1)}), bf16[4,64,2048]{2,1,0:T(8,128)(2,1)S(1)}, u32[]{:S(2)}, u32[]{:S(2)}) async-start(bf16[4,64,2048]{2,1,0:T(8,128)(2,1)} %bitcast.10), calls=%async_computation.2 | async-start | bytes 2097152 | tf_op jit(solution)/shard_map/all_to_all | solution.py:353
  91.9 10.9 %all-to-all-done.2.terms_ref = bf16[4,64,2048]{2,1,0:T(8,128)(2,1)S(1)} async-done(((bf16[4,64,2048]{2,1,0:T(8,128)(2,1)}), bf16[4,64,2048]{2,1,0:T(8,128)(2,1)S(1)}, u32[]{:S(2)}, u32[]{:S(2)}) %all-to-all-start.2) | async-done | bytes 1048608 | tf_op jit(solution)/shard_map/all_to_all | solution.py:353
  102.8 1.0 finish.1
  (10 shorter events, 0.1 us)
Async XLA Ops:
  0.0 21.7 %copy-start.3 = (bf16[2048,64]{0,1:T(8,128)(2,1)S(1)}, bf16[2048,64]{0,1:T(8,128)(2,1)}, u32[]{:S(2)}) copy-start(bf16[2048,64]{0,1:T(8,128)(2,1)} %param.17) | copy-start | bytes 786436
  0.0 21.7 %copy-start.5 = (bf16[1,32,2048]{2,1,0:T(8,128)(2,1)S(1)}, bf16[1,32,2048]{2,1,0:T(8,128)(2,1)}, u32[]{:S(2)}) copy-start(bf16[1,32,2048]{2,1,0:T(8,128)(2,1)} %param.12) | copy-start | bytes 393220
  0.0 21.7 %copy-start.8 = (f32[64]{0:T(128)S(1)}, f32[64]{0:T(128)}, u32[]{:S(2)}) copy-start(f32[64]{0:T(128)} %param.19) | copy-start | bytes 772
  0.0 21.7 %copy-start.9 = (f32[64]{0:T(128)S(1)}, f32[64]{0:T(128)}, u32[]{:S(2)}) copy-start(f32[64]{0:T(128)} %param.20) | copy-start | bytes 772
  2.0 33.5 %copy-start = (bf16[1,256,2048]{2,1,0:T(8,128)(2,1)S(1)}, bf16[1,256,2048]{2,1,0:T(8,128)(2,1)}, u32[]{:S(2)}) copy-start(bf16[1,256,2048]{2,1,0:T(8,128)(2,1)} %param.11) | copy-start | bytes 3145732
  2.0 33.5 %copy-start.2 = (bf16[2048,256]{1,0:T(8,128)(2,1)S(1)}, bf16[2048,256]{1,0:T(8,128)(2,1)}, u32[]{:S(2)}) copy-start(bf16[2048,256]{1,0:T(8,128)(2,1)} %wq_ref.1) | copy-start | bytes 3145732
  2.0 33.4 %all-to-all-start = ((f32[64,1,96]{2,1,0:T(1,128)}), f32[64,1,96]{2,1,0:T(1,128)S(1)}, u32[]{:S(2)}, u32[]{:S(2)}) async-start(f32[64,1,96]{2,1,0:T(1,128)} %modulate.1), calls=%async_computation | async-start | bytes 65536 | tf_op jit(solution)/shard_map/all_to_all | solution.py:288
  21.7 1.0 copy-start.4
  24.7 10.7 %copy-start.7 = (f32[2048]{0:T(1024)S(1)}, f32[2048]{0:T(1024)}, u32[]{:S(2)}) copy-start(f32[2048]{0:T(1024)} %param.15) | copy-start | bytes 24580
  38.8 3.7 %copy-start.6 = (bf16[248,128]{1,0:T(8,128)(2,1)}, bf16[248,128]{1,0:T(8,128)(2,1)S(1)}, u32[]{:S(2)}) copy-start(bf16[248,128]{1,0:T(8,128)(2,1)S(1)} %get-tuple-element.18) | copy-start | bytes 190468
  38.8 41.9 %copy-start.1 = (bf16[256,2048]{1,0:T(8,128)(2,1)S(1)}, bf16[256,2048]{1,0:T(8,128)(2,1)}, u32[]{:S(2)}) copy-start(bf16[256,2048]{1,0:T(8,128)(2,1)} %w_hbm.1) | copy-start | bytes 3145732
  38.8 41.9 %all-to-all-start.1 = ((bf16[16,40,128]{2,1,0:T(8,128)(2,1)}), bf16[16,40,128]{2,1,0:T(8,128)(2,1)S(1)}, u32[]{:S(2)}, u32[]{:S(2)}) async-start(bf16[16,40,128]{2,1,0:T(8,128)(2,1)} %get-tuple-element.19), calls=%async_computation.1 | async-start | bytes 327680 | tf_op jit(solution)/shard_map/all_to_all | solution.py:337
  88.4 14.4 %all-to-all-start.2 = ((bf16[4,64,2048]{2,1,0:T(8,128)(2,1)}), bf16[4,64,2048]{2,1,0:T(8,128)(2,1)S(1)}, u32[]{:S(2)}, u32[]{:S(2)}) async-start(bf16[4,64,2048]{2,1,0:T(8,128)(2,1)} %bitcast.10), calls=%async_computation.2 | async-start | bytes 2097152 | tf_op jit(solution)/shard_map/all_to_all | solution.py:353

commit v7 on v6

--- a/solution.py
+++ b/solution.py
@@ -225,9 +225,9 @@
     )
 
 
-def finish(at_ref, lat_hbm, terms_ref, gate_ref, out_ref, kept_ref, sems):
+def finish(lat_hbm, terms_ref, gate_ref, out_ref, kept_ref, sems):
     kept = kept_ref.shape[0]
-    at = pl.multiple_of(at_ref[0] * kept, kept)
+    at = pl.multiple_of(lax.axis_index("tp") * kept, kept)
     (copy,) = start_all(((lat_hbm.at[pl.ds(at, kept)], kept_ref),), sems)
     projected = terms_ref[0].astype(jnp.float32)
     for g in range(1, terms_ref.shape[0]):
@@ -354,11 +354,11 @@
     mixed = pl.pallas_call(
         finish,
         out_shape=shape((kept, width), half),
-        in_specs=[pl.BlockSpec(memory_space=pltpu.SMEM)] + in_hbm(1) + in_vmem(2),
+        in_specs=in_hbm(1) + in_vmem(2),
         scratch_shapes=[pltpu.VMEM((kept, width), half), dma(1)],
         compiler_params=vmem(8),
         name="finish",
-    )(lax.axis_index("tp").astype(jnp.int32)[None], latent[0], terms, gate)
+    )(latent[0], terms, gate)
     return mixed[None]
 
 

time: 104 us -> 103 us (level)
  blocking collectives: 38.2 us -> 52.2 us
  waiting for transfers between devices: 21.5 us -> 10.7 us
  starting transfers between devices: 26.1 us -> 22.5 us
    all_to_all x0 -> x1, blocking collectives: none -> 14 us  [shards(): lax.all_to_all(terms.reshape(tp, kept, width), 'tp', 0, 0, tiled=True)]
    all_to_all x1 -> x0, waiting for transfers between devices: 10.9 us -> none  [shards(): lax.all_to_all(terms.reshape(tp, kept, width), 'tp', 0, 0, tiled=True)]
    all_to_all x1 -> x0, starting transfers between devices: 3.53 us -> none  [shards(): lax.all_to_all(terms.reshape(tp, kept, width), 'tp', 0, 0, tiled=True)]
  transfers between devices with their start and end apart: 3 -> 2, of which waited for: 2 -> 1; matrix products, arithmetic and copies ran while one was open for 1% -> 1% of each run, Pallas kernels for 2% -> 2%
where the time goes in v7:
time: 103 us; the launch traced here: 102 us
  blocking collectives  52.2 us (51%)
  starting transfers between devices  22.5 us (22%)
  Pallas kernels  15 us (15%)
  waiting for transfers between devices  10.7 us (10%)
    all_gather x1, blocking collectives, shards(): all_main = lax.all_gather(own_main, 'sp', axis=0, tiled=True)  38.2 us
    all_to_all x1, starting transfers between devices, shards(): modulation = lax.all_to_all(mod_pieces, ('sp', 'tp'), 0, 0, tiled=True)  18.9 us
    all_to_all x1, blocking collectives, shards(): lax.all_to_all(terms.reshape(tp, kept, width), 'tp', 0, 0, tiled=True)  14 us
    all_to_all x1, waiting for transfers between devices, shards(): modulation = lax.all_to_all(mod_pieces, ('sp', 'tp'), 0, 0, tiled=True)  10.7 us
    pallas_call x1, Pallas kernels, shards(): pl.pallas_call(attend, out_shape=shape((length, width), half), in_specs=i...  6.65 us
    all_to_all x1, starting transfers between devices, shards(): lax.all_to_all(own_rest, 'sp', 0, 0, tiled=True).reshape(sp * rest, LANES)  3.66 us
    pallas_call x1, Pallas kernels, shards(): pl.pallas_call(project, out_shape=(shape((heads, length, LANES), half), s...  3.34 us
    pallas_call x1, Pallas kernels, shards(): pl.pallas_call(prepare, out_shape=(shape((length, LANES), single), shape(...  2.06 us
  transfers between devices with their start and end apart: 2, of which 1 were waited for; matrix products, arithmetic and copies ran while one was open for 1% of the time, Pallas kernels for 2%

profile of v7, /device:TPU:6, one launch (start us, length us, event | category | flops | bytes accessed | tf_op | source)
XLA Modules:
  0.0 102.3 jit_solution(3539084125165523976)
XLA Ops:
  0.0 0.0 copy-start.3
  0.0 0.0 copy-start.5
  0.0 0.0 copy-start.8
  0.0 0.0 copy-start.9
  0.0 1.9 %modulate.1 = f32[64,1,96]{2,1,0:T(1,128)} custom-call(bf16[1,2048]{1,0:T(2,128)(2,1)} %cond_hbm.1, bf16[96,2048]{1,0:T(8,128)(2,1)} %bitcast.22), custom_call_target="tpu_custom_call" | custom-call | tf_op jit(solution)/shard_map/modulate/pallas_call | solution.py:276
  2.0 0.0 copy-start
  2.0 0.0 copy-start.2
  2.0 18.9 %all-to-all-start = ((f32[64,1,96]{2,1,0:T(1,128)}), f32[64,1,96]{2,1,0:T(1,128)S(1)}, u32[]{:S(2)}, u32[]{:S(2)}) async-start(f32[64,1,96]{2,1,0:T(1,128)} %modulate.1), calls=%async_computation | async-start | bytes 65536 | tf_op jit(solution)/shard_map/all_to_all | solution.py:288
  21.0 0.7 negate_select_fusion
  21.7 0.0 copy-done.3
  21.7 0.0 copy-done.5
  21.7 0.0 copy-done.8
  21.7 0.0 copy-done.9
  21.7 0.0 copy-start.4
  21.7 0.9 copy-done.4
  22.6 2.1 %prepare.1 = (f32[256,128]{1,0:T(8,128)S(1)}, bf16[32,128]{1,0:T(8,128)(2,1)S(1)}, bf16[128,2048]{1,0:T(8,128)(2,1)S(1)}, f32[2,128]{1,0:T(2,128)S(1)}) custom-call(bf16[256,2048]{1,0:T(8,128)(2,1)} %bitcast.11, bf16[32,2048]{1,0:T(8,128)(2,1)S(1)} %bitcast.18, bf16[64,2048]{1,0:T(8,128)(2,1)S(1)} %bitcast.16, bf16[64,2048]{1,0:T(8,128)(2,1)S(1)} %bitcast.17, ...), custom_call_target="tpu_custom_call" | custom-call | tf_op jit(solution)/shard_map/prepare/pallas_call | solution.py:292
  24.7 0.0 copy-start.7
  24.7 10.7 %all-to-all-done.mod_ref = f32[64,1,96]{2,1,0:T(1,128)S(1)} async-done(((f32[64,1,96]{2,1,0:T(1,128)}), f32[64,1,96]{2,1,0:T(1,128)S(1)}, u32[]{:S(2)}, u32[]{:S(2)}) %all-to-all-start) | async-done | bytes 24608 | tf_op jit(solution)/shard_map/all_to_all | solution.py:288
  35.4 0.0 copy-done
  35.4 0.0 copy-done.2
  35.4 0.0 copy-done.7
  35.4 3.3 %project.1 = (bf16[4,256,128]{2,1,0:T(8,128)(2,1)S(1)}, bf16[248,128]{1,0:T(8,128)(2,1)S(1)}, bf16[16,40,128]{2,1,0:T(8,128)(2,1)}, f32[1,2048]{1,0:T(1,128)S(1)}) custom-call(bf16[256,2048]{1,0:T(8,128)(2,1)S(1)} %bitcast.12, bf16[2048,256]{1,0:T(8,128)(2,1)S(1)} %copy-done.2, bf16[128,2048]{1,0:T(8,128)(2,1)S(1)} %get-tuple-element.13.wkv_ref, ...), custom_call_target="tpu_custom_call" | custom-call | tf_op jit(solution)/shard_map/project/pallas_call | solution.py:305
  38.8 0.0 copy-start.6
  38.8 0.0 copy-start.1
  38.8 3.7 %all-to-all-start.1 = ((bf16[16,40,128]{2,1,0:T(8,128)(2,1)}), bf16[16,40,128]{2,1,0:T(8,128)(2,1)S(1)}, u32[]{:S(2)}, u32[]{:S(2)}) async-start(bf16[16,40,128]{2,1,0:T(8,128)(2,1)} %get-tuple-element.19), calls=%async_computation.1 | async-start | bytes 327680 | tf_op jit(solution)/shard_map/all_to_all | solution.py:337
  42.5 0.0 copy-done.6
  42.5 38.2 %all_gather.3.main_ref = bf16[3968,128]{1,0:T(8,128)(2,1)S(1)} all-gather(bf16[248,128]{1,0:T(8,128)(2,1)} %copy-done.6), channel_id=1, replica_groups=mesh['sp'=16,'tp'=4,'dp'=8] {'sp'}, dimensions={0}, use_global_device_ids=true | all-gather | bytes 1079296 | tf_op jit(solution)/shard_map/all_gather | solution.py:338
  80.7 0.0 all-to-all-done.1
  80.7 0.0 copy-done.1
  80.7 6.7 %attend.1 = bf16[256,2048]{1,0:T(8,128)(2,1)S(1)} custom-call(bf16[4,256,128]{2,1,0:T(8,128)(2,1)S(1)} %get-tuple-element.17.q_ref, bf16[3968,128]{1,0:T(8,128)(2,1)S(1)} %all_gather.3.main_ref, bf16[640,128]{1,0:T(8,128)(2,1)S(1)} %bitcast.15, bf16[256,2048]{1,0:T(8,128)(2,1)S(1)} %copy-done.1), custom_call_target="tpu_custom_call" | custom-call | tf_op jit(solution)/shard_map/attend/pallas_call | solution.py:340
  87.4 14.0 %all_to_all.15.terms_ref = bf16[4,64,2048]{2,1,0:T(8,128)(2,1)S(1)} all-to-all(bf16[4,64,2048]{2,1,0:T(8,128)(2,1)S(1)} %bitcast.14), channel_id=1, replica_groups=mesh['sp'=16,'tp'=4,'dp'=8] {'tp'}, dimensions={0} | all-to-all | bytes 2097152 | tf_op jit(solution)/shard_map/all_to_all | solution.py:353
  101.3 1.0 finish.1
  (9 shorter events, 0.1 us)
Async XLA Ops:
  0.0 21.7 %copy-start.3 = (bf16[2048,64]{0,1:T(8,128)(2,1)S(1)}, bf16[2048,64]{0,1:T(8,128)(2,1)}, u32[]{:S(2)}) copy-start(bf16[2048,64]{0,1:T(8,128)(2,1)} %param.17) | copy-start | bytes 786436
  0.0 21.7 %copy-start.5 = (bf16[1,32,2048]{2,1,0:T(8,128)(2,1)S(1)}, bf16[1,32,2048]{2,1,0:T(8,128)(2,1)}, u32[]{:S(2)}) copy-start(bf16[1,32,2048]{2,1,0:T(8,128)(2,1)} %param.12) | copy-start | bytes 393220
  0.0 21.7 %copy-start.8 = (f32[64]{0:T(128)S(1)}, f32[64]{0:T(128)}, u32[]{:S(2)}) copy-start(f32[64]{0:T(128)} %param.19) | copy-start | bytes 772
  0.0 21.7 %copy-start.9 = (f32[64]{0:T(128)S(1)}, f32[64]{0:T(128)}, u32[]{:S(2)}) copy-start(f32[64]{0:T(128)} %param.20) | copy-start | bytes 772
  2.0 33.5 %copy-start = (bf16[1,256,2048]{2,1,0:T(8,128)(2,1)S(1)}, bf16[1,256,2048]{2,1,0:T(8,128)(2,1)}, u32[]{:S(2)}) copy-start(bf16[1,256,2048]{2,1,0:T(8,128)(2,1)} %param.11) | copy-start | bytes 3145732
  2.0 33.5 %copy-start.2 = (bf16[2048,256]{1,0:T(8,128)(2,1)S(1)}, bf16[2048,256]{1,0:T(8,128)(2,1)}, u32[]{:S(2)}) copy-start(bf16[2048,256]{1,0:T(8,128)(2,1)} %wq_ref.1) | copy-start | bytes 3145732
  2.0 33.4 %all-to-all-start = ((f32[64,1,96]{2,1,0:T(1,128)}), f32[64,1,96]{2,1,0:T(1,128)S(1)}, u32[]{:S(2)}, u32[]{:S(2)}) async-start(f32[64,1,96]{2,1,0:T(1,128)} %modulate.1), calls=%async_computation | async-start | bytes 65536 | tf_op jit(solution)/shard_map/all_to_all | solution.py:288
  21.7 1.0 copy-start.4
  24.7 10.7 %copy-start.7 = (f32[2048]{0:T(1024)S(1)}, f32[2048]{0:T(1024)}, u32[]{:S(2)}) copy-start(f32[2048]{0:T(1024)} %param.15) | copy-start | bytes 24580
  38.8 3.7 %copy-start.6 = (bf16[248,128]{1,0:T(8,128)(2,1)}, bf16[248,128]{1,0:T(8,128)(2,1)S(1)}, u32[]{:S(2)}) copy-start(bf16[248,128]{1,0:T(8,128)(2,1)S(1)} %get-tuple-element.18) | copy-start | bytes 190468
  38.8 41.9 %copy-start.1 = (bf16[256,2048]{1,0:T(8,128)(2,1)S(1)}, bf16[256,2048]{1,0:T(8,128)(2,1)}, u32[]{:S(2)}) copy-start(bf16[256,2048]{1,0:T(8,128)(2,1)} %w_hbm.1) | copy-start | bytes 3145732
  38.8 41.9 %all-to-all-start.1 = ((bf16[16,40,128]{2,1,0:T(8,128)(2,1)}), bf16[16,40,128]{2,1,0:T(8,128)(2,1)S(1)}, u32[]{:S(2)}, u32[]{:S(2)}) async-start(bf16[16,40,128]{2,1,0:T(8,128)(2,1)} %get-tuple-element.19), calls=%async_computation.1 | async-start | bytes 327680 | tf_op jit(solution)/shard_map/all_to_all | solution.py:337

commit v8 on v7

--- a/solution.py
+++ b/solution.py
@@ -126,15 +126,13 @@
     gains_ref,
     cos_ref,
     sin_ref,
-    q_hbm,
+    q_ref,
     main_hbm,
     rest_hbm,
     gate_ref,
     hid_ref,
     mods_ref,
-    q_ref,
     kv_ref,
-    q_sems,
     out_sems,
 ):
     rows, width = lat_ref.shape
@@ -175,8 +173,6 @@
         other = pltpu.roll(pair, head_dim, 1)
         q_ref[2 * g] = jnp.where(low, pair, 0.0).astype(jnp.bfloat16)
         q_ref[2 * g + 1] = jnp.where(low, other, 0.0).astype(jnp.bfloat16)
-        pair_of = pl.ds(2 * g, 2)
-        outs += start_all(((q_ref.at[pair_of], q_hbm.at[pair_of]),), q_sems.at[pl.ds(g, 1)])
     for copy in outs:
         copy.wait()
 
@@ -225,15 +221,13 @@
     )
 
 
-def finish(lat_hbm, terms_ref, gate_ref, out_ref, kept_ref, sems):
-    kept = kept_ref.shape[0]
+def finish(lat_ref, terms_ref, gate_ref, out_ref):
+    kept = out_ref.shape[0]
     at = pl.multiple_of(lax.axis_index("tp") * kept, kept)
-    (copy,) = start_all(((lat_hbm.at[pl.ds(at, kept)], kept_ref),), sems)
     projected = terms_ref[0].astype(jnp.float32)
     for g in range(1, terms_ref.shape[0]):
         projected = projected + terms_ref[g].astype(jnp.float32)
-    copy.wait()
-    residual = kept_ref[...].astype(jnp.float32)
+    residual = lat_ref[pl.ds(at, kept), :].astype(jnp.float32)
     out_ref[...] = (residual + gate_ref[...] * projected).astype(jnp.bfloat16)
 
 
@@ -311,13 +305,11 @@
             shape((1, width), single),
         ),
         in_specs=in_vmem(10),
-        out_specs=tuple(in_hbm(3) + in_vmem(1)),
+        out_specs=tuple(in_vmem(1) + in_hbm(2) + in_vmem(1)),
         scratch_shapes=[
             pltpu.VMEM((length, width), half),
             pltpu.VMEM((8, 3 * width), single),
-            pltpu.VMEM((heads, length, LANES), half),
             pltpu.VMEM((main + rest, LANES), half),
-            dma(heads // 2),
             dma(1 + sp),
         ],
         compiler_params=vmem(16),
@@ -354,8 +346,7 @@
     mixed = pl.pallas_call(
         finish,
         out_shape=shape((kept, width), half),
-        in_specs=in_hbm(1) + in_vmem(2),
-        scratch_shapes=[pltpu.VMEM((kept, width), half), dma(1)],
+        in_specs=in_vmem(3),
         compiler_params=vmem(8),
         name="finish",
     )(latent[0], terms, gate)

time: 103 us -> 102 us (level)
  no operation moved by 1% of the time
where the time goes in v8:
time: 102 us; the launch traced here: 101 us
  blocking collectives  52.2 us (51%)
  starting transfers between devices  22.5 us (22%)
  Pallas kernels  14.1 us (14%)
  waiting for transfers between devices  10.7 us (10%)
    all_gather x1, blocking collectives, shards(): all_main = lax.all_gather(own_main, 'sp', axis=0, tiled=True)  38.2 us
    all_to_all x1, starting transfers between devices, shards(): modulation = lax.all_to_all(mod_pieces, ('sp', 'tp'), 0, 0, tiled=True)  18.9 us
    all_to_all x1, blocking collectives, shards(): lax.all_to_all(terms.reshape(tp, kept, width), 'tp', 0, 0, tiled=True)  14 us
    all_to_all x1, waiting for transfers between devices, shards(): modulation = lax.all_to_all(mod_pieces, ('sp', 'tp'), 0, 0, tiled=True)  10.7 us
    pallas_call x1, Pallas kernels, shards(): pl.pallas_call(attend, out_shape=shape((length, width), half), in_specs=i...  6.65 us
    all_to_all x1, starting transfers between devices, shards(): lax.all_to_all(own_rest, 'sp', 0, 0, tiled=True).reshape(sp * rest, LANES)  3.66 us
    pallas_call x1, Pallas kernels, shards(): pl.pallas_call(project, out_shape=(shape((heads, length, LANES), half), s...  2.56 us
    pallas_call x1, Pallas kernels, shards(): pl.pallas_call(prepare, out_shape=(shape((length, LANES), single), shape(...  2.06 us
  transfers between devices with their start and end apart: 2, of which 1 were waited for; matrix products, arithmetic and copies ran while one was open for 1% of the time, Pallas kernels for 2%

profile of v8, /device:TPU:6, one launch (start us, length us, event | category | flops | bytes accessed | tf_op | source)
XLA Modules:
  0.0 101.4 jit_solution(6930799216164751580)
XLA Ops:
  0.0 0.0 copy-start.3
  0.0 0.0 copy-start.5
  0.0 0.0 copy-start.8
  0.0 0.0 copy-start.9
  0.0 1.9 %modulate.1 = f32[64,1,96]{2,1,0:T(1,128)} custom-call(bf16[1,2048]{1,0:T(2,128)(2,1)} %cond_hbm.1, bf16[96,2048]{1,0:T(8,128)(2,1)} %bitcast.22), custom_call_target="tpu_custom_call" | custom-call | tf_op jit(solution)/shard_map/modulate/pallas_call | solution.py:270
  2.0 0.0 copy-start
  2.0 0.0 copy-start.2
  2.0 18.9 %all-to-all-start = ((f32[64,1,96]{2,1,0:T(1,128)}), f32[64,1,96]{2,1,0:T(1,128)S(1)}, u32[]{:S(2)}, u32[]{:S(2)}) async-start(f32[64,1,96]{2,1,0:T(1,128)} %modulate.1), calls=%async_computation | async-start | bytes 65536 | tf_op jit(solution)/shard_map/all_to_all | solution.py:282
  21.0 0.7 negate_select_fusion
  21.7 0.0 copy-done.3
  21.7 0.0 copy-done.5
  21.7 0.0 copy-done.8
  21.7 0.0 copy-done.9
  21.7 0.0 copy-start.4
  21.7 0.9 copy-done.4
  22.6 2.1 %prepare.1 = (f32[256,128]{1,0:T(8,128)S(1)}, bf16[32,128]{1,0:T(8,128)(2,1)S(1)}, bf16[128,2048]{1,0:T(8,128)(2,1)S(1)}, f32[2,128]{1,0:T(2,128)S(1)}) custom-call(bf16[256,2048]{1,0:T(8,128)(2,1)} %bitcast.11, bf16[32,2048]{1,0:T(8,128)(2,1)S(1)} %bitcast.18, bf16[64,2048]{1,0:T(8,128)(2,1)S(1)} %bitcast.16, bf16[64,2048]{1,0:T(8,128)(2,1)S(1)} %bitcast.17, ...), custom_call_target="tpu_custom_call" | custom-call | tf_op jit(solution)/shard_map/prepare/pallas_call | solution.py:286
  24.7 0.0 copy-start.7
  24.7 10.7 %all-to-all-done.mod_ref = f32[64,1,96]{2,1,0:T(1,128)S(1)} async-done(((f32[64,1,96]{2,1,0:T(1,128)}), f32[64,1,96]{2,1,0:T(1,128)S(1)}, u32[]{:S(2)}, u32[]{:S(2)}) %all-to-all-start) | async-done | bytes 24608 | tf_op jit(solution)/shard_map/all_to_all | solution.py:282
  35.4 0.0 copy-done
  35.4 0.0 copy-done.2
  35.4 0.0 copy-done.7
  35.4 2.6 %project.1 = (bf16[4,256,128]{2,1,0:T(8,128)(2,1)S(1)}, bf16[248,128]{1,0:T(8,128)(2,1)S(1)}, bf16[16,40,128]{2,1,0:T(8,128)(2,1)}, f32[1,2048]{1,0:T(1,128)S(1)}) custom-call(bf16[256,2048]{1,0:T(8,128)(2,1)S(1)} %bitcast.12, bf16[2048,256]{1,0:T(8,128)(2,1)S(1)} %copy-done.2, bf16[128,2048]{1,0:T(8,128)(2,1)S(1)} %get-tuple-element.13.wkv_ref, ...), custom_call_target="tpu_custom_call" | custom-call | tf_op jit(solution)/shard_map/project/pallas_call | solution.py:299
  38.0 0.0 copy-start.6
  38.0 0.0 copy-start.1
  38.0 3.7 %all-to-all-start.1 = ((bf16[16,40,128]{2,1,0:T(8,128)(2,1)}), bf16[16,40,128]{2,1,0:T(8,128)(2,1)S(1)}, u32[]{:S(2)}, u32[]{:S(2)}) async-start(bf16[16,40,128]{2,1,0:T(8,128)(2,1)} %get-tuple-element.19), calls=%async_computation.1 | async-start | bytes 327680 | tf_op jit(solution)/shard_map/all_to_all | solution.py:329
  41.7 0.0 copy-done.6
  41.7 38.2 %all_gather.3.main_ref = bf16[3968,128]{1,0:T(8,128)(2,1)S(1)} all-gather(bf16[248,128]{1,0:T(8,128)(2,1)} %copy-done.6), channel_id=1, replica_groups=mesh['sp'=16,'tp'=4,'dp'=8] {'sp'}, dimensions={0}, use_global_device_ids=true | all-gather | bytes 1079296 | tf_op jit(solution)/shard_map/all_gather | solution.py:330
  79.9 0.0 all-to-all-done.1
  79.9 0.0 copy-done.1
  79.9 6.7 %attend.1 = bf16[256,2048]{1,0:T(8,128)(2,1)S(1)} custom-call(bf16[4,256,128]{2,1,0:T(8,128)(2,1)S(1)} %get-tuple-element.17.q_ref, bf16[3968,128]{1,0:T(8,128)(2,1)S(1)} %all_gather.3.main_ref, bf16[640,128]{1,0:T(8,128)(2,1)S(1)} %bitcast.15, bf16[256,2048]{1,0:T(8,128)(2,1)S(1)} %copy-done.1), custom_call_target="tpu_custom_call" | custom-call | tf_op jit(solution)/shard_map/attend/pallas_call | solution.py:332
  86.6 14.0 %all_to_all.15.terms_ref = bf16[4,64,2048]{2,1,0:T(8,128)(2,1)S(1)} all-to-all(bf16[4,64,2048]{2,1,0:T(8,128)(2,1)S(1)} %bitcast.14), channel_id=1, replica_groups=mesh['sp'=16,'tp'=4,'dp'=8] {'tp'}, dimensions={0} | all-to-all | bytes 2097152 | tf_op jit(solution)/shard_map/all_to_all | solution.py:345
  100.6 0.9 finish.1
  (9 shorter events, 0.1 us)
Async XLA Ops:
  0.0 21.7 %copy-start.3 = (bf16[2048,64]{0,1:T(8,128)(2,1)S(1)}, bf16[2048,64]{0,1:T(8,128)(2,1)}, u32[]{:S(2)}) copy-start(bf16[2048,64]{0,1:T(8,128)(2,1)} %param.17) | copy-start | bytes 786436
  0.0 21.7 %copy-start.5 = (bf16[1,32,2048]{2,1,0:T(8,128)(2,1)S(1)}, bf16[1,32,2048]{2,1,0:T(8,128)(2,1)}, u32[]{:S(2)}) copy-start(bf16[1,32,2048]{2,1,0:T(8,128)(2,1)} %param.12) | copy-start | bytes 393220
  0.0 21.7 %copy-start.8 = (f32[64]{0:T(128)S(1)}, f32[64]{0:T(128)}, u32[]{:S(2)}) copy-start(f32[64]{0:T(128)} %param.19) | copy-start | bytes 772
  0.0 21.7 %copy-start.9 = (f32[64]{0:T(128)S(1)}, f32[64]{0:T(128)}, u32[]{:S(2)}) copy-start(f32[64]{0:T(128)} %param.20) | copy-start | bytes 772
  2.0 33.5 %copy-start = (bf16[1,256,2048]{2,1,0:T(8,128)(2,1)S(1)}, bf16[1,256,2048]{2,1,0:T(8,128)(2,1)}, u32[]{:S(2)}) copy-start(bf16[1,256,2048]{2,1,0:T(8,128)(2,1)} %param.11) | copy-start | bytes 3145732
  2.0 33.5 %copy-start.2 = (bf16[2048,256]{1,0:T(8,128)(2,1)S(1)}, bf16[2048,256]{1,0:T(8,128)(2,1)}, u32[]{:S(2)}) copy-start(bf16[2048,256]{1,0:T(8,128)(2,1)} %wq_ref.1) | copy-start | bytes 3145732
  2.0 33.4 %all-to-all-start = ((f32[64,1,96]{2,1,0:T(1,128)}), f32[64,1,96]{2,1,0:T(1,128)S(1)}, u32[]{:S(2)}, u32[]{:S(2)}) async-start(f32[64,1,96]{2,1,0:T(1,128)} %modulate.1), calls=%async_computation | async-start | bytes 65536 | tf_op jit(solution)/shard_map/all_to_all | solution.py:282
  21.7 1.0 copy-start.4
  24.7 10.7 %copy-start.7 = (f32[2048]{0:T(1024)S(1)}, f32[2048]{0:T(1024)}, u32[]{:S(2)}) copy-start(f32[2048]{0:T(1024)} %param.15) | copy-start | bytes 24580
  38.0 3.7 %copy-start.6 = (bf16[248,128]{1,0:T(8,128)(2,1)}, bf16[248,128]{1,0:T(8,128)(2,1)S(1)}, u32[]{:S(2)}) copy-start(bf16[248,128]{1,0:T(8,128)(2,1)S(1)} %get-tuple-element.18) | copy-start | bytes 190468
  38.0 41.9 %copy-start.1 = (bf16[256,2048]{1,0:T(8,128)(2,1)S(1)}, bf16[256,2048]{1,0:T(8,128)(2,1)}, u32[]{:S(2)}) copy-start(bf16[256,2048]{1,0:T(8,128)(2,1)} %w_hbm.1) | copy-start | bytes 3145732
  38.0 41.9 %all-to-all-start.1 = ((bf16[16,40,128]{2,1,0:T(8,128)(2,1)}), bf16[16,40,128]{2,1,0:T(8,128)(2,1)S(1)}, u32[]{:S(2)}, u32[]{:S(2)}) async-start(bf16[16,40,128]{2,1,0:T(8,128)(2,1)} %get-tuple-element.19), calls=%async_computation.1 | async-start | bytes 327680 | tf_op jit(solution)/shard_map/all_to_all | solution.py:329

commit v9 on v8

--- a/solution.py
+++ b/solution.py
@@ -24,7 +24,8 @@
     freqs = rope_base ** (-(lane % quarter).astype(jnp.float32) / quarter)
     angle = place.astype(jnp.float32) * freqs
     sine = jnp.sin(angle)
-    return jnp.cos(angle), jnp.where(lane % (2 * quarter) < quarter, -sine, sine)
+    sine = jnp.where(lane % (2 * quarter) < quarter, -sine, sine)
+    return jnp.where(lane < head_dim, jnp.cos(angle), sine)
 
 
 def turner(head_dim):
@@ -84,11 +85,13 @@
     ctx_kv_ref,
     wkv_ref,
     gains_ref,
+    kept_ref,
     lat_ref,
     ctx_ref,
     sems,
 ):
     rows = lat_ref.shape[0]
+    kept = kept_ref.shape[0]
     head_dim = kg_ref.shape[1]
     copies = start_all(
         (
@@ -103,6 +106,8 @@
     gains_ref[0:1, :] = jnp.concatenate([qg_ref[...]] * 2, axis=1)
     gains_ref[1:2, :] = kg
     copies[0].wait()
+    at = pl.multiple_of(lax.axis_index("tp") * kept, kept)
+    kept_ref[...] = lat_ref[pl.ds(at, kept), :]
     step = 32
     for r in range(0, rows, step):
         x = lat_ref[r : r + step, :].astype(jnp.float32)
@@ -124,8 +129,7 @@
     mod_ref,
     gain_ref,
     gains_ref,
-    cos_ref,
-    sin_ref,
+    table_ref,
     q_ref,
     main_hbm,
     rest_hbm,
@@ -154,7 +158,9 @@
 
     scaled, turned, low = turner(head_dim)
     qg, kg = gains_ref[0:1, :], gains_ref[1:2, :]
-    cosine, sine = cos_ref[...], sin_ref[...]
+    table = table_ref[...]
+    other = pltpu.roll(table, head_dim, 1)
+    cosine, sine = jnp.where(low, table, other), jnp.where(low, other, table)
     hid = hid_ref[...]
     both = contract_last(hid, wkv_ref[...])
     both = jnp.where(low, turned(scaled(both, kg), cosine, sine), both).astype(jnp.bfloat16)
@@ -221,13 +227,11 @@
     )
 
 
-def finish(lat_ref, terms_ref, gate_ref, out_ref):
-    kept = out_ref.shape[0]
-    at = pl.multiple_of(lax.axis_index("tp") * kept, kept)
+def finish(kept_ref, terms_ref, gate_ref, out_ref):
     projected = terms_ref[0].astype(jnp.float32)
     for g in range(1, terms_ref.shape[0]):
         projected = projected + terms_ref[g].astype(jnp.float32)
-    residual = lat_ref[pl.ds(at, kept), :].astype(jnp.float32)
+    residual = kept_ref[...].astype(jnp.float32)
     out_ref[...] = (residual + gate_ref[...] * projected).astype(jnp.bfloat16)
 
 
@@ -280,16 +284,17 @@
         name="modulate",
     )(condition, mod_weight.T)
     modulation = lax.all_to_all(mod_pieces, ("sp", "tp"), 0, 0, tiled=True)
-    cosine, sine = rotary_tables(lax.axis_index("sp") * length, length, 0, head_dim)
+    table = rotary_tables(lax.axis_index("sp") * length, length, 0, head_dim)
 
     wk, wv = w_key.T, w_value.T
-    inverse, ctx_kv, wkv, gains = pl.pallas_call(
+    inverse, ctx_kv, wkv, gains, kept_rows = pl.pallas_call(
         prepare,
         out_shape=(
             shape((length, LANES), single),
             shape((count, LANES), half),
             shape((2 * head_dim, width), half),
             shape((2, LANES), single),
+            shape((kept, width), half),
         ),
         in_specs=in_hbm(4) + in_vmem(2),
         scratch_shapes=[pltpu.VMEM((length, width), half), pltpu.VMEM((count, width), half), dma(4)],
@@ -304,7 +309,7 @@
             shape((sp, rest, LANES), half),
             shape((1, width), single),
         ),
-        in_specs=in_vmem(10),
+        in_specs=in_vmem(9),
         out_specs=tuple(in_vmem(1) + in_hbm(2) + in_vmem(1)),
         scratch_shapes=[
             pltpu.VMEM((length, width), half),
@@ -323,8 +328,7 @@
         modulation,
         norm_gain[None],
         gains,
-        cosine,
-        sine,
+        table,
     )
     all_rest = lax.all_to_all(own_rest, "sp", 0, 0, tiled=True).reshape(sp * rest, LANES)
     all_main = lax.all_gather(own_main, "sp", axis=0, tiled=True)
@@ -349,7 +353,7 @@
         in_specs=in_vmem(3),
         compiler_params=vmem(8),
         name="finish",
-    )(latent[0], terms, gate)
+    )(kept_rows, terms, gate)
     return mixed[None]
 
 

time: 102 us -> 104 us (1.020)
  waiting for transfers between devices: 10.7 us -> 8.46 us
  local copies, waits for them, and re-layouts: 0.99 us -> 3.18 us
  blocking collectives: 52.2 us -> 54 us
    all_to_all x1, waiting for transfers between devices: 10.7 us -> 8.46 us  [shards(): modulation = lax.all_to_all(mod_pieces, ('sp', 'tp'), 0, 0, tiled=True)]
    unnamed x20 -> x18, local copies, waits for them, and re-layouts: 0.99 us -> 3.18 us
where the time goes in v9:
time: 104 us
  blocking collectives  54 us (52%)
  starting transfers between devices  23 us (22%)
  Pallas kernels  14.1 us (14%)
  waiting for transfers between devices  8.46 us (8%)
  local copies, waits for them, and re-layouts  3.18 us (3%)
    all_gather x1, blocking collectives, shards(): all_main = lax.all_gather(own_main, 'sp', axis=0, tiled=True)  39 us
    all_to_all x1, starting transfers between devices, shards(): modulation = lax.all_to_all(mod_pieces, ('sp', 'tp'), 0, 0, tiled=True)  18.9 us
    all_to_all x1, blocking collectives, shards(): lax.all_to_all(terms.reshape(tp, kept, width), 'tp', 0, 0, tiled=True)  14.9 us
    all_to_all x1, waiting for transfers between devices, shards(): modulation = lax.all_to_all(mod_pieces, ('sp', 'tp'), 0, 0, tiled=True)  8.46 us
    pallas_call x1, Pallas kernels, shards(): pl.pallas_call(attend, out_shape=shape((length, width), half), in_specs=i...  6.65 us
    all_to_all x1, starting transfers between devices, shards(): lax.all_to_all(own_rest, 'sp', 0, 0, tiled=True).reshape(sp * rest, LANES)  4.12 us
    unnamed x18, local copies, waits for them, and re-layouts  3.18 us
    pallas_call x1, Pallas kernels, shards(): pl.pallas_call(project, out_shape=(shape((heads, length, LANES), half), s...  2.56 us
  transfers between devices with their start and end apart: 2, of which 1 were waited for; matrix products, arithmetic and copies ran while one was open for 1% of the time, Pallas kernels for 2%

profile of v9, /device:TPU:6, one launch (start us, length us, event | category | flops | bytes accessed | tf_op | source)
XLA Modules:
  0.0 103.7 jit_solution(3658506931146451667)
XLA Ops:
  0.0 0.0 copy-start.3
  0.0 0.0 copy-start.2
  0.0 2.0 %modulate.1 = f32[64,1,96]{2,1,0:T(1,128)} custom-call(bf16[1,2048]{1,0:T(2,128)(2,1)} %cond_hbm.1, bf16[96,2048]{1,0:T(8,128)(2,1)} %bitcast.21), custom_call_target="tpu_custom_call" | custom-call | tf_op jit(solution)/shard_map/modulate/pallas_call | solution.py:274
  2.0 0.0 copy-start
  2.0 18.9 %all-to-all-start = ((f32[64,1,96]{2,1,0:T(1,128)}), f32[64,1,96]{2,1,0:T(1,128)S(1)}, u32[]{:S(2)}, u32[]{:S(2)}) async-start(f32[64,1,96]{2,1,0:T(1,128)} %modulate.1), calls=%async_computation | async-start | bytes 65536 | tf_op jit(solution)/shard_map/all_to_all | solution.py:286
  21.0 0.7 fusion.table_ref
  21.7 0.0 copy-done.3
  21.7 0.0 copy-start.4
  21.7 0.9 copy-done.4
  22.7 0.0 copy-start.5
  22.7 0.9 copy-done.5
  23.6 0.0 copy-start.7
  23.6 0.7 copy-done.7
  24.2 0.0 copy-start.8
  24.2 0.7 copy-done.8
  24.9 2.1 %prepare.1 = (f32[256,128]{1,0:T(8,128)S(1)}, bf16[32,128]{1,0:T(8,128)(2,1)S(1)}, bf16[128,2048]{1,0:T(8,128)(2,1)S(1)}, f32[2,128]{1,0:T(2,128)S(1)}, bf16[64,2048]{1,0:T(8,128)(2,1)S(1)}) custom-call(bf16[256,2048]{1,0:T(8,128)(2,1)} %bitcast.12, bf16[32,2048]{1,0:T(8,128)(2,1)S(1)} %bitcast.17, bf16[64,2048]{1,0:T(8,128)(2,1)S(1)} %bitcast.15, ...), custom_call_target="tpu_custom_call" | custom-call | tf_op jit(solution)/shard_map/prepare/pallas_call | solution.py:290
  27.0 0.0 copy-start.6
  27.0 8.5 %all-to-all-done.mod_ref = f32[64,1,96]{2,1,0:T(1,128)S(1)} async-done(((f32[64,1,96]{2,1,0:T(1,128)}), f32[64,1,96]{2,1,0:T(1,128)S(1)}, u32[]{:S(2)}, u32[]{:S(2)}) %all-to-all-start) | async-done | bytes 24608 | tf_op jit(solution)/shard_map/all_to_all | solution.py:286
  35.4 0.0 copy-done.2
  35.4 0.0 copy-done
  35.4 0.0 copy-done.6
  35.5 2.6 %project.1 = (bf16[4,256,128]{2,1,0:T(8,128)(2,1)S(1)}, bf16[248,128]{1,0:T(8,128)(2,1)S(1)}, bf16[16,40,128]{2,1,0:T(8,128)(2,1)}, f32[1,2048]{1,0:T(1,128)S(1)}) custom-call(bf16[256,2048]{1,0:T(8,128)(2,1)S(1)} %bitcast.13, bf16[2048,256]{1,0:T(8,128)(2,1)S(1)} %copy-done.2, bf16[128,2048]{1,0:T(8,128)(2,1)S(1)} %get-tuple-element.15.wkv_ref, ...), custom_call_target="tpu_custom_call" | custom-call | tf_op jit(solution)/shard_map/project/pallas_call | solution.py:304
  38.0 0.0 copy-start.1
  38.0 4.1 %all-to-all-start.1 = ((bf16[16,40,128]{2,1,0:T(8,128)(2,1)}), bf16[16,40,128]{2,1,0:T(8,128)(2,1)S(1)}, u32[]{:S(2)}, u32[]{:S(2)}) async-start(bf16[16,40,128]{2,1,0:T(8,128)(2,1)} %get-tuple-element.21), calls=%async_computation.1 | async-start | bytes 327680 | tf_op jit(solution)/shard_map/all_to_all | solution.py:333
  42.2 39.0 %all_gather.3.main_ref = bf16[3968,128]{1,0:T(8,128)(2,1)S(1)} all-gather(bf16[248,128]{1,0:T(8,128)(2,1)S(1)} %get-tuple-element.20), channel_id=1, replica_groups=mesh['sp'=16,'tp'=4,'dp'=8] {'sp'}, dimensions={0}, use_global_device_ids=true | all-gather | bytes 1079296 | tf_op jit(solution)/shard_map/all_gather | solution.py:334
  81.2 0.0 all-to-all-done.1
  81.2 0.0 copy-done.1
  81.2 6.7 %attend.1 = bf16[256,2048]{1,0:T(8,128)(2,1)S(1)} custom-call(bf16[4,256,128]{2,1,0:T(8,128)(2,1)S(1)} %get-tuple-element.19.q_ref, bf16[3968,128]{1,0:T(8,128)(2,1)S(1)} %all_gather.3.main_ref, bf16[640,128]{1,0:T(8,128)(2,1)S(1)} %bitcast.14, bf16[256,2048]{1,0:T(8,128)(2,1)S(1)} %copy-done.1), custom_call_target="tpu_custom_call" | custom-call | tf_op jit(solution)/shard_map/attend/pallas_call | solution.py:336
  87.9 14.9 %all_to_all.15.terms_ref = bf16[4,64,2048]{2,1,0:T(8,128)(2,1)S(1)} all-to-all(bf16[4,64,2048]{2,1,0:T(8,128)(2,1)S(1)} %bitcast.11), channel_id=1, replica_groups=mesh['sp'=16,'tp'=4,'dp'=8] {'tp'}, dimensions={0} | all-to-all | bytes 2097152 | tf_op jit(solution)/shard_map/all_to_all | solution.py:349
  102.8 0.9 finish.1
  (9 shorter events, 0.1 us)
Async XLA Ops:
  0.0 21.7 %copy-start.3 = (bf16[2048,64]{0,1:T(8,128)(2,1)S(1)}, bf16[2048,64]{0,1:T(8,128)(2,1)}, u32[]{:S(2)}) copy-start(bf16[2048,64]{0,1:T(8,128)(2,1)} %param.17) | copy-start | bytes 786436
  0.0 35.4 %copy-start.2 = (bf16[2048,256]{1,0:T(8,128)(2,1)S(1)}, bf16[2048,256]{1,0:T(8,128)(2,1)}, u32[]{:S(2)}) copy-start(bf16[2048,256]{1,0:T(8,128)(2,1)} %wq_ref.1) | copy-start | bytes 3145732
  2.0 33.5 %copy-start = (bf16[1,256,2048]{2,1,0:T(8,128)(2,1)S(1)}, bf16[1,256,2048]{2,1,0:T(8,128)(2,1)}, u32[]{:S(2)}) copy-start(bf16[1,256,2048]{2,1,0:T(8,128)(2,1)} %param.11) | copy-start | bytes 3145732
  2.0 33.4 %all-to-all-start = ((f32[64,1,96]{2,1,0:T(1,128)}), f32[64,1,96]{2,1,0:T(1,128)S(1)}, u32[]{:S(2)}, u32[]{:S(2)}) async-start(f32[64,1,96]{2,1,0:T(1,128)} %modulate.1), calls=%async_computation | async-start | bytes 65536 | tf_op jit(solution)/shard_map/all_to_all | solution.py:286
  21.7 1.0 copy-start.4
  22.7 0.9 copy-start.5
  23.6 0.7 copy-start.7
  24.2 0.7 copy-start.8
  27.0 8.5 %copy-start.6 = (f32[2048]{0:T(1024)S(1)}, f32[2048]{0:T(1024)}, u32[]{:S(2)}) copy-start(f32[2048]{0:T(1024)} %param.15) | copy-start | bytes 24580
  38.0 43.2 %copy-start.1 = (bf16[256,2048]{1,0:T(8,128)(2,1)S(1)}, bf16[256,2048]{1,0:T(8,128)(2,1)}, u32[]{:S(2)}) copy-start(bf16[256,2048]{1,0:T(8,128)(2,1)} %w_hbm.1) | copy-start | bytes 3145732
  38.0 43.2 %all-to-all-start.1 = ((bf16[16,40,128]{2,1,0:T(8,128)(2,1)}), bf16[16,40,128]{2,1,0:T(8,128)(2,1)S(1)}, u32[]{:S(2)}, u32[]{:S(2)}) async-start(bf16[16,40,128]{2,1,0:T(8,128)(2,1)} %get-tuple-element.21), calls=%async_computation.1 | async-start | bytes 327680 | tf_op jit(solution)/shard_map/all_to_all | solution.py:333

commit v10 on v8

--- a/solution.py
+++ b/solution.py
@@ -140,8 +140,10 @@
     rest = rest_hbm.shape[1]
     head_dim = wkv_ref.shape[0] // 2
     pieces, _, piece = mod_ref.shape
+    tp = lax.axis_size("tp")
     for j in range(pieces):
-        mods_ref[0:1, piece * j : piece * (j + 1)] = mod_ref[j]
+        at = piece * (j % (pieces // tp) * tp + j // (pieces // tp))
+        mods_ref[0:1, at : at + piece] = mod_ref[j]
     shift = mods_ref[0:1, 0:width]
     scale = 1.0 + mods_ref[0:1, width : 2 * width]
     gate_ref[...] = mods_ref[0:1, 2 * width : 3 * width]
@@ -279,7 +281,7 @@
         compiler_params=vmem(60),
         name="modulate",
     )(condition, mod_weight.T)
-    modulation = lax.all_to_all(mod_pieces, ("sp", "tp"), 0, 0, tiled=True)
+    modulation = lax.all_to_all(mod_pieces, ("tp", "sp"), 0, 0, tiled=True)
     cosine, sine = rotary_tables(lax.axis_index("sp") * length, length, 0, head_dim)
 
     wk, wv = w_key.T, w_value.T

time: 102 us -> 102 us (level)
  no operation moved by 1% of the time
where the time goes in v10:
time: 102 us; the launch traced here: 101 us
  blocking collectives  52.4 us (51%)
  starting transfers between devices  22.5 us (22%)
  Pallas kernels  14.1 us (14%)
  waiting for transfers between devices  10.5 us (10%)
    all_gather x1, blocking collectives, shards(): all_main = lax.all_gather(own_main, 'sp', axis=0, tiled=True)  38.2 us
    all_to_all x1, starting transfers between devices, shards(): modulation = lax.all_to_all(mod_pieces, ('tp', 'sp'), 0, 0, tiled=True)  18.9 us
    all_to_all x1, blocking collectives, shards(): lax.all_to_all(terms.reshape(tp, kept, width), 'tp', 0, 0, tiled=True)  14.2 us
    all_to_all x1, waiting for transfers between devices, shards(): modulation = lax.all_to_all(mod_pieces, ('tp', 'sp'), 0, 0, tiled=True)  10.5 us
    pallas_call x1, Pallas kernels, shards(): pl.pallas_call(attend, out_shape=shape((length, width), half), in_specs=i...  6.65 us
    all_to_all x1, starting transfers between devices, shards(): lax.all_to_all(own_rest, 'sp', 0, 0, tiled=True).reshape(sp * rest, LANES)  3.66 us
    pallas_call x1, Pallas kernels, shards(): pl.pallas_call(project, out_shape=(shape((heads, length, LANES), half), s...  2.56 us
    pallas_call x1, Pallas kernels, shards(): pl.pallas_call(prepare, out_shape=(shape((length, LANES), single), shape(...  2.06 us
  transfers between devices with their start and end apart: 2, of which 1 were waited for; matrix products, arithmetic and copies ran while one was open for 1% of the time, Pallas kernels for 2%

profile of v10, /device:TPU:6, one launch (start us, length us, event | category | flops | bytes accessed | tf_op | source)
XLA Modules:
  0.0 101.5 jit_solution(11323729410357532951)
XLA Ops:
  0.0 0.0 copy-start.3
  0.0 0.0 copy-start.5
  0.0 0.0 copy-start.8
  0.0 0.0 copy-start.9
  0.0 1.9 %modulate.1 = f32[64,1,96]{2,1,0:T(1,128)} custom-call(bf16[1,2048]{1,0:T(2,128)(2,1)} %cond_hbm.1, bf16[96,2048]{1,0:T(8,128)(2,1)} %bitcast.22), custom_call_target="tpu_custom_call" | custom-call | tf_op jit(solution)/shard_map/modulate/pallas_call | solution.py:272
  2.0 0.0 copy-start
  2.0 0.0 copy-start.2
  2.0 18.9 %all-to-all-start = ((f32[64,1,96]{2,1,0:T(1,128)}), f32[64,1,96]{2,1,0:T(1,128)S(1)}, u32[]{:S(2)}, u32[]{:S(2)}) async-start(f32[64,1,96]{2,1,0:T(1,128)} %modulate.1), calls=%async_computation | async-start | bytes 65536 | tf_op jit(solution)/shard_map/all_to_all | solution.py:284
  21.0 0.7 negate_select_fusion
  21.7 0.0 copy-done.3
  21.7 0.0 copy-done.5
  21.7 0.0 copy-done.8
  21.7 0.0 copy-done.9
  21.7 0.0 copy-start.4
  21.7 0.9 copy-done.4
  22.6 2.1 %prepare.1 = (f32[256,128]{1,0:T(8,128)S(1)}, bf16[32,128]{1,0:T(8,128)(2,1)S(1)}, bf16[128,2048]{1,0:T(8,128)(2,1)S(1)}, f32[2,128]{1,0:T(2,128)S(1)}) custom-call(bf16[256,2048]{1,0:T(8,128)(2,1)} %bitcast.11, bf16[32,2048]{1,0:T(8,128)(2,1)S(1)} %bitcast.18, bf16[64,2048]{1,0:T(8,128)(2,1)S(1)} %bitcast.16, bf16[64,2048]{1,0:T(8,128)(2,1)S(1)} %bitcast.17, ...), custom_call_target="tpu_custom_call" | custom-call | tf_op jit(solution)/shard_map/prepare/pallas_call | solution.py:288
  24.7 0.0 copy-start.7
  24.7 10.5 %all-to-all-done.mod_ref = f32[64,1,96]{2,1,0:T(1,128)S(1)} async-done(((f32[64,1,96]{2,1,0:T(1,128)}), f32[64,1,96]{2,1,0:T(1,128)S(1)}, u32[]{:S(2)}, u32[]{:S(2)}) %all-to-all-start) | async-done | bytes 24608 | tf_op jit(solution)/shard_map/all_to_all | solution.py:284
  35.2 0.0 copy-done
  35.2 0.0 copy-done.2
  35.2 0.0 copy-done.7
  35.2 2.6 %project.1 = (bf16[4,256,128]{2,1,0:T(8,128)(2,1)S(1)}, bf16[248,128]{1,0:T(8,128)(2,1)S(1)}, bf16[16,40,128]{2,1,0:T(8,128)(2,1)}, f32[1,2048]{1,0:T(1,128)S(1)}) custom-call(bf16[256,2048]{1,0:T(8,128)(2,1)S(1)} %bitcast.12, bf16[2048,256]{1,0:T(8,128)(2,1)S(1)} %copy-done.2, bf16[128,2048]{1,0:T(8,128)(2,1)S(1)} %get-tuple-element.13.wkv_ref, ...), custom_call_target="tpu_custom_call" | custom-call | tf_op jit(solution)/shard_map/project/pallas_call | solution.py:301
  37.8 0.0 copy-start.6
  37.8 0.0 copy-start.1
  37.8 3.7 %all-to-all-start.1 = ((bf16[16,40,128]{2,1,0:T(8,128)(2,1)}), bf16[16,40,128]{2,1,0:T(8,128)(2,1)S(1)}, u32[]{:S(2)}, u32[]{:S(2)}) async-start(bf16[16,40,128]{2,1,0:T(8,128)(2,1)} %get-tuple-element.19), calls=%async_computation.1 | async-start | bytes 327680 | tf_op jit(solution)/shard_map/all_to_all | solution.py:331
  41.5 0.0 copy-done.6
  41.5 38.2 %all_gather.3.main_ref = bf16[3968,128]{1,0:T(8,128)(2,1)S(1)} all-gather(bf16[248,128]{1,0:T(8,128)(2,1)} %copy-done.6), channel_id=1, replica_groups=mesh['sp'=16,'tp'=4,'dp'=8] {'sp'}, dimensions={0}, use_global_device_ids=true | all-gather | bytes 1079296 | tf_op jit(solution)/shard_map/all_gather | solution.py:332
  79.7 0.0 all-to-all-done.1
  79.8 0.0 copy-done.1
  79.8 6.6 %attend.1 = bf16[256,2048]{1,0:T(8,128)(2,1)S(1)} custom-call(bf16[4,256,128]{2,1,0:T(8,128)(2,1)S(1)} %get-tuple-element.17.q_ref, bf16[3968,128]{1,0:T(8,128)(2,1)S(1)} %all_gather.3.main_ref, bf16[640,128]{1,0:T(8,128)(2,1)S(1)} %bitcast.15, bf16[256,2048]{1,0:T(8,128)(2,1)S(1)} %copy-done.1), custom_call_target="tpu_custom_call" | custom-call | tf_op jit(solution)/shard_map/attend/pallas_call | solution.py:334
  86.4 14.2 %all_to_all.15.terms_ref = bf16[4,64,2048]{2,1,0:T(8,128)(2,1)S(1)} all-to-all(bf16[4,64,2048]{2,1,0:T(8,128)(2,1)S(1)} %bitcast.14), channel_id=1, replica_groups=mesh['sp'=16,'tp'=4,'dp'=8] {'tp'}, dimensions={0} | all-to-all | bytes 2097152 | tf_op jit(solution)/shard_map/all_to_all | solution.py:347
  100.6 0.9 finish.1
  (9 shorter events, 0.1 us)
Async XLA Ops:
  0.0 21.7 %copy-start.3 = (bf16[2048,64]{0,1:T(8,128)(2,1)S(1)}, bf16[2048,64]{0,1:T(8,128)(2,1)}, u32[]{:S(2)}) copy-start(bf16[2048,64]{0,1:T(8,128)(2,1)} %param.17) | copy-start | bytes 786436
  0.0 21.7 %copy-start.5 = (bf16[1,32,2048]{2,1,0:T(8,128)(2,1)S(1)}, bf16[1,32,2048]{2,1,0:T(8,128)(2,1)}, u32[]{:S(2)}) copy-start(bf16[1,32,2048]{2,1,0:T(8,128)(2,1)} %param.12) | copy-start | bytes 393220
  0.0 21.7 %copy-start.8 = (f32[64]{0:T(128)S(1)}, f32[64]{0:T(128)}, u32[]{:S(2)}) copy-start(f32[64]{0:T(128)} %param.19) | copy-start | bytes 772
  0.0 21.7 %copy-start.9 = (f32[64]{0:T(128)S(1)}, f32[64]{0:T(128)}, u32[]{:S(2)}) copy-start(f32[64]{0:T(128)} %param.20) | copy-start | bytes 772
  2.0 33.3 %copy-start = (bf16[1,256,2048]{2,1,0:T(8,128)(2,1)S(1)}, bf16[1,256,2048]{2,1,0:T(8,128)(2,1)}, u32[]{:S(2)}) copy-start(bf16[1,256,2048]{2,1,0:T(8,128)(2,1)} %param.11) | copy-start | bytes 3145732
  2.0 33.3 %copy-start.2 = (bf16[2048,256]{1,0:T(8,128)(2,1)S(1)}, bf16[2048,256]{1,0:T(8,128)(2,1)}, u32[]{:S(2)}) copy-start(bf16[2048,256]{1,0:T(8,128)(2,1)} %wq_ref.1) | copy-start | bytes 3145732
  2.0 33.3 %all-to-all-start = ((f32[64,1,96]{2,1,0:T(1,128)}), f32[64,1,96]{2,1,0:T(1,128)S(1)}, u32[]{:S(2)}, u32[]{:S(2)}) async-start(f32[64,1,96]{2,1,0:T(1,128)} %modulate.1), calls=%async_computation | async-start | bytes 65536 | tf_op jit(solution)/shard_map/all_to_all | solution.py:284
  21.7 1.0 copy-start.4
  24.7 10.5 %copy-start.7 = (f32[2048]{0:T(1024)S(1)}, f32[2048]{0:T(1024)}, u32[]{:S(2)}) copy-start(f32[2048]{0:T(1024)} %param.15) | copy-start | bytes 24580
  37.8 3.7 %copy-start.6 = (bf16[248,128]{1,0:T(8,128)(2,1)}, bf16[248,128]{1,0:T(8,128)(2,1)S(1)}, u32[]{:S(2)}) copy-start(bf16[248,128]{1,0:T(8,128)(2,1)S(1)} %get-tuple-element.18) | copy-start | bytes 190468
  37.8 41.9 %copy-start.1 = (bf16[256,2048]{1,0:T(8,128)(2,1)S(1)}, bf16[256,2048]{1,0:T(8,128)(2,1)}, u32[]{:S(2)}) copy-start(bf16[256,2048]{1,0:T(8,128)(2,1)} %w_hbm.1) | copy-start | bytes 3145732
  37.8 41.9 %all-to-all-start.1 = ((bf16[16,40,128]{2,1,0:T(8,128)(2,1)}), bf16[16,40,128]{2,1,0:T(8,128)(2,1)S(1)}, u32[]{:S(2)}, u32[]{:S(2)}) async-start(bf16[16,40,128]{2,1,0:T(8,128)(2,1)} %get-tuple-element.19), calls=%async_computation.1 | async-start | bytes 327680 | tf_op jit(solution)/shard_map/all_to_all | solution.py:331

commit v11 on v10

--- a/solution.py
+++ b/solution.py
@@ -63,12 +63,17 @@
 
 
 def modulate(cond_hbm, w_hbm, out_ref, cond_ref, w_ref, sems):
-    cond_in, copy = start_all(((cond_hbm, cond_ref), (w_hbm, w_ref)), sems)
+    rows = w_ref.shape[0] // 4
+    cuts = [pl.ds(rows * k, rows) for k in range(4)]
+    cond_in, *copies = start_all(
+        [(cond_hbm, cond_ref)] + [(w_hbm.at[cut], w_ref.at[cut]) for cut in cuts], sems
+    )
     cond_in.wait()
     cond = cond_ref[...].astype(jnp.float32)
     active = (cond / (1.0 + jnp.exp(-cond))).astype(jnp.bfloat16)
     active = jnp.broadcast_to(active, (16, active.shape[1]))
-    copy.wait()
+    for copy in copies:
+        copy.wait()
     piece = contract_last(active, w_ref[...])[0:1]
     out_ref[...] = jnp.broadcast_to(piece[None], out_ref.shape)
 
@@ -276,7 +281,7 @@
         scratch_shapes=[
             pltpu.VMEM(condition.shape, half),
             pltpu.VMEM(mod_weight.shape[::-1], half),
-            dma(2),
+            dma(5),
         ],
         compiler_params=vmem(60),
         name="modulate",

time: 102 us -> 102 us (level)
  no operation moved by 1% of the time
where the time goes in v11:
time: 102 us
  blocking collectives  52.4 us (51%)
  starting transfers between devices  22.5 us (22%)
  Pallas kernels  14.1 us (14%)
  waiting for transfers between devices  10.5 us (10%)
    all_gather x1, blocking collectives, shards(): all_main = lax.all_gather(own_main, 'sp', axis=0, tiled=True)  38.2 us
    all_to_all x1, starting transfers between devices, shards(): modulation = lax.all_to_all(mod_pieces, ('tp', 'sp'), 0, 0, tiled=True)  18.9 us
    all_to_all x1, blocking collectives, shards(): lax.all_to_all(terms.reshape(tp, kept, width), 'tp', 0, 0, tiled=True)  14.2 us
    all_to_all x1, waiting for transfers between devices, shards(): modulation = lax.all_to_all(mod_pieces, ('tp', 'sp'), 0, 0, tiled=True)  10.5 us
    pallas_call x1, Pallas kernels, shards(): pl.pallas_call(attend, out_shape=shape((length, width), half), in_specs=i...  6.65 us
    all_to_all x1, starting transfers between devices, shards(): lax.all_to_all(own_rest, 'sp', 0, 0, tiled=True).reshape(sp * rest, LANES)  3.66 us
    pallas_call x1, Pallas kernels, shards(): pl.pallas_call(project, out_shape=(shape((heads, length, LANES), half), s...  2.56 us
    pallas_call x1, Pallas kernels, shards(): pl.pallas_call(prepare, out_shape=(shape((length, LANES), single), shape(...  2.06 us
  transfers between devices with their start and end apart: 2, of which 1 were waited for; matrix products, arithmetic and copies ran while one was open for 1% of the time, Pallas kernels for 2%

profile of v11, /device:TPU:6, one launch (start us, length us, event | category | flops | bytes accessed | tf_op | source)
XLA Modules:
  0.0 101.5 jit_solution(11296839118639388952)
XLA Ops:
  0.0 0.0 copy-start.3
  0.0 0.0 copy-start.5
  0.0 0.0 copy-start.8
  0.0 0.0 copy-start.9
  0.0 2.0 %modulate.1 = f32[64,1,96]{2,1,0:T(1,128)} custom-call(bf16[1,2048]{1,0:T(2,128)(2,1)} %cond_hbm.1, bf16[96,2048]{1,0:T(8,128)(2,1)} %bitcast.22), custom_call_target="tpu_custom_call" | custom-call | tf_op jit(solution)/shard_map/modulate/pallas_call | solution.py:277
  2.0 0.0 copy-start
  2.0 0.0 copy-start.2
  2.0 18.9 %all-to-all-start = ((f32[64,1,96]{2,1,0:T(1,128)}), f32[64,1,96]{2,1,0:T(1,128)S(1)}, u32[]{:S(2)}, u32[]{:S(2)}) async-start(f32[64,1,96]{2,1,0:T(1,128)} %modulate.1), calls=%async_computation | async-start | bytes 65536 | tf_op jit(solution)/shard_map/all_to_all | solution.py:289
  21.0 0.7 negate_select_fusion
  21.7 0.0 copy-done.3
  21.7 0.0 copy-done.5
  21.7 0.0 copy-done.8
  21.7 0.0 copy-done.9
  21.8 0.0 copy-start.4
  21.8 0.9 copy-done.4
  22.7 2.1 %prepare.1 = (f32[256,128]{1,0:T(8,128)S(1)}, bf16[32,128]{1,0:T(8,128)(2,1)S(1)}, bf16[128,2048]{1,0:T(8,128)(2,1)S(1)}, f32[2,128]{1,0:T(2,128)S(1)}) custom-call(bf16[256,2048]{1,0:T(8,128)(2,1)} %bitcast.11, bf16[32,2048]{1,0:T(8,128)(2,1)S(1)} %bitcast.18, bf16[64,2048]{1,0:T(8,128)(2,1)S(1)} %bitcast.16, bf16[64,2048]{1,0:T(8,128)(2,1)S(1)} %bitcast.17, ...), custom_call_target="tpu_custom_call" | custom-call | tf_op jit(solution)/shard_map/prepare/pallas_call | solution.py:293
  24.8 0.0 copy-start.7
  24.8 10.5 %all-to-all-done.mod_ref = f32[64,1,96]{2,1,0:T(1,128)S(1)} async-done(((f32[64,1,96]{2,1,0:T(1,128)}), f32[64,1,96]{2,1,0:T(1,128)S(1)}, u32[]{:S(2)}, u32[]{:S(2)}) %all-to-all-start) | async-done | bytes 24608 | tf_op jit(solution)/shard_map/all_to_all | solution.py:289
  35.3 0.0 copy-done
  35.3 0.0 copy-done.2
  35.3 0.0 copy-done.7
  35.3 2.6 %project.1 = (bf16[4,256,128]{2,1,0:T(8,128)(2,1)S(1)}, bf16[248,128]{1,0:T(8,128)(2,1)S(1)}, bf16[16,40,128]{2,1,0:T(8,128)(2,1)}, f32[1,2048]{1,0:T(1,128)S(1)}) custom-call(bf16[256,2048]{1,0:T(8,128)(2,1)S(1)} %bitcast.12, bf16[2048,256]{1,0:T(8,128)(2,1)S(1)} %copy-done.2, bf16[128,2048]{1,0:T(8,128)(2,1)S(1)} %get-tuple-element.13.wkv_ref, ...), custom_call_target="tpu_custom_call" | custom-call | tf_op jit(solution)/shard_map/project/pallas_call | solution.py:306
  37.9 0.0 copy-start.6
  37.9 0.0 copy-start.1
  37.9 3.7 %all-to-all-start.1 = ((bf16[16,40,128]{2,1,0:T(8,128)(2,1)}), bf16[16,40,128]{2,1,0:T(8,128)(2,1)S(1)}, u32[]{:S(2)}, u32[]{:S(2)}) async-start(bf16[16,40,128]{2,1,0:T(8,128)(2,1)} %get-tuple-element.19), calls=%async_computation.1 | async-start | bytes 327680 | tf_op jit(solution)/shard_map/all_to_all | solution.py:336
  41.6 0.0 copy-done.6
  41.6 38.2 %all_gather.3.main_ref = bf16[3968,128]{1,0:T(8,128)(2,1)S(1)} all-gather(bf16[248,128]{1,0:T(8,128)(2,1)} %copy-done.6), channel_id=1, replica_groups=mesh['sp'=16,'tp'=4,'dp'=8] {'sp'}, dimensions={0}, use_global_device_ids=true | all-gather | bytes 1079296 | tf_op jit(solution)/shard_map/all_gather | solution.py:337
  79.8 0.0 all-to-all-done.1
  79.8 0.0 copy-done.1
  79.8 6.7 %attend.1 = bf16[256,2048]{1,0:T(8,128)(2,1)S(1)} custom-call(bf16[4,256,128]{2,1,0:T(8,128)(2,1)S(1)} %get-tuple-element.17.q_ref, bf16[3968,128]{1,0:T(8,128)(2,1)S(1)} %all_gather.3.main_ref, bf16[640,128]{1,0:T(8,128)(2,1)S(1)} %bitcast.15, bf16[256,2048]{1,0:T(8,128)(2,1)S(1)} %copy-done.1), custom_call_target="tpu_custom_call" | custom-call | tf_op jit(solution)/shard_map/attend/pallas_call | solution.py:339
  86.5 14.2 %all_to_all.15.terms_ref = bf16[4,64,2048]{2,1,0:T(8,128)(2,1)S(1)} all-to-all(bf16[4,64,2048]{2,1,0:T(8,128)(2,1)S(1)} %bitcast.14), channel_id=1, replica_groups=mesh['sp'=16,'tp'=4,'dp'=8] {'tp'}, dimensions={0} | all-to-all | bytes 2097152 | tf_op jit(solution)/shard_map/all_to_all | solution.py:352
  100.7 0.9 finish.1
  (9 shorter events, 0.1 us)
Async XLA Ops:
  0.0 21.7 %copy-start.3 = (bf16[2048,64]{0,1:T(8,128)(2,1)S(1)}, bf16[2048,64]{0,1:T(8,128)(2,1)}, u32[]{:S(2)}) copy-start(bf16[2048,64]{0,1:T(8,128)(2,1)} %param.17) | copy-start | bytes 786436
  0.0 21.7 %copy-start.5 = (bf16[1,32,2048]{2,1,0:T(8,128)(2,1)S(1)}, bf16[1,32,2048]{2,1,0:T(8,128)(2,1)}, u32[]{:S(2)}) copy-start(bf16[1,32,2048]{2,1,0:T(8,128)(2,1)} %param.12) | copy-start | bytes 393220
  0.0 21.7 %copy-start.8 = (f32[64]{0:T(128)S(1)}, f32[64]{0:T(128)}, u32[]{:S(2)}) copy-start(f32[64]{0:T(128)} %param.19) | copy-start | bytes 772
  0.0 21.7 %copy-start.9 = (f32[64]{0:T(128)S(1)}, f32[64]{0:T(128)}, u32[]{:S(2)}) copy-start(f32[64]{0:T(128)} %param.20) | copy-start | bytes 772
  2.0 33.3 %copy-start = (bf16[1,256,2048]{2,1,0:T(8,128)(2,1)S(1)}, bf16[1,256,2048]{2,1,0:T(8,128)(2,1)}, u32[]{:S(2)}) copy-start(bf16[1,256,2048]{2,1,0:T(8,128)(2,1)} %param.11) | copy-start | bytes 3145732
  2.0 33.3 %copy-start.2 = (bf16[2048,256]{1,0:T(8,128)(2,1)S(1)}, bf16[2048,256]{1,0:T(8,128)(2,1)}, u32[]{:S(2)}) copy-start(bf16[2048,256]{1,0:T(8,128)(2,1)} %wq_ref.1) | copy-start | bytes 3145732
  2.0 33.3 %all-to-all-start = ((f32[64,1,96]{2,1,0:T(1,128)}), f32[64,1,96]{2,1,0:T(1,128)S(1)}, u32[]{:S(2)}, u32[]{:S(2)}) async-start(f32[64,1,96]{2,1,0:T(1,128)} %modulate.1), calls=%async_computation | async-start | bytes 65536 | tf_op jit(solution)/shard_map/all_to_all | solution.py:289
  21.8 1.0 copy-start.4
  24.8 10.5 %copy-start.7 = (f32[2048]{0:T(1024)S(1)}, f32[2048]{0:T(1024)}, u32[]{:S(2)}) copy-start(f32[2048]{0:T(1024)} %param.15) | copy-start | bytes 24580
  37.9 3.7 %copy-start.6 = (bf16[248,128]{1,0:T(8,128)(2,1)}, bf16[248,128]{1,0:T(8,128)(2,1)S(1)}, u32[]{:S(2)}) copy-start(bf16[248,128]{1,0:T(8,128)(2,1)S(1)} %get-tuple-element.18) | copy-start | bytes 190468
  37.9 41.9 %copy-start.1 = (bf16[256,2048]{1,0:T(8,128)(2,1)S(1)}, bf16[256,2048]{1,0:T(8,128)(2,1)}, u32[]{:S(2)}) copy-start(bf16[256,2048]{1,0:T(8,128)(2,1)} %w_hbm.1) | copy-start | bytes 3145732
  37.9 41.9 %all-to-all-start.1 = ((bf16[16,40,128]{2,1,0:T(8,128)(2,1)}), bf16[16,40,128]{2,1,0:T(8,128)(2,1)S(1)}, u32[]{:S(2)}, u32[]{:S(2)}) async-start(bf16[16,40,128]{2,1,0:T(8,128)(2,1)} %get-tuple-element.19), calls=%async_computation.1 | async-start | bytes 327680 | tf_op jit(solution)/shard_map/all_to_all | solution.py:336

commit v12 on v10

--- a/solution.py
+++ b/solution.py
@@ -7,7 +7,7 @@
 
 GRID_W = 64
 LANES = 128
-KEY_STEP = 512
+KEY_STEP = 768
 
 epsilon = 1e-06
 rope_base = 10000.0

time: 102 us -> 102 us (level)
  no operation moved by 1% of the time
where the time goes in v12:
time: 102 us; the launch traced here: 101 us
  blocking collectives  52.4 us (51%)
  starting transfers between devices  22.5 us (22%)
  Pallas kernels  14 us (14%)
  waiting for transfers between devices  10.5 us (10%)
    all_gather x1, blocking collectives, shards(): all_main = lax.all_gather(own_main, 'sp', axis=0, tiled=True)  38.2 us
    all_to_all x1, starting transfers between devices, shards(): modulation = lax.all_to_all(mod_pieces, ('tp', 'sp'), 0, 0, tiled=True)  18.9 us
    all_to_all x1, blocking collectives, shards(): lax.all_to_all(terms.reshape(tp, kept, width), 'tp', 0, 0, tiled=True)  14.2 us
    all_to_all x1, waiting for transfers between devices, shards(): modulation = lax.all_to_all(mod_pieces, ('tp', 'sp'), 0, 0, tiled=True)  10.5 us
    pallas_call x1, Pallas kernels, shards(): pl.pallas_call(attend, out_shape=shape((length, width), half), in_specs=i...  6.61 us
    all_to_all x1, starting transfers between devices, shards(): lax.all_to_all(own_rest, 'sp', 0, 0, tiled=True).reshape(sp * rest, LANES)  3.66 us
    pallas_call x1, Pallas kernels, shards(): pl.pallas_call(project, out_shape=(shape((heads, length, LANES), half), s...  2.56 us
    pallas_call x1, Pallas kernels, shards(): pl.pallas_call(prepare, out_shape=(shape((length, LANES), single), shape(...  2.06 us
  transfers between devices with their start and end apart: 2, of which 1 were waited for; matrix products, arithmetic and copies ran while one was open for 1% of the time, Pallas kernels for 2%

profile of v12, /device:TPU:6, one launch (start us, length us, event | category | flops | bytes accessed | tf_op | source)
XLA Modules:
  0.0 101.4 jit_solution(10350166345248653163)
XLA Ops:
  0.0 0.0 copy-start.3
  0.0 0.0 copy-start.5
  0.0 0.0 copy-start.8
  0.0 0.0 copy-start.9
  0.0 1.9 %modulate.1 = f32[64,1,96]{2,1,0:T(1,128)} custom-call(bf16[1,2048]{1,0:T(2,128)(2,1)} %cond_hbm.1, bf16[96,2048]{1,0:T(8,128)(2,1)} %bitcast.22), custom_call_target="tpu_custom_call" | custom-call | tf_op jit(solution)/shard_map/modulate/pallas_call | solution.py:272
  2.0 0.0 copy-start
  2.0 0.0 copy-start.2
  2.0 18.9 %all-to-all-start = ((f32[64,1,96]{2,1,0:T(1,128)}), f32[64,1,96]{2,1,0:T(1,128)S(1)}, u32[]{:S(2)}, u32[]{:S(2)}) async-start(f32[64,1,96]{2,1,0:T(1,128)} %modulate.1), calls=%async_computation | async-start | bytes 65536 | tf_op jit(solution)/shard_map/all_to_all | solution.py:284
  21.0 0.7 negate_select_fusion
  21.7 0.0 copy-done.3
  21.7 0.0 copy-done.5
  21.7 0.0 copy-done.8
  21.7 0.0 copy-done.9
  21.7 0.0 copy-start.4
  21.7 0.9 copy-done.4
  22.6 2.1 %prepare.1 = (f32[256,128]{1,0:T(8,128)S(1)}, bf16[32,128]{1,0:T(8,128)(2,1)S(1)}, bf16[128,2048]{1,0:T(8,128)(2,1)S(1)}, f32[2,128]{1,0:T(2,128)S(1)}) custom-call(bf16[256,2048]{1,0:T(8,128)(2,1)} %bitcast.11, bf16[32,2048]{1,0:T(8,128)(2,1)S(1)} %bitcast.18, bf16[64,2048]{1,0:T(8,128)(2,1)S(1)} %bitcast.16, bf16[64,2048]{1,0:T(8,128)(2,1)S(1)} %bitcast.17, ...), custom_call_target="tpu_custom_call" | custom-call | tf_op jit(solution)/shard_map/prepare/pallas_call | solution.py:288
  24.7 0.0 copy-start.7
  24.7 10.5 %all-to-all-done.mod_ref = f32[64,1,96]{2,1,0:T(1,128)S(1)} async-done(((f32[64,1,96]{2,1,0:T(1,128)}), f32[64,1,96]{2,1,0:T(1,128)S(1)}, u32[]{:S(2)}, u32[]{:S(2)}) %all-to-all-start) | async-done | bytes 24608 | tf_op jit(solution)/shard_map/all_to_all | solution.py:284
  35.2 0.0 copy-done
  35.2 0.0 copy-done.2
  35.2 0.0 copy-done.7
  35.2 2.6 %project.1 = (bf16[4,256,128]{2,1,0:T(8,128)(2,1)S(1)}, bf16[248,128]{1,0:T(8,128)(2,1)S(1)}, bf16[16,40,128]{2,1,0:T(8,128)(2,1)}, f32[1,2048]{1,0:T(1,128)S(1)}) custom-call(bf16[256,2048]{1,0:T(8,128)(2,1)S(1)} %bitcast.12, bf16[2048,256]{1,0:T(8,128)(2,1)S(1)} %copy-done.2, bf16[128,2048]{1,0:T(8,128)(2,1)S(1)} %get-tuple-element.13.wkv_ref, ...), custom_call_target="tpu_custom_call" | custom-call | tf_op jit(solution)/shard_map/project/pallas_call | solution.py:301
  37.8 0.0 copy-start.6
  37.8 0.0 copy-start.1
  37.8 3.7 %all-to-all-start.1 = ((bf16[16,40,128]{2,1,0:T(8,128)(2,1)}), bf16[16,40,128]{2,1,0:T(8,128)(2,1)S(1)}, u32[]{:S(2)}, u32[]{:S(2)}) async-start(bf16[16,40,128]{2,1,0:T(8,128)(2,1)} %get-tuple-element.19), calls=%async_computation.1 | async-start | bytes 327680 | tf_op jit(solution)/shard_map/all_to_all | solution.py:331
  41.5 0.0 copy-done.6
  41.5 38.2 %all_gather.3.main_ref = bf16[3968,128]{1,0:T(8,128)(2,1)S(1)} all-gather(bf16[248,128]{1,0:T(8,128)(2,1)} %copy-done.6), channel_id=1, replica_groups=mesh['sp'=16,'tp'=4,'dp'=8] {'sp'}, dimensions={0}, use_global_device_ids=true | all-gather | bytes 1079296 | tf_op jit(solution)/shard_map/all_gather | solution.py:332
  79.7 0.0 all-to-all-done.1
  79.8 0.0 copy-done.1
  79.8 6.6 %attend.1 = bf16[256,2048]{1,0:T(8,128)(2,1)S(1)} custom-call(bf16[4,256,128]{2,1,0:T(8,128)(2,1)S(1)} %get-tuple-element.17.q_ref, bf16[3968,128]{1,0:T(8,128)(2,1)S(1)} %all_gather.3.main_ref, bf16[640,128]{1,0:T(8,128)(2,1)S(1)} %bitcast.15, bf16[256,2048]{1,0:T(8,128)(2,1)S(1)} %copy-done.1), custom_call_target="tpu_custom_call" | custom-call | tf_op jit(solution)/shard_map/attend/pallas_call | solution.py:334
  86.4 14.2 %all_to_all.15.terms_ref = bf16[4,64,2048]{2,1,0:T(8,128)(2,1)S(1)} all-to-all(bf16[4,64,2048]{2,1,0:T(8,128)(2,1)S(1)} %bitcast.14), channel_id=1, replica_groups=mesh['sp'=16,'tp'=4,'dp'=8] {'tp'}, dimensions={0} | all-to-all | bytes 2097152 | tf_op jit(solution)/shard_map/all_to_all | solution.py:347
  100.6 0.9 finish.1
  (9 shorter events, 0.1 us)
Async XLA Ops:
  0.0 21.7 %copy-start.3 = (bf16[2048,64]{0,1:T(8,128)(2,1)S(1)}, bf16[2048,64]{0,1:T(8,128)(2,1)}, u32[]{:S(2)}) copy-start(bf16[2048,64]{0,1:T(8,128)(2,1)} %param.17) | copy-start | bytes 786436
  0.0 21.7 %copy-start.5 = (bf16[1,32,2048]{2,1,0:T(8,128)(2,1)S(1)}, bf16[1,32,2048]{2,1,0:T(8,128)(2,1)}, u32[]{:S(2)}) copy-start(bf16[1,32,2048]{2,1,0:T(8,128)(2,1)} %param.12) | copy-start | bytes 393220
  0.0 21.7 %copy-start.8 = (f32[64]{0:T(128)S(1)}, f32[64]{0:T(128)}, u32[]{:S(2)}) copy-start(f32[64]{0:T(128)} %param.19) | copy-start | bytes 772
  0.0 21.7 %copy-start.9 = (f32[64]{0:T(128)S(1)}, f32[64]{0:T(128)}, u32[]{:S(2)}) copy-start(f32[64]{0:T(128)} %param.20) | copy-start | bytes 772
  2.0 33.3 %copy-start = (bf16[1,256,2048]{2,1,0:T(8,128)(2,1)S(1)}, bf16[1,256,2048]{2,1,0:T(8,128)(2,1)}, u32[]{:S(2)}) copy-start(bf16[1,256,2048]{2,1,0:T(8,128)(2,1)} %param.11) | copy-start | bytes 3145732
  2.0 33.3 %copy-start.2 = (bf16[2048,256]{1,0:T(8,128)(2,1)S(1)}, bf16[2048,256]{1,0:T(8,128)(2,1)}, u32[]{:S(2)}) copy-start(bf16[2048,256]{1,0:T(8,128)(2,1)} %wq_ref.1) | copy-start | bytes 3145732
  2.0 33.3 %all-to-all-start = ((f32[64,1,96]{2,1,0:T(1,128)}), f32[64,1,96]{2,1,0:T(1,128)S(1)}, u32[]{:S(2)}, u32[]{:S(2)}) async-start(f32[64,1,96]{2,1,0:T(1,128)} %modulate.1), calls=%async_computation | async-start | bytes 65536 | tf_op jit(solution)/shard_map/all_to_all | solution.py:284
  21.7 1.0 copy-start.4
  24.7 10.5 %copy-start.7 = (f32[2048]{0:T(1024)S(1)}, f32[2048]{0:T(1024)}, u32[]{:S(2)}) copy-start(f32[2048]{0:T(1024)} %param.15) | copy-start | bytes 24580
  37.8 3.7 %copy-start.6 = (bf16[248,128]{1,0:T(8,128)(2,1)}, bf16[248,128]{1,0:T(8,128)(2,1)S(1)}, u32[]{:S(2)}) copy-start(bf16[248,128]{1,0:T(8,128)(2,1)S(1)} %get-tuple-element.18) | copy-start | bytes 190468
  37.8 41.9 %copy-start.1 = (bf16[256,2048]{1,0:T(8,128)(2,1)S(1)}, bf16[256,2048]{1,0:T(8,128)(2,1)}, u32[]{:S(2)}) copy-start(bf16[256,2048]{1,0:T(8,128)(2,1)} %w_hbm.1) | copy-start | bytes 3145732
  37.8 41.9 %all-to-all-start.1 = ((bf16[16,40,128]{2,1,0:T(8,128)(2,1)}), bf16[16,40,128]{2,1,0:T(8,128)(2,1)S(1)}, u32[]{:S(2)}, u32[]{:S(2)}) async-start(bf16[16,40,128]{2,1,0:T(8,128)(2,1)} %get-tuple-element.19), calls=%async_computation.1 | async-start | bytes 327680 | tf_op jit(solution)/shard_map/all_to_all | solution.py:331
